TPU v7x, 256 devices: a whole 4x4x8 slice. The times are simulated.
256 devices in a mesh: sp: 32 (over z, y), tp: 8 (over x, core).
Axes of the slice: x: 4, y: 4, z: 8, core: 2. Of those that a mesh axis runs over, the one named last changes fastest.
Arguments:
- tokens: bfloat16 [16384, 2048], P(('sp', 'tp')), may hold values from -8 to 8, as said below
- w_query: bfloat16 [2048, 1024], P(None, 'tp'), may hold values from -0.125 to 0.125
- w_key: bfloat16 [2048, 1024], P(None, 'tp'), may hold values from -0.125 to 0.125
- w_value: bfloat16 [2048, 1024], P(None, 'tp'), may hold values from -0.125 to 0.125
- head_bias: float32 [16], P('tp'), may hold values from -40 to -3
- w_out: bfloat16 [1024, 2048], P('tp'), may hold values from -0.1875 to 0.1875
Outputs:
- mixed: bfloat16 [16384, 2048], P(('sp', 'tp'))
Inputs may be any that keep to these rules, and one draw needn't show every extreme that they name: `tokens`: activations of order one whose mean shifts between blocks of 512 positions.
All inputs are finite; a program needn't handle non-finite values.
Results may differ from a plain program's by a relative error of at most 0.014.
Values may be sent and summed in bfloat16 or wider, within the bound.
No kernel may reach another device: no remote copies, remote signals or barrier semaphores. Data moves between devices by JAX's collectives and lax.ppermute only.
A program may use at most 128 MiB of HBM per device.

v0:
```python
import jax
import jax.numpy as jnp
from jax import lax
from jax.experimental import pallas as pl
from jax.experimental.pallas import tpu as pltpu
from jax.sharding import PartitionSpec as P

Z, Y, X, C = 8, 4, 4, 2
AXES = ("sp", "tp")
LANES = 128
TOK = 512
ROWS = 64
HEAD = 64
QROWS = 80
RUN = 16
CHUNK = 8 * RUN
DEPTH = 256
ZSEGS = 4


def moves(target):
    def index(z, y, x, c):
        return ((z * Y + y) * X + x) * C + c

    return [
        (index(z, y, x, c), index(*target(z, y, x, c)))
        for z in range(Z)
        for y in range(Y)
        for x in range(X)
        for c in range(C)
    ]


Z_FIRST = moves(lambda z, y, x, c: ((z + 1 - 2 * c) % Z, y, x, c))
Z_SECOND = moves(lambda z, y, x, c: ((z - 1 + 2 * c) % Z, y, x, c))
X_FIRST = moves(lambda z, y, x, c: (z, y, (x + 1 - 2 * c) % X, c))
X_SECOND = moves(lambda z, y, x, c: (z, y, (x - 1 + 2 * c) % X, c))
OTHER_CORE = moves(lambda z, y, x, c: (z, y, x, 1 - c))
KV_MOVE = [
    moves(lambda z, y, x, c, r=r: (z, 2 * c + (r ^ (y >> 1)), x, y & 1)) for r in range(2)
]
Q_MOVE = [
    moves(
        lambda z, y, x, c, r=r: (z, 2 * c + r, x, y)
        if y < 2
        else (Z - 1 - z, 2 * c + 1 - r, x, 3 - y)
    )
    for r in range(2)
]
Q_BACK = [[(d, s) for s, d in m] for m in Q_MOVE]


def send(a, move):
    return lax.ppermute(a, AXES, move)


def in_vmem():
    return pl.BlockSpec(memory_space=pltpu.VMEM)


def in_smem():
    return pl.BlockSpec(memory_space=pltpu.SMEM)


def piece_origins(x, c):
    origins = []
    for core in (c, 1 - c):
        way = 1 - 2 * core
        origins += [((x - way * far + 2 * X) % X) * C + core for far in (0, 1, -1, 2)]
    return origins


def project_body(pos, bias, *refs):
    tok, (wq, wk, wv) = refs[:8], refs[8:11]
    (q0, q1, kv0, kv1), (rows, q_t, kv) = refs[11:15], refs[15:]
    x, c, high = pos[1] // C, pos[1] % C, (pos[0] % Y) // 2
    for n, origin in enumerate(piece_origins(x, c)):
        rows[pl.ds(pl.multiple_of(origin * ROWS, ROWS), ROWS)] = tok[n][...]
    full = rows[...]
    one, bf = jnp.float32, jnp.bfloat16

    def product(w):
        return jnp.dot(full, w[...], preferred_element_type=one).astype(bf)

    key, value, query = product(wk), product(wv), product(wq)
    q_t[...] = (query * bf(HEAD**-0.5)).T
    value_t = value.T
    place = lax.broadcasted_iota(jnp.int32, (CHUNK, CHUNK), 0)
    origin = lax.broadcasted_iota(jnp.int32, (CHUNK, CHUNK), 1)
    order = jnp.where((place % 8) * RUN + place // 8 == origin, 1.0, 0.0).astype(bf)
    order_t = jnp.where((origin % 8) * RUN + origin // 8 == place, 1.0, 0.0).astype(bf)
    keys = []
    for n in range(TOK // CHUNK):
        s = slice(n * CHUNK, (n + 1) * CHUNK)
        keys.append(jnp.dot(order, key[s], preferred_element_type=one).astype(bf))
        v_t = jnp.dot(value_t[:, s], order_t, preferred_element_type=one).astype(bf)
        for k in range(2):
            kv[k, 256 + n * HEAD : 256 + (n + 1) * HEAD] = v_t[k * HEAD : (k + 1) * HEAD]
    for n in range(2):
        s = slice(n * CHUNK, (n + 1) * CHUNK)
        for k in range(2):
            cols = slice(k * HEAD, (k + 1) * HEAD)
            kv[k, s] = jnp.concatenate([keys[n][:, cols], keys[n + 2][:, cols]], axis=1)
    row = lax.broadcasted_iota(jnp.int32, (16, TOK), 0)
    for r, (q_out, kv_out) in enumerate(((q0, kv0), (q1, kv1))):
        k = high if r == 0 else 1 - high
        kv_out[...] = kv[k]
        q_out[:HEAD] = q_t[pl.ds(pl.multiple_of(k * HEAD, HEAD), HEAD)]
        b = jnp.full((16, TOK), bias[k], one)
        b_hi = b.astype(bf).astype(one)
        b_mid = (b - b_hi).astype(bf).astype(one)
        b_lo = b - b_hi - b_mid
        parts = jnp.where(row == 0, b_hi, jnp.where(row == 1, b_mid, jnp.where(row == 2, b_lo, 0.0)))
        q_out[HEAD:] = parts.astype(bf)


def project(pos, bias, pieces, weights):
    bf = jnp.bfloat16
    return pl.pallas_call(
        project_body,
        out_shape=(jax.ShapeDtypeStruct((QROWS, TOK), bf),) * 2
        + (jax.ShapeDtypeStruct((TOK, LANES), bf),) * 2,
        in_specs=[in_smem(), in_smem()] + [in_vmem()] * 11,
        out_specs=(in_vmem(),) * 4,
        scratch_shapes=[
            pltpu.VMEM((TOK, 2048), bf),
            pltpu.VMEM((2 * HEAD, TOK), bf),
            pltpu.VMEM((2, TOK, LANES), bf),
        ],
        cost_estimate=pl.CostEstimate(flops=1 << 26, bytes_accessed=4 << 20, transcendentals=0),
        name="project",
    )(pos, bias, *pieces, *weights)


def chunk_weights(scores, ahead, carry, masked):
    sub = lax.broadcasted_iota(jnp.int32, (8, LANES), 0)
    if masked:
        gap = lax.broadcasted_iota(jnp.int32, (8, LANES), 1) + ahead - sub * RUN
    kept, out = None, [None] * RUN
    for v in range(RUN - 1, -1, -1):
        e = jnp.exp(jnp.minimum(scores[v * 8 : (v + 1) * 8], 87.0))
        keep = 1.0 / (1.0 + e)
        take = e * keep
        if masked:
            live = gap > v
            keep = jnp.where(live, keep, 1.0)
            take = jnp.where(live, take, 0.0)
        out[v] = take if kept is None else take * kept
        kept = keep if kept is None else kept * keep
    later = jnp.where(sub < 7, pltpu.roll(kept, 7, 0), 1.0)
    later = later * jnp.where(sub < 7, pltpu.roll(later, 7, 0), 1.0)
    later = later * jnp.where(sub < 6, pltpu.roll(later, 6, 0), 1.0)
    later = later * jnp.where(sub < 4, pltpu.roll(later, 4, 0), 1.0)
    total = jnp.broadcast_to((later * kept)[0:1], (8, LANES))
    scale = later * carry
    return jnp.concatenate([w * scale for w in out]).astype(jnp.bfloat16), carry * total


def segment(m_ref, q_ref, w_ref, acc_ref, kept_ref, place, g, b, masked):
    carries = [jnp.ones((8, LANES), jnp.float32)] * (TOK // LANES)
    lane = lax.broadcasted_iota(jnp.int32, (1, LANES), 1)
    ones = jnp.broadcast_to(jnp.where(lane < 3, 1.0, 0.0), (256, LANES)).astype(jnp.bfloat16)
    keys = jnp.concatenate([m_ref[place, :256], ones], axis=1)
    out = None
    for half in (1, 0):
        scores = jnp.dot(keys, q_ref[b, half], preferred_element_type=jnp.float32)
        for s in (CHUNK, 0):
            for n in range(TOK // LANES):
                t = slice(n * LANES, (n + 1) * LANES)
                w_ref[s : s + CHUNK, t], carries[n] = chunk_weights(
                    scores[s : s + CHUNK, t], n * LANES - s - 256 * half, carries[n], masked
                )
        first = 256 + 2 * HEAD * half
        values = jnp.concatenate(
            [m_ref[place, first : first + HEAD], m_ref[place, first + HEAD : first + 2 * HEAD]], axis=1
        )
        part = jnp.dot(values, w_ref[...], preferred_element_type=jnp.float32)
        out = part if out is None else out + part
    kept = kept_ref[g, b]
    acc_ref[g, b] = acc_ref[g, b] + kept[0:1] * out
    kept_ref[g, b] = kept * jnp.concatenate(carries, axis=1)


def group_of(z, c, far):
    return (z + (1 - 2 * c) * far + Z) % Z


def attend_body(fars, pos, q0, q1, *refs):
    count = len(fars)
    kvs, (acc_ref, kept_ref, m_ref, q_ref, w_ref) = refs[: 2 * count], refs[2 * count :]
    z, y, c = pos[0] // Y, pos[0] % Y, pos[1] % C
    acc_ref[...] = jnp.zeros_like(acc_ref)
    kept_ref[...] = jnp.ones_like(kept_ref)
    for g in range(count):
        for n in range(4):
            half = y % 2 if n % 2 == 0 else 1 - y % 2
            slot = 2 * half + (c if n < 2 else 1 - c)
            m_ref[ZSEGS * g + slot] = kvs[2 * g + n // 2][n % 2]
    q_ref[...] = jnp.zeros_like(q_ref)
    for b, q in enumerate((q0, q1)):
        for half in range(2):
            q_ref[b, half, HEAD * half : HEAD * (half + 1)] = q[:HEAD]
            q_ref[b, half, LANES : LANES + 16] = q[HEAD:]

    def step(n, _):
        g, b, j = n // (2 * ZSEGS), n // ZSEGS % 2, ZSEGS - 1 - n % ZSEGS
        far = jnp.where(g == 0, fars[0], fars[-1])
        block = jnp.where(b == y % 2, 4 * z + c, 31 - 4 * z - c)
        ahead = block - (group_of(z, c, far) * ZSEGS + j)
        args = (m_ref, q_ref, w_ref, acc_ref, kept_ref, ZSEGS * g + j, g, b)

        @pl.when(ahead > 0)
        def _():
            segment(*args, False)

        @pl.when(ahead == 0)
        def _():
            segment(*args, True)

        return 0

    lax.fori_loop(0, count * 2 * ZSEGS, step, 0)


def attend(fars, pos, q0, q1, kvs):
    bf = jnp.bfloat16
    count = len(fars)

    def body(*refs):
        attend_body(fars, *refs)

    return pl.pallas_call(
        body,
        out_shape=(
            jax.ShapeDtypeStruct((count, 2, HEAD, TOK), jnp.float32),
            jax.ShapeDtypeStruct((count, 2, 8, TOK), jnp.float32),
        ),
        in_specs=[in_smem()] + [in_vmem()] * (2 + 2 * count),
        out_specs=(in_vmem(), in_vmem()),
        scratch_shapes=[
            pltpu.VMEM((count * ZSEGS, TOK, LANES), bf),
            pltpu.VMEM((2, 2, 2 * LANES, TOK), bf),
            pltpu.VMEM((2 * CHUNK, TOK), bf),
        ],
        cost_estimate=pl.CostEstimate(flops=count << 31, bytes_accessed=1 << 20, transcendentals=1 << 22),
        name=f"attend{fars[-1]}",
    )(pos, q0, q1, *kvs)


def merge_body(fars, pos, *refs):
    n = len(fars)
    accs, kepts, outs = refs[:n], refs[n : 2 * n], refs[2 * n :]
    z, c = pos[0] // Y, pos[1] % C
    places = [(i, g, group_of(z, c, far)) for i in range(n) for g, far in enumerate(fars[i])]
    for b in range(2):
        total = None
        for i, g, group in places:
            factor = jnp.ones((8, TOK), jnp.float32)
            for k, h, other in places:
                if (k, h) != (i, g):
                    factor = factor * jnp.where(other > group, kepts[k][h, b], 1.0)
            part = factor[0:1] * accs[i][g, b]
            total = part if total is None else total + part
        outs[b][...] = total.astype(jnp.bfloat16)


def merge(fars, pos, parts):
    def body(*refs):
        merge_body(fars, *refs)

    return pl.pallas_call(
        body,
        out_shape=(jax.ShapeDtypeStruct((HEAD, TOK), jnp.bfloat16),) * 2,
        in_specs=[in_smem()] + [in_vmem()] * (2 * len(fars)),
        out_specs=(in_vmem(),) * 2,
        name="merge",
    )(pos, *[a for a, _ in parts], *[k for _, k in parts])


def output_body(pos, att, *refs):
    ws, out = refs[:8], refs[8]
    total = None
    for n, origin in enumerate(piece_origins(pos[1] // C, pos[1] % C)):
        part = jnp.dot(att[origin], ws[n][...], preferred_element_type=jnp.float32)
        total = part if total is None else total + part
    out[...] = total.astype(jnp.bfloat16)


def output(pos, att, pieces):
    return pl.pallas_call(
        output_body,
        out_shape=jax.ShapeDtypeStruct((ROWS, 2048), jnp.bfloat16),
        in_specs=[in_smem()] + [in_vmem()] * 9,
        out_specs=in_vmem(),
        name="output",
    )(pos, att, *pieces)


def after(a, *others):
    return lax.optimization_barrier((a, *others))[0]


def across_x(a):
    first, second = send(a, X_FIRST), send(a, X_SECOND)
    return [a, first, second, send(first, X_FIRST)]


def from_all_tp(mine):
    return mine + [send(p, OTHER_CORE) for p in mine]


def shards(tokens, w_query, w_key, w_value, head_bias, w_out):
    sp, tp = lax.axis_index("sp"), lax.axis_index("tp")
    pos = jnp.stack([sp, tp]).astype(jnp.int32)
    y = sp % Y
    mine = across_x(tokens)
    pieces = from_all_tp(mine)
    q0, q1, kv0, kv1 = project(pos, head_bias, pieces, (w_query, w_key, w_value))
    q0, q1 = send(q0, Q_MOVE[0]), send(q1, Q_MOVE[1])
    own = jnp.stack([send(kv0, KV_MOVE[0]), send(kv1, KV_MOVE[1])])
    fars = [(0,), (-1, 1), (-2, 2), (-3, 3), (4,)]
    steps = [(own,), (send(own, Z_FIRST), send(own, Z_SECOND))]
    theirs = [(send(own, OTHER_CORE),)]
    parts = []
    w_mine = across_x(after(w_out, own))
    w_pieces = []
    for n in range(len(fars)):
        if n + 1 < len(fars):
            ahead = after(steps[n + 1], *parts)
            theirs.append(tuple(send(a, OTHER_CORE) for a in reversed(ahead)))
            q0, q1, *_ = lax.optimization_barrier((q0, q1, *ahead))
            if n + 2 < len(fars) - 1:
                steps.append((send(ahead[0], Z_FIRST), send(ahead[1], Z_SECOND)))
            elif n + 2 == len(fars) - 1:
                steps.append((send(ahead[0], Z_FIRST),))
        else:
            q0, q1, *w_pieces = lax.optimization_barrier((q0, q1, *w_pieces))
        kvs = [a for pair in zip(steps[n], theirs[n]) for a in pair]
        parts.append(attend(fars[n], pos, q0, q1, kvs))
        if n == 1:
            w_pieces = from_all_tp([after(w, parts[n]) for w in w_mine])
    att0, att1 = merge(fars, pos, parts)
    att0, att1 = send(att0, Q_BACK[0]), send(att1, Q_BACK[1])
    att = jnp.where(y < 2, jnp.concatenate([att0, att1]), jnp.concatenate([att1, att0])).T
    att = lax.all_to_all(att.reshape(X * C, ROWS, 2 * HEAD), "tp", 0, 0, tiled=True)
    return output(pos, att, w_pieces)


def solution(mesh):
    placed = (
        P(("sp", "tp"), None),
        P(None, "tp"),
        P(None, "tp"),
        P(None, "tp"),
        P("tp"),
        P("tp", None),
    )
    return jax.shard_map(
        shards, mesh=mesh, in_specs=placed, out_specs=P(("sp", "tp"), None), check_vma=False
    )
```

profile of v0, /device:TPU:56, one launch (start us, length us, event | category | flops | bytes accessed | tf_op | source)
XLA Modules:
  0.0 147.0 jit_solution(4846673044952323791)
XLA Ops:
  0.0 1.5 %collective-permute-start = (bf16[64,2048]{1,0:T(8,128)(2,1)}, bf16[64,2048]{1,0:T(8,128)(2,1)S(1)}, u32[]{:S(2)}, u32[]{:S(2)}) collective-permute-start(bf16[64,2048]{1,0:T(8,128)(2,1)} %refs_0_.1), channel_id=1, source_target_pairs={{0,2},{1,7},{2,4},{3,1},{4,6},{5,3},{6,0},{7,5},{8,10},{9,15},{10,... | collective-permute-start | bytes 786440 | tf_op jit(solution)/shard_map/ppermute | solution.py:54
  1.5 1.7 %collective-permute-start.1 = (bf16[64,2048]{1,0:T(8,128)(2,1)}, bf16[64,2048]{1,0:T(8,128)(2,1)S(1)}, u32[]{:S(2)}, u32[]{:S(2)}) collective-permute-start(bf16[64,2048]{1,0:T(8,128)(2,1)} %refs_0_.1), channel_id=1, source_target_pairs={{0,6},{1,3},{2,0},{3,5},{4,2},{5,7},{6,4},{7,1},{8,14},{9,11},{10,... | collective-permute-start | bytes 786440 | tf_op jit(solution)/shard_map/ppermute | solution.py:54
  3.2 6.0 %collective-permute-done.refs_1_ = bf16[64,2048]{1,0:T(8,128)(2,1)S(1)} collective-permute-done((bf16[64,2048]{1,0:T(8,128)(2,1)}, bf16[64,2048]{1,0:T(8,128)(2,1)S(1)}, u32[]{:S(2)}, u32[]{:S(2)}) %collective-permute-start) | collective-permute-done | bytes 262176 | tf_op jit(solution)/shard_map/ppermute | solution.py:54
  9.3 1.5 collective-permute-start.2
  10.7 0.5 collective-permute-start.4
  11.3 5.5 %collective-permute-done.2.refs_3_ = bf16[64,2048]{1,0:T(8,128)(2,1)S(1)} collective-permute-done((bf16[64,2048]{1,0:T(8,128)(2,1)S(1)}, bf16[64,2048]{1,0:T(8,128)(2,1)S(1)}, u32[]{:S(2)}, u32[]{:S(2)}) %collective-permute-start.2) | collective-permute-done | bytes 262176 | tf_op jit(solution)/shard_map/ppermute | solution.py:54
  16.8 0.7 pad_add_fusion.pos.refs_0_
  17.5 0.8 collective-permute-done.6.refs_7_
  18.4 0.7 copy-done.13
  19.1 4.9 %project.1 = (bf16[80,512]{1,0:T(8,128)(2,1)}, bf16[80,512]{1,0:T(8,128)(2,1)}, bf16[512,128]{1,0:T(8,128)(2,1)}, bf16[512,128]{1,0:T(8,128)(2,1)}) custom-call(s32[2]{0:T(128)} %pad_add_fusion.pos.refs_0_, f32[2]{0:T(128)} %bias.1, bf16[64,2048]{1,0:T(8,128)(2,1)} %refs_0_.1, bf16[64,2048]{1,0:T(8,128)(2,1)} %copy-done.7, bf16[64,2048]{1,0:T(8,128)(2,1)} %copy-done.8, ...), custom_call_target="tpu_custom_call" | custom-call | flops 67108864 | bytes 4194304 | tf_op jit(solution)/shard_map/project/pallas_call | solution.py:119
  24.0 3.3 %collective-permute-start.9 = (bf16[512,128]{1,0:T(8,128)(2,1)}, bf16[512,128]{1,0:T(8,128)(2,1)S(1)}, u32[]{:S(2)}, u32[]{:S(2)}) collective-permute-start(bf16[512,128]{1,0:T(8,128)(2,1)} %get-tuple-element.53), channel_id=1, source_target_pairs={{0,0},{1,16},{2,2},{3,18},{4,4},{5,20},{6,6},{7,22},{8,1},{9,17},{... | collective-permute-start | bytes 393224 | tf_op jit(solution)/shard_map/ppermute | solution.py:54
  27.4 1.9 %collective-permute-start.10 = (bf16[512,128]{1,0:T(8,128)(2,1)}, bf16[512,128]{1,0:T(8,128)(2,1)S(1)}, u32[]{:S(2)}, u32[]{:S(2)}) collective-permute-start(bf16[512,128]{1,0:T(8,128)(2,1)} %get-tuple-element.54), channel_id=1, source_target_pairs={{0,8},{1,24},{2,10},{3,26},{4,12},{5,28},{6,14},{7,30},{8,9},{9,25... | collective-permute-start | bytes 393224 | tf_op jit(solution)/shard_map/ppermute | solution.py:54
  29.3 2.6 %collective-permute-done.9 = bf16[512,128]{1,0:T(8,128)(2,1)S(1)} collective-permute-done((bf16[512,128]{1,0:T(8,128)(2,1)}, bf16[512,128]{1,0:T(8,128)(2,1)S(1)}, u32[]{:S(2)}, u32[]{:S(2)}) %collective-permute-start.9) | collective-permute-done | bytes 131104 | tf_op jit(solution)/shard_map/ppermute | solution.py:54
  31.9 1.9 %collective-permute-done.10 = bf16[512,128]{1,0:T(8,128)(2,1)S(1)} collective-permute-done((bf16[512,128]{1,0:T(8,128)(2,1)}, bf16[512,128]{1,0:T(8,128)(2,1)S(1)}, u32[]{:S(2)}, u32[]{:S(2)}) %collective-permute-start.10) | collective-permute-done | bytes 131104 | tf_op jit(solution)/shard_map/ppermute | solution.py:54
  33.8 0.3 collective-permute-start.25
  34.1 0.2 collective-permute-start.12
  34.3 1.8 %collective-permute-start.11 = (bf16[2,512,128]{2,1,0:T(8,128)(2,1)S(1)}, bf16[2,512,128]{2,1,0:T(8,128)(2,1)S(1)}, u32[]{:S(2)}, u32[]{:S(2)}) collective-permute-start(bf16[2,512,128]{2,1,0:T(8,128)(2,1)S(1)} %pad_maximum_fusion.refs_3_), channel_id=1, source_target_pairs={{0,32},{1,225},{2,34},{3,227},{4,36},{5,229},{6,38},{7,231},{8,40}... | collective-permute-start | bytes 786440 | tf_op jit(solution)/shard_map/ppermute | solution.py:54
  36.1 8.7 %collective-permute-start.7 = (bf16[80,512]{1,0:T(8,128)(2,1)}, bf16[80,512]{1,0:T(8,128)(2,1)S(1)}, u32[]{:S(2)}, u32[]{:S(2)}) collective-permute-start(bf16[80,512]{1,0:T(8,128)(2,1)} %get-tuple-element.51), channel_id=1, source_target_pairs={{0,0},{1,16},{2,2},{3,18},{4,4},{5,20},{6,6},{7,22},{8,1},{9,17},{... | collective-permute-start | bytes 245768 | tf_op jit(solution)/shard_map/ppermute | solution.py:54
  44.8 2.9 %collective-permute-start.8 = (bf16[80,512]{1,0:T(8,128)(2,1)}, bf16[80,512]{1,0:T(8,128)(2,1)S(1)}, u32[]{:S(2)}, u32[]{:S(2)}) collective-permute-start(bf16[80,512]{1,0:T(8,128)(2,1)} %get-tuple-element.52), channel_id=1, source_target_pairs={{0,8},{1,24},{2,10},{3,26},{4,12},{5,28},{6,14},{7,30},{8,9},{9,25... | collective-permute-start | bytes 245768 | tf_op jit(solution)/shard_map/ppermute | solution.py:54
  47.8 1.0 collective-permute-start.14
  48.8 1.8 %collective-permute-start.15 = (bf16[2,512,128]{2,1,0:T(8,128)(2,1)S(1)}, bf16[2,512,128]{2,1,0:T(8,128)(2,1)}, u32[]{:S(2)}, u32[]{:S(2)}) collective-permute-start(bf16[2,512,128]{2,1,0:T(8,128)(2,1)S(1)} %collective-permute-done.12.refs_5_), channel_id=1, source_target_pairs={{0,224},{1,33},{2,226},{3,35},{4,228},{5,37},{6,230},{7,39},{8,232... | collective-permute-start | bytes 786440 | tf_op jit(solution)/shard_map/ppermute | solution.py:54
  50.6 0.3 collective-permute-done.8.refs_2_
  50.9 0.5 collective-permute-start.16
  51.4 0.1 copy-done.24
  51.6 4.8 %collective-permute-start.26 = (bf16[128,2048]{1,0:T(8,128)(2,1)S(1)}, bf16[128,2048]{1,0:T(8,128)(2,1)S(1)}, u32[]{:S(2)}, u32[]{:S(2)}) collective-permute-start(bf16[128,2048]{1,0:T(8,128)(2,1)S(1)} %copy-done), channel_id=1, source_target_pairs={{0,6},{1,3},{2,0},{3,5},{4,2},{5,7},{6,4},{7,1},{8,14},{9,11},{10,... | collective-permute-start | bytes 1572872 | tf_op jit(solution)/shard_map/ppermute | solution.py:54
  56.4 6.3 %attend0.1 = (f32[1,2,64,512]{3,2,1,0:T(8,128)}, f32[1,2,8,512]{3,2,1,0:T(8,128)}) custom-call(s32[2]{0:T(128)} %pad_add_fusion.pos.refs_0_, bf16[80,512]{1,0:T(8,128)(2,1)} %copy-done.23, bf16[80,512]{1,0:T(8,128)(2,1)} %copy-done.24, bf16[2,512,128]{2,1,0:T(8,128)(2,1)} %copy-done.6, bf16[2,512,128]{2,1,0:T(8,128)(2,1)} %copy-done.19), custom_call_target="tpu_custom_call" | custom-call | flops 2147483648 | bytes 1048576 | tf_op jit(solution)/shard_map/attend0/pallas_call | solution.py:232
  62.8 1.1 collective-permute-start.21
  63.9 3.0 %collective-permute-start.19 = (bf16[2,512,128]{2,1,0:T(8,128)(2,1)}, bf16[2,512,128]{2,1,0:T(8,128)(2,1)}, u32[]{:S(2)}, u32[]{:S(2)}) collective-permute-start(bf16[2,512,128]{2,1,0:T(8,128)(2,1)} %collective-permute-done.15.refs_5_), channel_id=1, source_target_pairs={{0,224},{1,33},{2,226},{3,35},{4,228},{5,37},{6,230},{7,39},{8,232... | collective-permute-start | bytes 786440 | tf_op jit(solution)/shard_map/ppermute | solution.py:54
  66.9 12.4 %attend1.1 = (f32[2,2,64,512]{3,2,1,0:T(8,128)}, f32[2,2,8,512]{3,2,1,0:T(8,128)}) custom-call(s32[2]{0:T(128)} %pad_add_fusion.pos.refs_0_, bf16[80,512]{1,0:T(8,128)(2,1)} %copy-done.23, bf16[80,512]{1,0:T(8,128)(2,1)} %copy-done.24, bf16[2,512,128]{2,1,0:T(8,128)(2,1)} %copy-done.16, bf16[2,512,128]{2,1,0:T(8,128)(2,1)} %copy-done.21, ...), custom_call_target="tpu_custom_call" | custom-call | flops 4294967296 | bytes 1048576 | tf_op jit(solution)/shard_map/attend1/pallas_call | solution.py:232
  79.3 0.5 collective-permute-start.20
  80.0 0.5 collective-permute-start.28
  80.5 0.1 collective-permute-start.30
  80.6 0.6 collective-permute-done.20.refs_4_
  81.2 0.4 collective-permute-start.29
  81.6 0.4 collective-permute-start.24
  81.9 0.3 copy-done.17
  82.3 4.4 %collective-permute-done.22.refs_3_ = bf16[2,512,128]{2,1,0:T(8,128)(2,1)} collective-permute-done((bf16[2,512,128]{2,1,0:T(8,128)(2,1)}, bf16[2,512,128]{2,1,0:T(8,128)(2,1)}, u32[]{:S(2)}, u32[]{:S(2)}) %collective-permute-start.22) | collective-permute-done | bytes 262176 | tf_op jit(solution)/shard_map/ppermute | solution.py:54
  86.6 6.0 %attend2.1 = (f32[2,2,64,512]{3,2,1,0:T(8,128)}, f32[2,2,8,512]{3,2,1,0:T(8,128)}) custom-call(s32[2]{0:T(128)} %pad_add_fusion.pos.refs_0_, bf16[80,512]{1,0:T(8,128)(2,1)} %copy-done.23, bf16[80,512]{1,0:T(8,128)(2,1)} %copy-done.24, bf16[2,512,128]{2,1,0:T(8,128)(2,1)} %copy-done.14, bf16[2,512,128]{2,1,0:T(8,128)(2,1)} %copy-done.18, ...), custom_call_target="tpu_custom_call" | custom-call | flops 4294967296 | bytes 1048576 | tf_op jit(solution)/shard_map/attend2/pallas_call | solution.py:232
  92.7 0.6 collective-permute-start.32
  93.4 9.3 %attend3.1 = (f32[2,2,64,512]{3,2,1,0:T(8,128)}, f32[2,2,8,512]{3,2,1,0:T(8,128)}) custom-call(s32[2]{0:T(128)} %pad_add_fusion.pos.refs_0_, bf16[80,512]{1,0:T(8,128)(2,1)} %copy-done.23, bf16[80,512]{1,0:T(8,128)(2,1)} %copy-done.24, bf16[2,512,128]{2,1,0:T(8,128)(2,1)} %collective-permute-done.18.refs_3_, bf16[2,512,128]{2,1,0:T(8,128)(2,1)} %copy-done.17, ...), custom_call_target="tpu_custom_call" | custom-call | flops 4294967296 | bytes 1048576 | tf_op jit(solution)/shard_map/attend3/pallas_call | solution.py:232
  102.7 5.7 %attend4.1 = (f32[1,2,64,512]{3,2,1,0:T(8,128)}, f32[1,2,8,512]{3,2,1,0:T(8,128)}) custom-call(s32[2]{0:T(128)} %pad_add_fusion.pos.refs_0_, bf16[80,512]{1,0:T(8,128)(2,1)} %copy-done.23, bf16[80,512]{1,0:T(8,128)(2,1)} %copy-done.24, bf16[2,512,128]{2,1,0:T(8,128)(2,1)} %collective-permute-done.22.refs_3_, bf16[2,512,128]{2,1,0:T(8,128)(2,1)} %collective-permute-done.32.refs_4_), custom_call_target="tpu_custom_call" | custom-call | flops 2147483648 | bytes 1048576 | tf_op jit(solution)/shard_map/attend4/pallas_call | solution.py:232
  108.5 2.5 %merge.1 = (bf16[64,512]{1,0:T(8,128)(2,1)}, bf16[64,512]{1,0:T(8,128)(2,1)}) custom-call(s32[2]{0:T(128)} %pad_add_fusion.pos.refs_0_, f32[1,2,64,512]{3,2,1,0:T(8,128)} %get-tuple-element.59.refs_1_, f32[2,2,64,512]{3,2,1,0:T(8,128)} %get-tuple-element.65.refs_2_, f32[2,2,64,512]{3,2,1,0:T(8,128)} %get-tuple-element.71.refs_3_, ...), custom_call_target="tpu_custom_call" | custom-call | tf_op jit(solution)/shard_map/merge/pallas_call | solution.py:271
  111.0 13.1 %collective-permute-start.33 = (bf16[64,512]{1,0:T(8,128)(2,1)}, bf16[64,512]{1,0:T(8,128)(2,1)S(1)}, u32[]{:S(2)}, u32[]{:S(2)}) collective-permute-start(bf16[64,512]{1,0:T(8,128)(2,1)} %get-tuple-element.87), channel_id=1, source_target_pairs={{0,0},{16,1},{2,2},{18,3},{4,4},{20,5},{6,6},{22,7},{1,8},{17,9},{... | collective-permute-start | bytes 196616 | tf_op jit(solution)/shard_map/ppermute | solution.py:54
  124.2 4.0 %collective-permute-done.33 = bf16[64,512]{1,0:T(8,128)(2,1)S(1)} collective-permute-done((bf16[64,512]{1,0:T(8,128)(2,1)}, bf16[64,512]{1,0:T(8,128)(2,1)S(1)}, u32[]{:S(2)}, u32[]{:S(2)}) %collective-permute-start.33) | collective-permute-done | bytes 65568 | tf_op jit(solution)/shard_map/ppermute | solution.py:54
  128.1 5.6 %collective-permute-done.34 = bf16[64,512]{1,0:T(8,128)(2,1)S(1)} collective-permute-done((bf16[64,512]{1,0:T(8,128)(2,1)}, bf16[64,512]{1,0:T(8,128)(2,1)S(1)}, u32[]{:S(2)}, u32[]{:S(2)}) %collective-permute-start.34) | collective-permute-done | bytes 65568 | tf_op jit(solution)/shard_map/ppermute | solution.py:54
  133.8 0.1 copy.7
  133.9 9.5 %all_to_all.5.att = bf16[8,64,128]{2,1,0:T(8,128)(2,1)} all-to-all(bf16[8,64,128]{2,1,0:T(8,128)(2,1)S(1)} %bitcast.7), channel_id=1, replica_groups=mesh['sp'=32,'tp'=8] {'tp'}, dimensions={0} | all-to-all | bytes 262144 | tf_op jit(solution)/shard_map/all_to_all | solution.py:345
  143.4 3.6 %output.1 = bf16[64,2048]{1,0:T(8,128)(2,1)} custom-call(s32[2]{0:T(128)} %pad_add_fusion.pos.refs_0_, bf16[8,64,128]{2,1,0:T(8,128)(2,1)} %all_to_all.5.att, bf16[128,2048]{1,0:T(8,128)(2,1)} %refs_0_.2, bf16[128,2048]{1,0:T(8,128)(2,1)} %copy-done.1, bf16[128,2048]{1,0:T(8,128)(2,1)} %copy-done.2, bf16[128,2048]{1,0:T(8,128)(2,1)} %copy-done.3, ...), custom_call_target="tpu_custom_call" | custom-call | tf_op jit(solution)/shard_map/output/pallas_call | solution.py:290
  (85 shorter events, 0.7 us)
Async XLA Ops:
  0.0 9.3 %collective-permute-start = (bf16[64,2048]{1,0:T(8,128)(2,1)}, bf16[64,2048]{1,0:T(8,128)(2,1)S(1)}, u32[]{:S(2)}, u32[]{:S(2)}) collective-permute-start(bf16[64,2048]{1,0:T(8,128)(2,1)} %refs_0_.1), channel_id=1, source_target_pairs={{0,2},{1,7},{2,4},{3,1},{4,6},{5,3},{6,0},{7,5},{8,10},{9,15},{10,... | collective-permute-start | bytes 786440 | tf_op jit(solution)/shard_map/ppermute | solution.py:54
  1.5 9.7 %collective-permute-start.1 = (bf16[64,2048]{1,0:T(8,128)(2,1)}, bf16[64,2048]{1,0:T(8,128)(2,1)S(1)}, u32[]{:S(2)}, u32[]{:S(2)}) collective-permute-start(bf16[64,2048]{1,0:T(8,128)(2,1)} %refs_0_.1), channel_id=1, source_target_pairs={{0,6},{1,3},{2,0},{3,5},{4,2},{5,7},{6,4},{7,1},{8,14},{9,11},{10,... | collective-permute-start | bytes 786440 | tf_op jit(solution)/shard_map/ppermute | solution.py:54
  9.3 9.1 %copy-start.7 = (bf16[64,2048]{1,0:T(8,128)(2,1)}, bf16[64,2048]{1,0:T(8,128)(2,1)S(1)}, u32[]{:S(2)}) copy-start(bf16[64,2048]{1,0:T(8,128)(2,1)S(1)} %collective-permute-done.refs_1_) | copy-start | bytes 786436
  9.3 7.6 %collective-permute-start.2 = (bf16[64,2048]{1,0:T(8,128)(2,1)S(1)}, bf16[64,2048]{1,0:T(8,128)(2,1)S(1)}, u32[]{:S(2)}, u32[]{:S(2)}) collective-permute-start(bf16[64,2048]{1,0:T(8,128)(2,1)S(1)} %collective-permute-done.refs_1_), channel_id=1, source_target_pairs={{0,2},{1,7},{2,4},{3,1},{4,6},{5,3},{6,0},{7,5},{8,10},{9,15},{10,... | collective-permute-start | bytes 786440 | tf_op jit(solution)/shard_map/ppermute | solution.py:54
  10.7 6.8 %collective-permute-start.3 = (bf16[64,2048]{1,0:T(8,128)(2,1)}, bf16[64,2048]{1,0:T(8,128)(2,1)S(1)}, u32[]{:S(2)}, u32[]{:S(2)}) collective-permute-start(bf16[64,2048]{1,0:T(8,128)(2,1)} %refs_0_.1), channel_id=1, source_target_pairs={{0,1},{1,0},{2,3},{3,2},{4,5},{5,4},{6,7},{7,6},{8,9},{9,8},{10,11... | collective-permute-start | bytes 786440 | tf_op jit(solution)/shard_map/ppermute | solution.py:54
  10.7 6.8 %collective-permute-start.4 = (bf16[64,2048]{1,0:T(8,128)(2,1)S(1)}, bf16[64,2048]{1,0:T(8,128)(2,1)S(1)}, u32[]{:S(2)}, u32[]{:S(2)}) collective-permute-start(bf16[64,2048]{1,0:T(8,128)(2,1)S(1)} %collective-permute-done.refs_1_), channel_id=1, source_target_pairs={{0,1},{1,0},{2,3},{3,2},{4,5},{5,4},{6,7},{7,6},{8,9},{9,8},{10,11... | collective-permute-start | bytes 786440 | tf_op jit(solution)/shard_map/ppermute | solution.py:54
  11.2 7.2 %copy-start.8 = (bf16[64,2048]{1,0:T(8,128)(2,1)}, bf16[64,2048]{1,0:T(8,128)(2,1)S(1)}, u32[]{:S(2)}) copy-start(bf16[64,2048]{1,0:T(8,128)(2,1)S(1)} %collective-permute-done.1.refs_2_) | copy-start | bytes 786436
  11.2 6.3 %collective-permute-start.5 = (bf16[64,2048]{1,0:T(8,128)(2,1)S(1)}, bf16[64,2048]{1,0:T(8,128)(2,1)S(1)}, u32[]{:S(2)}, u32[]{:S(2)}) collective-permute-start(bf16[64,2048]{1,0:T(8,128)(2,1)S(1)} %collective-permute-done.1.refs_2_), channel_id=1, source_target_pairs={{0,1},{1,0},{2,3},{3,2},{4,5},{5,4},{6,7},{7,6},{8,9},{9,8},{10,11... | collective-permute-start | bytes 786440 | tf_op jit(solution)/shard_map/ppermute | solution.py:54
  16.8 1.5 %collective-permute-start.6 = (bf16[64,2048]{1,0:T(8,128)(2,1)S(1)}, bf16[64,2048]{1,0:T(8,128)(2,1)S(1)}, u32[]{:S(2)}, u32[]{:S(2)}) collective-permute-start(bf16[64,2048]{1,0:T(8,128)(2,1)S(1)} %collective-permute-done.2.refs_3_), channel_id=1, source_target_pairs={{0,1},{1,0},{2,3},{3,2},{4,5},{5,4},{6,7},{7,6},{8,9},{9,8},{10,11... | collective-permute-start | bytes 786440 | tf_op jit(solution)/shard_map/ppermute | solution.py:54
  24.0 9.8 %copy-start = (bf16[128,2048]{1,0:T(8,128)(2,1)S(1)}, bf16[128,2048]{1,0:T(8,128)(2,1)}, u32[]{:S(2)}) copy-start(bf16[128,2048]{1,0:T(8,128)(2,1)} %refs_0_.2) | copy-start | bytes 1572868
  24.0 7.9 %collective-permute-start.9 = (bf16[512,128]{1,0:T(8,128)(2,1)}, bf16[512,128]{1,0:T(8,128)(2,1)S(1)}, u32[]{:S(2)}, u32[]{:S(2)}) collective-permute-start(bf16[512,128]{1,0:T(8,128)(2,1)} %get-tuple-element.53), channel_id=1, source_target_pairs={{0,0},{1,16},{2,2},{3,18},{4,4},{5,20},{6,6},{7,22},{8,1},{9,17},{... | collective-permute-start | bytes 393224 | tf_op jit(solution)/shard_map/ppermute | solution.py:54
  27.4 6.4 %collective-permute-start.10 = (bf16[512,128]{1,0:T(8,128)(2,1)}, bf16[512,128]{1,0:T(8,128)(2,1)S(1)}, u32[]{:S(2)}, u32[]{:S(2)}) collective-permute-start(bf16[512,128]{1,0:T(8,128)(2,1)} %get-tuple-element.54), channel_id=1, source_target_pairs={{0,8},{1,24},{2,10},{3,26},{4,12},{5,28},{6,14},{7,30},{8,9},{9,25... | collective-permute-start | bytes 393224 | tf_op jit(solution)/shard_map/ppermute | solution.py:54
  33.8 22.6 %copy-start.6 = (bf16[2,512,128]{2,1,0:T(8,128)(2,1)}, bf16[2,512,128]{2,1,0:T(8,128)(2,1)S(1)}, u32[]{:S(2)}) copy-start(bf16[2,512,128]{2,1,0:T(8,128)(2,1)S(1)} %pad_maximum_fusion.refs_3_) | copy-start | bytes 786436
  33.8 17.8 %collective-permute-start.25 = (bf16[128,2048]{1,0:T(8,128)(2,1)S(1)}, bf16[128,2048]{1,0:T(8,128)(2,1)S(1)}, u32[]{:S(2)}, u32[]{:S(2)}) collective-permute-start(bf16[128,2048]{1,0:T(8,128)(2,1)S(1)} %copy-done), channel_id=1, source_target_pairs={{0,2},{1,7},{2,4},{3,1},{4,6},{5,3},{6,0},{7,5},{8,10},{9,15},{10,... | collective-permute-start | bytes 1572872 | tf_op jit(solution)/shard_map/ppermute | solution.py:54
  34.1 10.7 %collective-permute-start.12 = (bf16[2,512,128]{2,1,0:T(8,128)(2,1)S(1)}, bf16[2,512,128]{2,1,0:T(8,128)(2,1)S(1)}, u32[]{:S(2)}, u32[]{:S(2)}) collective-permute-start(bf16[2,512,128]{2,1,0:T(8,128)(2,1)S(1)} %pad_maximum_fusion.refs_3_), channel_id=1, source_target_pairs={{0,224},{1,33},{2,226},{3,35},{4,228},{5,37},{6,230},{7,39},{8,232... | collective-permute-start | bytes 786440 | tf_op jit(solution)/shard_map/ppermute | solution.py:54
  34.3 13.5 %collective-permute-start.11 = (bf16[2,512,128]{2,1,0:T(8,128)(2,1)S(1)}, bf16[2,512,128]{2,1,0:T(8,128)(2,1)S(1)}, u32[]{:S(2)}, u32[]{:S(2)}) collective-permute-start(bf16[2,512,128]{2,1,0:T(8,128)(2,1)S(1)} %pad_maximum_fusion.refs_3_), channel_id=1, source_target_pairs={{0,32},{1,225},{2,34},{3,227},{4,36},{5,229},{6,38},{7,231},{8,40}... | collective-permute-start | bytes 786440 | tf_op jit(solution)/shard_map/ppermute | solution.py:54
  36.1 14.8 %collective-permute-start.13 = (bf16[2,512,128]{2,1,0:T(8,128)(2,1)S(1)}, bf16[2,512,128]{2,1,0:T(8,128)(2,1)S(1)}, u32[]{:S(2)}, u32[]{:S(2)}) collective-permute-start(bf16[2,512,128]{2,1,0:T(8,128)(2,1)S(1)} %pad_maximum_fusion.refs_3_), channel_id=1, source_target_pairs={{0,1},{1,0},{2,3},{3,2},{4,5},{5,4},{6,7},{7,6},{8,9},{9,8},{10,11... | collective-permute-start | bytes 786440 | tf_op jit(solution)/shard_map/ppermute | solution.py:54
  36.1 12.6 %collective-permute-start.7 = (bf16[80,512]{1,0:T(8,128)(2,1)}, bf16[80,512]{1,0:T(8,128)(2,1)S(1)}, u32[]{:S(2)}, u32[]{:S(2)}) collective-permute-start(bf16[80,512]{1,0:T(8,128)(2,1)} %get-tuple-element.51), channel_id=1, source_target_pairs={{0,0},{1,16},{2,2},{3,18},{4,4},{5,20},{6,6},{7,22},{8,1},{9,17},{... | collective-permute-start | bytes 245768 | tf_op jit(solution)/shard_map/ppermute | solution.py:54
  44.8 17.8 %copy-start.15 = (bf16[2,512,128]{2,1,0:T(8,128)(2,1)}, bf16[2,512,128]{2,1,0:T(8,128)(2,1)S(1)}, u32[]{:S(2)}) copy-start(bf16[2,512,128]{2,1,0:T(8,128)(2,1)S(1)} %collective-permute-done.12.refs_5_) | copy-start | bytes 786436
  44.8 6.1 %collective-permute-start.8 = (bf16[80,512]{1,0:T(8,128)(2,1)}, bf16[80,512]{1,0:T(8,128)(2,1)S(1)}, u32[]{:S(2)}, u32[]{:S(2)}) collective-permute-start(bf16[80,512]{1,0:T(8,128)(2,1)} %get-tuple-element.52), channel_id=1, source_target_pairs={{0,8},{1,24},{2,10},{3,26},{4,12},{5,28},{6,14},{7,30},{8,9},{9,25... | collective-permute-start | bytes 245768 | tf_op jit(solution)/shard_map/ppermute | solution.py:54
  47.8 14.9 %copy-start.16 = (bf16[2,512,128]{2,1,0:T(8,128)(2,1)}, bf16[2,512,128]{2,1,0:T(8,128)(2,1)S(1)}, u32[]{:S(2)}) copy-start(bf16[2,512,128]{2,1,0:T(8,128)(2,1)S(1)} %collective-permute-done.11.refs_3_) | copy-start | bytes 786436
  47.8 14.9 %collective-permute-start.14 = (bf16[2,512,128]{2,1,0:T(8,128)(2,1)S(1)}, bf16[2,512,128]{2,1,0:T(8,128)(2,1)S(1)}, u32[]{:S(2)}, u32[]{:S(2)}) collective-permute-start(bf16[2,512,128]{2,1,0:T(8,128)(2,1)S(1)} %collective-permute-done.11.refs_3_), channel_id=1, source_target_pairs={{0,32},{1,225},{2,34},{3,227},{4,36},{5,229},{6,38},{7,231},{8,40}... | collective-permute-start | bytes 786440 | tf_op jit(solution)/shard_map/ppermute | solution.py:54
  48.8 7.6 %copy-start.23 = (bf16[80,512]{1,0:T(8,128)(2,1)}, bf16[80,512]{1,0:T(8,128)(2,1)S(1)}, u32[]{:S(2)}) copy-start(bf16[80,512]{1,0:T(8,128)(2,1)S(1)} %collective-permute-done.7.refs_1_) | copy-start | bytes 245764
  48.8 14.0 %collective-permute-start.15 = (bf16[2,512,128]{2,1,0:T(8,128)(2,1)S(1)}, bf16[2,512,128]{2,1,0:T(8,128)(2,1)}, u32[]{:S(2)}, u32[]{:S(2)}) collective-permute-start(bf16[2,512,128]{2,1,0:T(8,128)(2,1)S(1)} %collective-permute-done.12.refs_5_), channel_id=1, source_target_pairs={{0,224},{1,33},{2,226},{3,35},{4,228},{5,37},{6,230},{7,39},{8,232... | collective-permute-start | bytes 786440 | tf_op jit(solution)/shard_map/ppermute | solution.py:54
  50.9 12.9 %collective-permute-start.17 = (bf16[2,512,128]{2,1,0:T(8,128)(2,1)S(1)}, bf16[2,512,128]{2,1,0:T(8,128)(2,1)S(1)}, u32[]{:S(2)}, u32[]{:S(2)}) collective-permute-start(bf16[2,512,128]{2,1,0:T(8,128)(2,1)S(1)} %collective-permute-done.11.refs_3_), channel_id=1, source_target_pairs={{0,1},{1,0},{2,3},{3,2},{4,5},{5,4},{6,7},{7,6},{8,9},{9,8},{10,11... | collective-permute-start | bytes 786440 | tf_op jit(solution)/shard_map/ppermute | solution.py:54
  50.9 12.9 %collective-permute-start.16 = (bf16[2,512,128]{2,1,0:T(8,128)(2,1)S(1)}, bf16[2,512,128]{2,1,0:T(8,128)(2,1)S(1)}, u32[]{:S(2)}, u32[]{:S(2)}) collective-permute-start(bf16[2,512,128]{2,1,0:T(8,128)(2,1)S(1)} %collective-permute-done.12.refs_5_), channel_id=1, source_target_pairs={{0,1},{1,0},{2,3},{3,2},{4,5},{5,4},{6,7},{7,6},{8,9},{9,8},{10,11... | collective-permute-start | bytes 786440 | tf_op jit(solution)/shard_map/ppermute | solution.py:54
  51.6 29.6 %copy-start.1 = (bf16[128,2048]{1,0:T(8,128)(2,1)}, bf16[128,2048]{1,0:T(8,128)(2,1)S(1)}, u32[]{:S(2)}) copy-start(bf16[128,2048]{1,0:T(8,128)(2,1)S(1)} %collective-permute-done.25.refs_1_) | copy-start | bytes 1572868
  51.6 28.4 %collective-permute-start.26 = (bf16[128,2048]{1,0:T(8,128)(2,1)S(1)}, bf16[128,2048]{1,0:T(8,128)(2,1)S(1)}, u32[]{:S(2)}, u32[]{:S(2)}) collective-permute-start(bf16[128,2048]{1,0:T(8,128)(2,1)S(1)} %copy-done), channel_id=1, source_target_pairs={{0,6},{1,3},{2,0},{3,5},{4,2},{5,7},{6,4},{7,1},{8,14},{9,11},{10,... | collective-permute-start | bytes 1572872 | tf_op jit(solution)/shard_map/ppermute | solution.py:54
  62.7 16.6 %copy-start.14 = (bf16[2,512,128]{2,1,0:T(8,128)(2,1)}, bf16[2,512,128]{2,1,0:T(8,128)(2,1)S(1)}, u32[]{:S(2)}) copy-start(bf16[2,512,128]{2,1,0:T(8,128)(2,1)S(1)} %collective-permute-done.14.refs_3_) | copy-start | bytes 786436
  62.7 17.2 %collective-permute-start.27 = (bf16[128,2048]{1,0:T(8,128)(2,1)S(1)}, bf16[128,2048]{1,0:T(8,128)(2,1)S(1)}, u32[]{:S(2)}, u32[]{:S(2)}) collective-permute-start(bf16[128,2048]{1,0:T(8,128)(2,1)S(1)} %collective-permute-done.25.refs_1_), channel_id=1, source_target_pairs={{0,2},{1,7},{2,4},{3,1},{4,6},{5,3},{6,0},{7,5},{8,10},{9,15},{10,... | collective-permute-start | bytes 1572872 | tf_op jit(solution)/shard_map/ppermute | solution.py:54
  62.8 17.7 %collective-permute-start.21 = (bf16[2,512,128]{2,1,0:T(8,128)(2,1)S(1)}, bf16[2,512,128]{2,1,0:T(8,128)(2,1)}, u32[]{:S(2)}, u32[]{:S(2)}) collective-permute-start(bf16[2,512,128]{2,1,0:T(8,128)(2,1)S(1)} %collective-permute-done.14.refs_3_), channel_id=1, source_target_pairs={{0,1},{1,0},{2,3},{3,2},{4,5},{5,4},{6,7},{7,6},{8,9},{9,8},{10,11... | collective-permute-start | bytes 786440 | tf_op jit(solution)/shard_map/ppermute | solution.py:54
  63.9 15.5 %collective-permute-start.18 = (bf16[2,512,128]{2,1,0:T(8,128)(2,1)S(1)}, bf16[2,512,128]{2,1,0:T(8,128)(2,1)}, u32[]{:S(2)}, u32[]{:S(2)}) collective-permute-start(bf16[2,512,128]{2,1,0:T(8,128)(2,1)S(1)} %collective-permute-done.14.refs_3_), channel_id=1, source_target_pairs={{0,32},{1,225},{2,34},{3,227},{4,36},{5,229},{6,38},{7,231},{8,40}... | collective-permute-start | bytes 786440 | tf_op jit(solution)/shard_map/ppermute | solution.py:54
  63.9 15.9 %collective-permute-start.19 = (bf16[2,512,128]{2,1,0:T(8,128)(2,1)}, bf16[2,512,128]{2,1,0:T(8,128)(2,1)}, u32[]{:S(2)}, u32[]{:S(2)}) collective-permute-start(bf16[2,512,128]{2,1,0:T(8,128)(2,1)} %collective-permute-done.15.refs_5_), channel_id=1, source_target_pairs={{0,224},{1,33},{2,226},{3,35},{4,228},{5,37},{6,230},{7,39},{8,232... | collective-permute-start | bytes 786440 | tf_op jit(solution)/shard_map/ppermute | solution.py:54
  79.3 1.9 %collective-permute-start.20 = (bf16[2,512,128]{2,1,0:T(8,128)(2,1)}, bf16[2,512,128]{2,1,0:T(8,128)(2,1)S(1)}, u32[]{:S(2)}, u32[]{:S(2)}) collective-permute-start(bf16[2,512,128]{2,1,0:T(8,128)(2,1)} %collective-permute-done.15.refs_5_), channel_id=1, source_target_pairs={{0,1},{1,0},{2,3},{3,2},{4,5},{5,4},{6,7},{7,6},{8,9},{9,8},{10,11... | collective-permute-start | bytes 786440 | tf_op jit(solution)/shard_map/ppermute | solution.py:54
  79.8 1.8 %collective-permute-start.23 = (bf16[2,512,128]{2,1,0:T(8,128)(2,1)}, bf16[2,512,128]{2,1,0:T(8,128)(2,1)S(1)}, u32[]{:S(2)}, u32[]{:S(2)}) collective-permute-start(bf16[2,512,128]{2,1,0:T(8,128)(2,1)} %collective-permute-done.19.refs_5_), channel_id=1, source_target_pairs={{0,1},{1,0},{2,3},{3,2},{4,5},{5,4},{6,7},{7,6},{8,9},{9,8},{10,11... | collective-permute-start | bytes 786440 | tf_op jit(solution)/shard_map/ppermute | solution.py:54
  79.9 12.7 %copy-start.2 = (bf16[128,2048]{1,0:T(8,128)(2,1)}, bf16[128,2048]{1,0:T(8,128)(2,1)S(1)}, u32[]{:S(2)}) copy-start(bf16[128,2048]{1,0:T(8,128)(2,1)S(1)} %collective-permute-done.26.refs_2_) | copy-start | bytes 1572868
  79.9 6.7 %collective-permute-start.22 = (bf16[2,512,128]{2,1,0:T(8,128)(2,1)}, bf16[2,512,128]{2,1,0:T(8,128)(2,1)}, u32[]{:S(2)}, u32[]{:S(2)}) collective-permute-start(bf16[2,512,128]{2,1,0:T(8,128)(2,1)} %collective-permute-done.18.refs_3_), channel_id=1, source_target_pairs={{0,32},{1,225},{2,34},{3,227},{4,36},{5,229},{6,38},{7,231},{8,40}... | collective-permute-start | bytes 786440 | tf_op jit(solution)/shard_map/ppermute | solution.py:54
  79.9 12.7 %copy-start.3 = (bf16[128,2048]{1,0:T(8,128)(2,1)}, bf16[128,2048]{1,0:T(8,128)(2,1)S(1)}, u32[]{:S(2)}) copy-start(bf16[128,2048]{1,0:T(8,128)(2,1)S(1)} %collective-permute-done.27.refs_3_) | copy-start | bytes 1572868
  80.0 22.7 %collective-permute-start.28 = (bf16[128,2048]{1,0:T(8,128)(2,1)S(1)}, bf16[128,2048]{1,0:T(8,128)(2,1)S(1)}, u32[]{:S(2)}, u32[]{:S(2)}) collective-permute-start(bf16[128,2048]{1,0:T(8,128)(2,1)S(1)} %copy-done), channel_id=1, source_target_pairs={{0,1},{1,0},{2,3},{3,2},{4,5},{5,4},{6,7},{7,6},{8,9},{9,8},{10,11... | collective-permute-start | bytes 1572872 | tf_op jit(solution)/shard_map/ppermute | solution.py:54
  80.5 22.2 %collective-permute-start.30 = (bf16[128,2048]{1,0:T(8,128)(2,1)S(1)}, bf16[128,2048]{1,0:T(8,128)(2,1)S(1)}, u32[]{:S(2)}, u32[]{:S(2)}) collective-permute-start(bf16[128,2048]{1,0:T(8,128)(2,1)S(1)} %collective-permute-done.26.refs_2_), channel_id=1, source_target_pairs={{0,1},{1,0},{2,3},{3,2},{4,5},{5,4},{6,7},{7,6},{8,9},{9,8},{10,11... | collective-permute-start | bytes 1572872 | tf_op jit(solution)/shard_map/ppermute | solution.py:54
  81.2 21.5 %collective-permute-start.29 = (bf16[128,2048]{1,0:T(8,128)(2,1)S(1)}, bf16[128,2048]{1,0:T(8,128)(2,1)}, u32[]{:S(2)}, u32[]{:S(2)}) collective-permute-start(bf16[128,2048]{1,0:T(8,128)(2,1)S(1)} %collective-permute-done.25.refs_1_), channel_id=1, source_target_pairs={{0,1},{1,0},{2,3},{3,2},{4,5},{5,4},{6,7},{7,6},{8,9},{9,8},{10,11... | collective-permute-start | bytes 1572872 | tf_op jit(solution)/shard_map/ppermute | solution.py:54
  81.6 11.1 %collective-permute-start.24 = (bf16[2,512,128]{2,1,0:T(8,128)(2,1)}, bf16[2,512,128]{2,1,0:T(8,128)(2,1)S(1)}, u32[]{:S(2)}, u32[]{:S(2)}) collective-permute-start(bf16[2,512,128]{2,1,0:T(8,128)(2,1)} %collective-permute-done.18.refs_3_), channel_id=1, source_target_pairs={{0,1},{1,0},{2,3},{3,2},{4,5},{5,4},{6,7},{7,6},{8,9},{9,8},{10,11... | collective-permute-start | bytes 786440 | tf_op jit(solution)/shard_map/ppermute | solution.py:54
  86.6 16.1 %collective-permute-start.31 = (bf16[128,2048]{1,0:T(8,128)(2,1)S(1)}, bf16[128,2048]{1,0:T(8,128)(2,1)}, u32[]{:S(2)}, u32[]{:S(2)}) collective-permute-start(bf16[128,2048]{1,0:T(8,128)(2,1)S(1)} %collective-permute-done.27.refs_3_), channel_id=1, source_target_pairs={{0,1},{1,0},{2,3},{3,2},{4,5},{5,4},{6,7},{7,6},{8,9},{9,8},{10,11... | collective-permute-start | bytes 1572872 | tf_op jit(solution)/shard_map/ppermute | solution.py:54
  92.7 10.0 %collective-permute-start.32 = (bf16[2,512,128]{2,1,0:T(8,128)(2,1)}, bf16[2,512,128]{2,1,0:T(8,128)(2,1)}, u32[]{:S(2)}, u32[]{:S(2)}) collective-permute-start(bf16[2,512,128]{2,1,0:T(8,128)(2,1)} %collective-permute-done.22.refs_3_), channel_id=1, source_target_pairs={{0,1},{1,0},{2,3},{3,2},{4,5},{5,4},{6,7},{7,6},{8,9},{9,8},{10,11... | collective-permute-start | bytes 786440 | tf_op jit(solution)/shard_map/ppermute | solution.py:54
  102.7 5.8 %copy-start.4 = (bf16[128,2048]{1,0:T(8,128)(2,1)}, bf16[128,2048]{1,0:T(8,128)(2,1)S(1)}, u32[]{:S(2)}) copy-start(bf16[128,2048]{1,0:T(8,128)(2,1)S(1)} %collective-permute-done.28.refs_4_) | copy-start | bytes 1572868
  102.7 5.8 %copy-start.5 = (bf16[128,2048]{1,0:T(8,128)(2,1)}, bf16[128,2048]{1,0:T(8,128)(2,1)S(1)}, u32[]{:S(2)}) copy-start(bf16[128,2048]{1,0:T(8,128)(2,1)S(1)} %collective-permute-done.30.refs_6_) | copy-start | bytes 1572868
  111.0 17.2 %collective-permute-start.33 = (bf16[64,512]{1,0:T(8,128)(2,1)}, bf16[64,512]{1,0:T(8,128)(2,1)S(1)}, u32[]{:S(2)}, u32[]{:S(2)}) collective-permute-start(bf16[64,512]{1,0:T(8,128)(2,1)} %get-tuple-element.87), channel_id=1, source_target_pairs={{0,0},{16,1},{2,2},{18,3},{4,4},{20,5},{6,6},{22,7},{1,8},{17,9},{... | collective-permute-start | bytes 196616 | tf_op jit(solution)/shard_map/ppermute | solution.py:54
  124.1 9.7 %collective-permute-start.34 = (bf16[64,512]{1,0:T(8,128)(2,1)}, bf16[64,512]{1,0:T(8,128)(2,1)S(1)}, u32[]{:S(2)}, u32[]{:S(2)}) collective-permute-start(bf16[64,512]{1,0:T(8,128)(2,1)} %get-tuple-element.88), channel_id=1, source_target_pairs={{8,0},{24,1},{10,2},{26,3},{12,4},{28,5},{14,6},{30,7},{9,8},{25,9... | collective-permute-start | bytes 196616 | tf_op jit(solution)/shard_map/ppermute | solution.py:54
  (12 other events, 24.0 us)
where the time goes:
time: 147 us
  starting transfers between devices  52.5 us (36%)
  Pallas kernels  50.7 us (34%)
  waiting for transfers between devices  31.8 us (22%)
  blocking collectives  9.53 us (6%)
    ppermute x35, starting transfers between devices, send(): return lax.ppermute(a, AXES, move)  52.5 us
    pallas_call x5, Pallas kernels, attend(): pl.pallas_call(body, out_shape=(jax.ShapeDtypeStruct((count, 2, HEAD, TOK...  39.7 us
    ppermute x35, waiting for transfers between devices, send(): return lax.ppermute(a, AXES, move)  31.8 us
    all_to_all x1, blocking collectives, shards(): lax.all_to_all(att.reshape(X * C, ROWS, 2 * HEAD), 'tp', 0, 0, tiled=True)  9.53 us
    pallas_call x1, Pallas kernels, project(): pl.pallas_call(project_body, out_shape=(jax.ShapeDtypeStruct((QROWS, TOK)...  4.88 us
    pallas_call x1, Pallas kernels, output(): pl.pallas_call(output_body, out_shape=jax.ShapeDtypeStruct((ROWS, 2048),...  3.6 us
  transfers between devices with their start and end apart: 35, of which 10 were waited for; matrix products, arithmetic and copies ran while one was open for 0% of the time, Pallas kernels for 23%

commit v1 on v0

--- a/solution.py
+++ b/solution.py
@@ -4,6 +4,7 @@
 from jax.experimental import pallas as pl
 from jax.experimental.pallas import tpu as pltpu
 from jax.sharding import PartitionSpec as P
+
 
 Z, Y, X, C = 8, 4, 4, 2
 AXES = ("sp", "tp")
@@ -14,7 +15,6 @@
 QROWS = 80
 RUN = 16
 CHUNK = 8 * RUN
-DEPTH = 256
 ZSEGS = 4
 
 
@@ -132,7 +132,8 @@
     )(pos, bias, *pieces, *weights)
 
 
-def chunk_weights(scores, ahead, carry, masked):
+def chunk_weights(scores, ahead, carry):
+    masked = ahead is not None
     sub = lax.broadcasted_iota(jnp.int32, (8, LANES), 0)
     if masked:
         gap = lax.broadcasted_iota(jnp.int32, (8, LANES), 1) + ahead - sub * RUN
@@ -156,26 +157,32 @@
     return jnp.concatenate([w * scale for w in out]).astype(jnp.bfloat16), carry * total
 
 
-def segment(m_ref, q_ref, w_ref, acc_ref, kept_ref, place, g, b, masked):
+def segments(m_ref, q_ref, w_ref, acc_ref, kept_ref, places, g, b, ahead):
     carries = [jnp.ones((8, LANES), jnp.float32)] * (TOK // LANES)
     lane = lax.broadcasted_iota(jnp.int32, (1, LANES), 1)
     ones = jnp.broadcast_to(jnp.where(lane < 3, 1.0, 0.0), (256, LANES)).astype(jnp.bfloat16)
-    keys = jnp.concatenate([m_ref[place, :256], ones], axis=1)
     out = None
-    for half in (1, 0):
-        scores = jnp.dot(keys, q_ref[b, half], preferred_element_type=jnp.float32)
-        for s in (CHUNK, 0):
-            for n in range(TOK // LANES):
-                t = slice(n * LANES, (n + 1) * LANES)
-                w_ref[s : s + CHUNK, t], carries[n] = chunk_weights(
-                    scores[s : s + CHUNK, t], n * LANES - s - 256 * half, carries[n], masked
-                )
-        first = 256 + 2 * HEAD * half
-        values = jnp.concatenate(
-            [m_ref[place, first : first + HEAD], m_ref[place, first + HEAD : first + 2 * HEAD]], axis=1
-        )
-        part = jnp.dot(values, w_ref[...], preferred_element_type=jnp.float32)
-        out = part if out is None else out + part
+    for i, place in enumerate(places):
+        keys = jnp.concatenate([m_ref[place, :256], ones], axis=1)
+        for half in (1, 0):
+            scores = jnp.dot(keys, q_ref[b, half], preferred_element_type=jnp.float32)
+            w = w_ref.at[2 * i + half]
+            for s in (CHUNK, 0):
+                for n in range(TOK // LANES):
+                    t = slice(n * LANES, (n + 1) * LANES)
+                    start = n * LANES - s - 256 * half
+                    w[s : s + CHUNK, t], carries[n] = chunk_weights(
+                        scores[s : s + CHUNK, t],
+                        None if ahead is None else start + TOK * ahead,
+                        carries[n],
+                    )
+            first = 256 + 2 * HEAD * half
+            values = jnp.concatenate(
+                [m_ref[place, first : first + HEAD], m_ref[place, first + HEAD : first + 2 * HEAD]],
+                axis=1,
+            )
+            part = jnp.dot(values, w[...], preferred_element_type=jnp.float32)
+            out = part if out is None else out + part
     kept = kept_ref[g, b]
     acc_ref[g, b] = acc_ref[g, b] + kept[0:1] * out
     kept_ref[g, b] = kept * jnp.concatenate(carries, axis=1)
@@ -202,24 +209,35 @@
             q_ref[b, half, HEAD * half : HEAD * (half + 1)] = q[:HEAD]
             q_ref[b, half, LANES : LANES + 16] = q[HEAD:]
 
-    def step(n, _):
-        g, b, j = n // (2 * ZSEGS), n // ZSEGS % 2, ZSEGS - 1 - n % ZSEGS
+    def side(n, _):
+        g, b = n // 2, n % 2
         far = jnp.where(g == 0, fars[0], fars[-1])
         block = jnp.where(b == y % 2, 4 * z + c, 31 - 4 * z - c)
-        ahead = block - (group_of(z, c, far) * ZSEGS + j)
-        args = (m_ref, q_ref, w_ref, acc_ref, kept_ref, ZSEGS * g + j, g, b)
-
-        @pl.when(ahead > 0)
+        ahead = block - group_of(z, c, far) * ZSEGS
+        refs = (m_ref, q_ref, w_ref, acc_ref, kept_ref)
+
+        @pl.when(ahead >= ZSEGS)
         def _():
-            segment(*args, False)
-
-        @pl.when(ahead == 0)
-        def _():
-            segment(*args, True)
+            def pair(i, _):
+                j = ZSEGS * g + ZSEGS - 1 - 2 * i
+                segments(*refs, (j, j - 1), g, b, None)
+                return 0
+
+            lax.fori_loop(0, ZSEGS // 2, pair, 0)
+
+        if fars[-1] % 2 or fars == (0,):
+
+            @pl.when((ahead >= 0) & (ahead < ZSEGS))
+            def _():
+                def single(i, _):
+                    segments(*refs, (ZSEGS * g + ahead - i,), g, b, i)
+                    return 0
+
+                lax.fori_loop(0, ahead + 1, single, 0)
 
         return 0
 
-    lax.fori_loop(0, count * 2 * ZSEGS, step, 0)
+    lax.fori_loop(0, count * 2, side, 0)
 
 
 def attend(fars, pos, q0, q1, kvs):
@@ -240,10 +258,9 @@
         scratch_shapes=[
             pltpu.VMEM((count * ZSEGS, TOK, LANES), bf),
             pltpu.VMEM((2, 2, 2 * LANES, TOK), bf),
-            pltpu.VMEM((2 * CHUNK, TOK), bf),
+            pltpu.VMEM((4, 2 * CHUNK, TOK), bf),
         ],
         cost_estimate=pl.CostEstimate(flops=count << 31, bytes_accessed=1 << 20, transcendentals=1 << 22),
-        name=f"attend{fars[-1]}",
     )(pos, q0, q1, *kvs)
 
 
@@ -355,6 +372,7 @@
         P("tp"),
         P("tp", None),
     )
+
     return jax.shard_map(
         shards, mesh=mesh, in_specs=placed, out_specs=P(("sp", "tp"), None), check_vma=False
     )

time: 147 us -> 146 us (level)
  Pallas kernels: 50.7 us -> 49.2 us
    pallas_call x5, Pallas kernels: 39.7 us -> 38.2 us  [attend(): pl.pallas_call(body, out_shape=(jax.ShapeDtypeStruct((count, 2, HEAD, TOK...]
  transfers between devices with their start and end apart: 35 -> 35, of which waited for: 10 -> 10; matrix products, arithmetic and copies ran while one was open for 0% -> 0% of each run, Pallas kernels for 23% -> 22%
where the time goes in v1:
time: 146 us
  starting transfers between devices  52.9 us (36%)
  Pallas kernels  49.2 us (34%)
  waiting for transfers between devices  31.6 us (22%)
  blocking collectives  9.48 us (6%)
  local copies, waits for them, and re-layouts  1.46 us (1%)
    ppermute x35, starting transfers between devices, send(): return lax.ppermute(a, AXES, move)  52.9 us
    pallas_call x5, Pallas kernels, attend(): pl.pallas_call(body, out_shape=(jax.ShapeDtypeStruct((count, 2, HEAD, TOK...  38.2 us
    ppermute x35, waiting for transfers between devices, send(): return lax.ppermute(a, AXES, move)  31.6 us
    all_to_all x1, blocking collectives, shards(): lax.all_to_all(att.reshape(X * C, ROWS, 2 * HEAD), 'tp', 0, 0, tiled=True)  9.48 us
    pallas_call x1, Pallas kernels, project(): pl.pallas_call(project_body, out_shape=(jax.ShapeDtypeStruct((QROWS, TOK)...  4.88 us
    pallas_call x1, Pallas kernels, output(): pl.pallas_call(output_body, out_shape=jax.ShapeDtypeStruct((ROWS, 2048),...  3.6 us
  transfers between devices with their start and end apart: 35, of which 10 were waited for; matrix products, arithmetic and copies ran while one was open for 0% of the time, Pallas kernels for 22%

profile of v1, /device:TPU:56, one launch (start us, length us, event | category | flops | bytes accessed | tf_op | source)
XLA Modules:
  0.0 145.7 jit_solution(10793252057510030440)
XLA Ops:
  0.0 1.5 %collective-permute-start = (bf16[64,2048]{1,0:T(8,128)(2,1)}, bf16[64,2048]{1,0:T(8,128)(2,1)S(1)}, u32[]{:S(2)}, u32[]{:S(2)}) collective-permute-start(bf16[64,2048]{1,0:T(8,128)(2,1)} %refs_0_.1), channel_id=1, source_target_pairs={{0,2},{1,7},{2,4},{3,1},{4,6},{5,3},{6,0},{7,5},{8,10},{9,15},{10,... | collective-permute-start | bytes 786440 | tf_op jit(solution)/shard_map/ppermute | solution.py:54
  1.5 1.7 %collective-permute-start.1 = (bf16[64,2048]{1,0:T(8,128)(2,1)}, bf16[64,2048]{1,0:T(8,128)(2,1)S(1)}, u32[]{:S(2)}, u32[]{:S(2)}) collective-permute-start(bf16[64,2048]{1,0:T(8,128)(2,1)} %refs_0_.1), channel_id=1, source_target_pairs={{0,6},{1,3},{2,0},{3,5},{4,2},{5,7},{6,4},{7,1},{8,14},{9,11},{10,... | collective-permute-start | bytes 786440 | tf_op jit(solution)/shard_map/ppermute | solution.py:54
  3.2 6.0 %collective-permute-done.refs_1_ = bf16[64,2048]{1,0:T(8,128)(2,1)S(1)} collective-permute-done((bf16[64,2048]{1,0:T(8,128)(2,1)}, bf16[64,2048]{1,0:T(8,128)(2,1)S(1)}, u32[]{:S(2)}, u32[]{:S(2)}) %collective-permute-start) | collective-permute-done | bytes 262176 | tf_op jit(solution)/shard_map/ppermute | solution.py:54
  9.3 1.5 collective-permute-start.2
  10.7 0.5 collective-permute-start.4
  11.3 5.5 %collective-permute-done.2.refs_3_ = bf16[64,2048]{1,0:T(8,128)(2,1)S(1)} collective-permute-done((bf16[64,2048]{1,0:T(8,128)(2,1)S(1)}, bf16[64,2048]{1,0:T(8,128)(2,1)S(1)}, u32[]{:S(2)}, u32[]{:S(2)}) %collective-permute-start.2) | collective-permute-done | bytes 262176 | tf_op jit(solution)/shard_map/ppermute | solution.py:54
  16.8 0.7 pad_add_fusion.pos.refs_0_
  17.5 0.8 collective-permute-done.6.refs_7_
  18.4 0.7 copy-done.13
  19.1 4.9 %project.1 = (bf16[80,512]{1,0:T(8,128)(2,1)}, bf16[80,512]{1,0:T(8,128)(2,1)}, bf16[512,128]{1,0:T(8,128)(2,1)}, bf16[512,128]{1,0:T(8,128)(2,1)}) custom-call(s32[2]{0:T(128)} %pad_add_fusion.pos.refs_0_, f32[2]{0:T(128)} %bias.1, bf16[64,2048]{1,0:T(8,128)(2,1)} %refs_0_.1, bf16[64,2048]{1,0:T(8,128)(2,1)} %copy-done.7, bf16[64,2048]{1,0:T(8,128)(2,1)} %copy-done.8, ...), custom_call_target="tpu_custom_call" | custom-call | flops 67108864 | bytes 4194304 | tf_op jit(solution)/shard_map/project/pallas_call | solution.py:119
  24.0 3.3 %collective-permute-start.9 = (bf16[512,128]{1,0:T(8,128)(2,1)}, bf16[512,128]{1,0:T(8,128)(2,1)S(1)}, u32[]{:S(2)}, u32[]{:S(2)}) collective-permute-start(bf16[512,128]{1,0:T(8,128)(2,1)} %get-tuple-element.53), channel_id=1, source_target_pairs={{0,0},{1,16},{2,2},{3,18},{4,4},{5,20},{6,6},{7,22},{8,1},{9,17},{... | collective-permute-start | bytes 393224 | tf_op jit(solution)/shard_map/ppermute | solution.py:54
  27.4 1.9 %collective-permute-start.10 = (bf16[512,128]{1,0:T(8,128)(2,1)}, bf16[512,128]{1,0:T(8,128)(2,1)S(1)}, u32[]{:S(2)}, u32[]{:S(2)}) collective-permute-start(bf16[512,128]{1,0:T(8,128)(2,1)} %get-tuple-element.54), channel_id=1, source_target_pairs={{0,8},{1,24},{2,10},{3,26},{4,12},{5,28},{6,14},{7,30},{8,9},{9,25... | collective-permute-start | bytes 393224 | tf_op jit(solution)/shard_map/ppermute | solution.py:54
  29.3 2.6 %collective-permute-done.9 = bf16[512,128]{1,0:T(8,128)(2,1)S(1)} collective-permute-done((bf16[512,128]{1,0:T(8,128)(2,1)}, bf16[512,128]{1,0:T(8,128)(2,1)S(1)}, u32[]{:S(2)}, u32[]{:S(2)}) %collective-permute-start.9) | collective-permute-done | bytes 131104 | tf_op jit(solution)/shard_map/ppermute | solution.py:54
  31.9 1.9 %collective-permute-done.10 = bf16[512,128]{1,0:T(8,128)(2,1)S(1)} collective-permute-done((bf16[512,128]{1,0:T(8,128)(2,1)}, bf16[512,128]{1,0:T(8,128)(2,1)S(1)}, u32[]{:S(2)}, u32[]{:S(2)}) %collective-permute-start.10) | collective-permute-done | bytes 131104 | tf_op jit(solution)/shard_map/ppermute | solution.py:54
  33.8 0.3 collective-permute-start.25
  34.1 0.2 collective-permute-start.12
  34.3 1.8 %collective-permute-start.11 = (bf16[2,512,128]{2,1,0:T(8,128)(2,1)S(1)}, bf16[2,512,128]{2,1,0:T(8,128)(2,1)S(1)}, u32[]{:S(2)}, u32[]{:S(2)}) collective-permute-start(bf16[2,512,128]{2,1,0:T(8,128)(2,1)S(1)} %pad_maximum_fusion.refs_3_), channel_id=1, source_target_pairs={{0,32},{1,225},{2,34},{3,227},{4,36},{5,229},{6,38},{7,231},{8,40}... | collective-permute-start | bytes 786440 | tf_op jit(solution)/shard_map/ppermute | solution.py:54
  36.1 8.7 %collective-permute-start.7 = (bf16[80,512]{1,0:T(8,128)(2,1)}, bf16[80,512]{1,0:T(8,128)(2,1)S(1)}, u32[]{:S(2)}, u32[]{:S(2)}) collective-permute-start(bf16[80,512]{1,0:T(8,128)(2,1)} %get-tuple-element.51), channel_id=1, source_target_pairs={{0,0},{1,16},{2,2},{3,18},{4,4},{5,20},{6,6},{7,22},{8,1},{9,17},{... | collective-permute-start | bytes 245768 | tf_op jit(solution)/shard_map/ppermute | solution.py:54
  44.8 2.9 %collective-permute-start.8 = (bf16[80,512]{1,0:T(8,128)(2,1)}, bf16[80,512]{1,0:T(8,128)(2,1)S(1)}, u32[]{:S(2)}, u32[]{:S(2)}) collective-permute-start(bf16[80,512]{1,0:T(8,128)(2,1)} %get-tuple-element.52), channel_id=1, source_target_pairs={{0,8},{1,24},{2,10},{3,26},{4,12},{5,28},{6,14},{7,30},{8,9},{9,25... | collective-permute-start | bytes 245768 | tf_op jit(solution)/shard_map/ppermute | solution.py:54
  47.8 1.0 collective-permute-start.14
  48.8 1.8 %collective-permute-start.15 = (bf16[2,512,128]{2,1,0:T(8,128)(2,1)S(1)}, bf16[2,512,128]{2,1,0:T(8,128)(2,1)}, u32[]{:S(2)}, u32[]{:S(2)}) collective-permute-start(bf16[2,512,128]{2,1,0:T(8,128)(2,1)S(1)} %collective-permute-done.12.refs_5_), channel_id=1, source_target_pairs={{0,224},{1,33},{2,226},{3,35},{4,228},{5,37},{6,230},{7,39},{8,232... | collective-permute-start | bytes 786440 | tf_op jit(solution)/shard_map/ppermute | solution.py:54
  50.6 0.3 collective-permute-done.8.refs_2_
  50.9 0.5 collective-permute-start.16
  51.4 0.1 copy-done.24
  51.6 4.8 %collective-permute-start.26 = (bf16[128,2048]{1,0:T(8,128)(2,1)S(1)}, bf16[128,2048]{1,0:T(8,128)(2,1)S(1)}, u32[]{:S(2)}, u32[]{:S(2)}) collective-permute-start(bf16[128,2048]{1,0:T(8,128)(2,1)S(1)} %copy-done), channel_id=1, source_target_pairs={{0,6},{1,3},{2,0},{3,5},{4,2},{5,7},{6,4},{7,1},{8,14},{9,11},{10,... | collective-permute-start | bytes 1572872 | tf_op jit(solution)/shard_map/ppermute | solution.py:54
  56.4 6.1 %shard_map.64 = (f32[1,2,64,512]{3,2,1,0:T(8,128)}, f32[1,2,8,512]{3,2,1,0:T(8,128)}) custom-call(s32[2]{0:T(128)} %pad_add_fusion.pos.refs_0_, bf16[80,512]{1,0:T(8,128)(2,1)} %copy-done.23, bf16[80,512]{1,0:T(8,128)(2,1)} %copy-done.24, bf16[2,512,128]{2,1,0:T(8,128)(2,1)} %copy-done.6, bf16[2,512,128]{2,1,0:T(8,128)(2,1)} %copy-done.19), custom_call_target="tpu_custom_call" | custom-call | flops 2147483648 | bytes 1048576 | tf_op jit(solution)/shard_map/pallas_call | solution.py:250
  62.6 1.1 collective-permute-start.21
  63.7 3.0 %collective-permute-start.19 = (bf16[2,512,128]{2,1,0:T(8,128)(2,1)}, bf16[2,512,128]{2,1,0:T(8,128)(2,1)}, u32[]{:S(2)}, u32[]{:S(2)}) collective-permute-start(bf16[2,512,128]{2,1,0:T(8,128)(2,1)} %collective-permute-done.15.refs_5_), channel_id=1, source_target_pairs={{0,224},{1,33},{2,226},{3,35},{4,228},{5,37},{6,230},{7,39},{8,232... | collective-permute-start | bytes 786440 | tf_op jit(solution)/shard_map/ppermute | solution.py:54
  66.8 12.0 %shard_map.65 = (f32[2,2,64,512]{3,2,1,0:T(8,128)}, f32[2,2,8,512]{3,2,1,0:T(8,128)}) custom-call(s32[2]{0:T(128)} %pad_add_fusion.pos.refs_0_, bf16[80,512]{1,0:T(8,128)(2,1)} %copy-done.23, bf16[80,512]{1,0:T(8,128)(2,1)} %copy-done.24, bf16[2,512,128]{2,1,0:T(8,128)(2,1)} %copy-done.16, bf16[2,512,128]{2,1,0:T(8,128)(2,1)} %copy-done.21, ...), custom_call_target="tpu_custom_call" | custom-call | flops 4294967296 | bytes 1048576 | tf_op jit(solution)/shard_map/pallas_call | solution.py:250
  78.8 0.5 collective-permute-start.20
  79.5 0.5 collective-permute-start.28
  80.0 0.3 collective-permute-start.30
  80.3 0.4 collective-permute-done.20.refs_4_
  80.7 0.4 collective-permute-start.29
  81.1 0.4 collective-permute-start.24
  81.4 0.3 copy-done.17
  81.8 4.4 %collective-permute-done.22.refs_3_ = bf16[2,512,128]{2,1,0:T(8,128)(2,1)} collective-permute-done((bf16[2,512,128]{2,1,0:T(8,128)(2,1)}, bf16[2,512,128]{2,1,0:T(8,128)(2,1)}, u32[]{:S(2)}, u32[]{:S(2)}) %collective-permute-start.22) | collective-permute-done | bytes 262176 | tf_op jit(solution)/shard_map/ppermute | solution.py:54
  86.1 5.6 %shard_map.66 = (f32[2,2,64,512]{3,2,1,0:T(8,128)}, f32[2,2,8,512]{3,2,1,0:T(8,128)}) custom-call(s32[2]{0:T(128)} %pad_add_fusion.pos.refs_0_, bf16[80,512]{1,0:T(8,128)(2,1)} %copy-done.23, bf16[80,512]{1,0:T(8,128)(2,1)} %copy-done.24, bf16[2,512,128]{2,1,0:T(8,128)(2,1)} %copy-done.14, bf16[2,512,128]{2,1,0:T(8,128)(2,1)} %copy-done.18, ...), custom_call_target="tpu_custom_call" | custom-call | flops 4294967296 | bytes 1048576 | tf_op jit(solution)/shard_map/pallas_call | solution.py:250
  91.7 0.6 collective-permute-start.32
  92.4 9.0 %shard_map.67 = (f32[2,2,64,512]{3,2,1,0:T(8,128)}, f32[2,2,8,512]{3,2,1,0:T(8,128)}) custom-call(s32[2]{0:T(128)} %pad_add_fusion.pos.refs_0_, bf16[80,512]{1,0:T(8,128)(2,1)} %copy-done.23, bf16[80,512]{1,0:T(8,128)(2,1)} %copy-done.24, bf16[2,512,128]{2,1,0:T(8,128)(2,1)} %collective-permute-done.18.refs_3_, bf16[2,512,128]{2,1,0:T(8,128)(2,1)} %copy-done.17, ...), custom_call_target="tpu_custom_call" | custom-call | flops 4294967296 | bytes 1048576 | tf_op jit(solution)/shard_map/pallas_call | solution.py:250
  101.5 5.5 %shard_map.68 = (f32[1,2,64,512]{3,2,1,0:T(8,128)}, f32[1,2,8,512]{3,2,1,0:T(8,128)}) custom-call(s32[2]{0:T(128)} %pad_add_fusion.pos.refs_0_, bf16[80,512]{1,0:T(8,128)(2,1)} %copy-done.23, bf16[80,512]{1,0:T(8,128)(2,1)} %copy-done.24, bf16[2,512,128]{2,1,0:T(8,128)(2,1)} %collective-permute-done.22.refs_3_, ...), custom_call_target="tpu_custom_call" | custom-call | flops 2147483648 | bytes 1048576 | tf_op jit(solution)/shard_map/pallas_call | solution.py:250
  107.0 2.5 %merge.1 = (bf16[64,512]{1,0:T(8,128)(2,1)}, bf16[64,512]{1,0:T(8,128)(2,1)}) custom-call(s32[2]{0:T(128)} %pad_add_fusion.pos.refs_0_, f32[1,2,64,512]{3,2,1,0:T(8,128)} %get-tuple-element.59.refs_1_, f32[2,2,64,512]{3,2,1,0:T(8,128)} %get-tuple-element.65.refs_2_, f32[2,2,64,512]{3,2,1,0:T(8,128)} %get-tuple-element.71.refs_3_, ...), custom_call_target="tpu_custom_call" | custom-call | tf_op jit(solution)/shard_map/merge/pallas_call | solution.py:288
  109.5 13.2 %collective-permute-start.33 = (bf16[64,512]{1,0:T(8,128)(2,1)}, bf16[64,512]{1,0:T(8,128)(2,1)S(1)}, u32[]{:S(2)}, u32[]{:S(2)}) collective-permute-start(bf16[64,512]{1,0:T(8,128)(2,1)} %get-tuple-element.87), channel_id=1, source_target_pairs={{0,0},{16,1},{2,2},{18,3},{4,4},{20,5},{6,6},{22,7},{1,8},{17,9},{... | collective-permute-start | bytes 196616 | tf_op jit(solution)/shard_map/ppermute | solution.py:54
  122.9 4.0 %collective-permute-done.33 = bf16[64,512]{1,0:T(8,128)(2,1)S(1)} collective-permute-done((bf16[64,512]{1,0:T(8,128)(2,1)}, bf16[64,512]{1,0:T(8,128)(2,1)S(1)}, u32[]{:S(2)}, u32[]{:S(2)}) %collective-permute-start.33) | collective-permute-done | bytes 65568 | tf_op jit(solution)/shard_map/ppermute | solution.py:54
  126.9 5.6 %collective-permute-done.34 = bf16[64,512]{1,0:T(8,128)(2,1)S(1)} collective-permute-done((bf16[64,512]{1,0:T(8,128)(2,1)}, bf16[64,512]{1,0:T(8,128)(2,1)S(1)}, u32[]{:S(2)}, u32[]{:S(2)}) %collective-permute-start.34) | collective-permute-done | bytes 65568 | tf_op jit(solution)/shard_map/ppermute | solution.py:54
  132.5 0.1 copy.7
  132.6 9.5 %all_to_all.5.att = bf16[8,64,128]{2,1,0:T(8,128)(2,1)} all-to-all(bf16[8,64,128]{2,1,0:T(8,128)(2,1)S(1)} %bitcast.7), channel_id=1, replica_groups=mesh['sp'=32,'tp'=8] {'tp'}, dimensions={0} | all-to-all | bytes 262144 | tf_op jit(solution)/shard_map/all_to_all | solution.py:362
  142.1 3.6 %output.1 = bf16[64,2048]{1,0:T(8,128)(2,1)} custom-call(s32[2]{0:T(128)} %pad_add_fusion.pos.refs_0_, bf16[8,64,128]{2,1,0:T(8,128)(2,1)} %all_to_all.5.att, bf16[128,2048]{1,0:T(8,128)(2,1)} %refs_0_.2, bf16[128,2048]{1,0:T(8,128)(2,1)} %copy-done.1, bf16[128,2048]{1,0:T(8,128)(2,1)} %copy-done.2, bf16[128,2048]{1,0:T(8,128)(2,1)} %copy-done.3, ...), custom_call_target="tpu_custom_call" | custom-call | tf_op jit(solution)/shard_map/output/pallas_call | solution.py:307
  (85 shorter events, 0.7 us)
Async XLA Ops:
  0.0 9.3 %collective-permute-start = (bf16[64,2048]{1,0:T(8,128)(2,1)}, bf16[64,2048]{1,0:T(8,128)(2,1)S(1)}, u32[]{:S(2)}, u32[]{:S(2)}) collective-permute-start(bf16[64,2048]{1,0:T(8,128)(2,1)} %refs_0_.1), channel_id=1, source_target_pairs={{0,2},{1,7},{2,4},{3,1},{4,6},{5,3},{6,0},{7,5},{8,10},{9,15},{10,... | collective-permute-start | bytes 786440 | tf_op jit(solution)/shard_map/ppermute | solution.py:54
  1.5 9.7 %collective-permute-start.1 = (bf16[64,2048]{1,0:T(8,128)(2,1)}, bf16[64,2048]{1,0:T(8,128)(2,1)S(1)}, u32[]{:S(2)}, u32[]{:S(2)}) collective-permute-start(bf16[64,2048]{1,0:T(8,128)(2,1)} %refs_0_.1), channel_id=1, source_target_pairs={{0,6},{1,3},{2,0},{3,5},{4,2},{5,7},{6,4},{7,1},{8,14},{9,11},{10,... | collective-permute-start | bytes 786440 | tf_op jit(solution)/shard_map/ppermute | solution.py:54
  9.3 9.1 %copy-start.7 = (bf16[64,2048]{1,0:T(8,128)(2,1)}, bf16[64,2048]{1,0:T(8,128)(2,1)S(1)}, u32[]{:S(2)}) copy-start(bf16[64,2048]{1,0:T(8,128)(2,1)S(1)} %collective-permute-done.refs_1_) | copy-start | bytes 786436
  9.3 7.6 %collective-permute-start.2 = (bf16[64,2048]{1,0:T(8,128)(2,1)S(1)}, bf16[64,2048]{1,0:T(8,128)(2,1)S(1)}, u32[]{:S(2)}, u32[]{:S(2)}) collective-permute-start(bf16[64,2048]{1,0:T(8,128)(2,1)S(1)} %collective-permute-done.refs_1_), channel_id=1, source_target_pairs={{0,2},{1,7},{2,4},{3,1},{4,6},{5,3},{6,0},{7,5},{8,10},{9,15},{10,... | collective-permute-start | bytes 786440 | tf_op jit(solution)/shard_map/ppermute | solution.py:54
  10.7 6.8 %collective-permute-start.3 = (bf16[64,2048]{1,0:T(8,128)(2,1)}, bf16[64,2048]{1,0:T(8,128)(2,1)S(1)}, u32[]{:S(2)}, u32[]{:S(2)}) collective-permute-start(bf16[64,2048]{1,0:T(8,128)(2,1)} %refs_0_.1), channel_id=1, source_target_pairs={{0,1},{1,0},{2,3},{3,2},{4,5},{5,4},{6,7},{7,6},{8,9},{9,8},{10,11... | collective-permute-start | bytes 786440 | tf_op jit(solution)/shard_map/ppermute | solution.py:54
  10.7 6.8 %collective-permute-start.4 = (bf16[64,2048]{1,0:T(8,128)(2,1)S(1)}, bf16[64,2048]{1,0:T(8,128)(2,1)S(1)}, u32[]{:S(2)}, u32[]{:S(2)}) collective-permute-start(bf16[64,2048]{1,0:T(8,128)(2,1)S(1)} %collective-permute-done.refs_1_), channel_id=1, source_target_pairs={{0,1},{1,0},{2,3},{3,2},{4,5},{5,4},{6,7},{7,6},{8,9},{9,8},{10,11... | collective-permute-start | bytes 786440 | tf_op jit(solution)/shard_map/ppermute | solution.py:54
  11.2 7.2 %copy-start.8 = (bf16[64,2048]{1,0:T(8,128)(2,1)}, bf16[64,2048]{1,0:T(8,128)(2,1)S(1)}, u32[]{:S(2)}) copy-start(bf16[64,2048]{1,0:T(8,128)(2,1)S(1)} %collective-permute-done.1.refs_2_) | copy-start | bytes 786436
  11.2 6.3 %collective-permute-start.5 = (bf16[64,2048]{1,0:T(8,128)(2,1)S(1)}, bf16[64,2048]{1,0:T(8,128)(2,1)S(1)}, u32[]{:S(2)}, u32[]{:S(2)}) collective-permute-start(bf16[64,2048]{1,0:T(8,128)(2,1)S(1)} %collective-permute-done.1.refs_2_), channel_id=1, source_target_pairs={{0,1},{1,0},{2,3},{3,2},{4,5},{5,4},{6,7},{7,6},{8,9},{9,8},{10,11... | collective-permute-start | bytes 786440 | tf_op jit(solution)/shard_map/ppermute | solution.py:54
  16.8 1.5 %collective-permute-start.6 = (bf16[64,2048]{1,0:T(8,128)(2,1)S(1)}, bf16[64,2048]{1,0:T(8,128)(2,1)S(1)}, u32[]{:S(2)}, u32[]{:S(2)}) collective-permute-start(bf16[64,2048]{1,0:T(8,128)(2,1)S(1)} %collective-permute-done.2.refs_3_), channel_id=1, source_target_pairs={{0,1},{1,0},{2,3},{3,2},{4,5},{5,4},{6,7},{7,6},{8,9},{9,8},{10,11... | collective-permute-start | bytes 786440 | tf_op jit(solution)/shard_map/ppermute | solution.py:54
  24.0 9.8 %copy-start = (bf16[128,2048]{1,0:T(8,128)(2,1)S(1)}, bf16[128,2048]{1,0:T(8,128)(2,1)}, u32[]{:S(2)}) copy-start(bf16[128,2048]{1,0:T(8,128)(2,1)} %refs_0_.2) | copy-start | bytes 1572868
  24.0 7.9 %collective-permute-start.9 = (bf16[512,128]{1,0:T(8,128)(2,1)}, bf16[512,128]{1,0:T(8,128)(2,1)S(1)}, u32[]{:S(2)}, u32[]{:S(2)}) collective-permute-start(bf16[512,128]{1,0:T(8,128)(2,1)} %get-tuple-element.53), channel_id=1, source_target_pairs={{0,0},{1,16},{2,2},{3,18},{4,4},{5,20},{6,6},{7,22},{8,1},{9,17},{... | collective-permute-start | bytes 393224 | tf_op jit(solution)/shard_map/ppermute | solution.py:54
  27.4 6.4 %collective-permute-start.10 = (bf16[512,128]{1,0:T(8,128)(2,1)}, bf16[512,128]{1,0:T(8,128)(2,1)S(1)}, u32[]{:S(2)}, u32[]{:S(2)}) collective-permute-start(bf16[512,128]{1,0:T(8,128)(2,1)} %get-tuple-element.54), channel_id=1, source_target_pairs={{0,8},{1,24},{2,10},{3,26},{4,12},{5,28},{6,14},{7,30},{8,9},{9,25... | collective-permute-start | bytes 393224 | tf_op jit(solution)/shard_map/ppermute | solution.py:54
  33.8 22.6 %copy-start.6 = (bf16[2,512,128]{2,1,0:T(8,128)(2,1)}, bf16[2,512,128]{2,1,0:T(8,128)(2,1)S(1)}, u32[]{:S(2)}) copy-start(bf16[2,512,128]{2,1,0:T(8,128)(2,1)S(1)} %pad_maximum_fusion.refs_3_) | copy-start | bytes 786436
  33.8 17.8 %collective-permute-start.25 = (bf16[128,2048]{1,0:T(8,128)(2,1)S(1)}, bf16[128,2048]{1,0:T(8,128)(2,1)S(1)}, u32[]{:S(2)}, u32[]{:S(2)}) collective-permute-start(bf16[128,2048]{1,0:T(8,128)(2,1)S(1)} %copy-done), channel_id=1, source_target_pairs={{0,2},{1,7},{2,4},{3,1},{4,6},{5,3},{6,0},{7,5},{8,10},{9,15},{10,... | collective-permute-start | bytes 1572872 | tf_op jit(solution)/shard_map/ppermute | solution.py:54
  34.1 10.7 %collective-permute-start.12 = (bf16[2,512,128]{2,1,0:T(8,128)(2,1)S(1)}, bf16[2,512,128]{2,1,0:T(8,128)(2,1)S(1)}, u32[]{:S(2)}, u32[]{:S(2)}) collective-permute-start(bf16[2,512,128]{2,1,0:T(8,128)(2,1)S(1)} %pad_maximum_fusion.refs_3_), channel_id=1, source_target_pairs={{0,224},{1,33},{2,226},{3,35},{4,228},{5,37},{6,230},{7,39},{8,232... | collective-permute-start | bytes 786440 | tf_op jit(solution)/shard_map/ppermute | solution.py:54
  34.3 13.5 %collective-permute-start.11 = (bf16[2,512,128]{2,1,0:T(8,128)(2,1)S(1)}, bf16[2,512,128]{2,1,0:T(8,128)(2,1)S(1)}, u32[]{:S(2)}, u32[]{:S(2)}) collective-permute-start(bf16[2,512,128]{2,1,0:T(8,128)(2,1)S(1)} %pad_maximum_fusion.refs_3_), channel_id=1, source_target_pairs={{0,32},{1,225},{2,34},{3,227},{4,36},{5,229},{6,38},{7,231},{8,40}... | collective-permute-start | bytes 786440 | tf_op jit(solution)/shard_map/ppermute | solution.py:54
  36.1 14.8 %collective-permute-start.13 = (bf16[2,512,128]{2,1,0:T(8,128)(2,1)S(1)}, bf16[2,512,128]{2,1,0:T(8,128)(2,1)S(1)}, u32[]{:S(2)}, u32[]{:S(2)}) collective-permute-start(bf16[2,512,128]{2,1,0:T(8,128)(2,1)S(1)} %pad_maximum_fusion.refs_3_), channel_id=1, source_target_pairs={{0,1},{1,0},{2,3},{3,2},{4,5},{5,4},{6,7},{7,6},{8,9},{9,8},{10,11... | collective-permute-start | bytes 786440 | tf_op jit(solution)/shard_map/ppermute | solution.py:54
  36.1 12.6 %collective-permute-start.7 = (bf16[80,512]{1,0:T(8,128)(2,1)}, bf16[80,512]{1,0:T(8,128)(2,1)S(1)}, u32[]{:S(2)}, u32[]{:S(2)}) collective-permute-start(bf16[80,512]{1,0:T(8,128)(2,1)} %get-tuple-element.51), channel_id=1, source_target_pairs={{0,0},{1,16},{2,2},{3,18},{4,4},{5,20},{6,6},{7,22},{8,1},{9,17},{... | collective-permute-start | bytes 245768 | tf_op jit(solution)/shard_map/ppermute | solution.py:54
  44.8 17.6 %copy-start.15 = (bf16[2,512,128]{2,1,0:T(8,128)(2,1)}, bf16[2,512,128]{2,1,0:T(8,128)(2,1)S(1)}, u32[]{:S(2)}) copy-start(bf16[2,512,128]{2,1,0:T(8,128)(2,1)S(1)} %collective-permute-done.12.refs_5_) | copy-start | bytes 786436
  44.8 6.1 %collective-permute-start.8 = (bf16[80,512]{1,0:T(8,128)(2,1)}, bf16[80,512]{1,0:T(8,128)(2,1)S(1)}, u32[]{:S(2)}, u32[]{:S(2)}) collective-permute-start(bf16[80,512]{1,0:T(8,128)(2,1)} %get-tuple-element.52), channel_id=1, source_target_pairs={{0,8},{1,24},{2,10},{3,26},{4,12},{5,28},{6,14},{7,30},{8,9},{9,25... | collective-permute-start | bytes 245768 | tf_op jit(solution)/shard_map/ppermute | solution.py:54
  47.8 14.7 %copy-start.16 = (bf16[2,512,128]{2,1,0:T(8,128)(2,1)}, bf16[2,512,128]{2,1,0:T(8,128)(2,1)S(1)}, u32[]{:S(2)}) copy-start(bf16[2,512,128]{2,1,0:T(8,128)(2,1)S(1)} %collective-permute-done.11.refs_3_) | copy-start | bytes 786436
  47.8 14.7 %collective-permute-start.14 = (bf16[2,512,128]{2,1,0:T(8,128)(2,1)S(1)}, bf16[2,512,128]{2,1,0:T(8,128)(2,1)S(1)}, u32[]{:S(2)}, u32[]{:S(2)}) collective-permute-start(bf16[2,512,128]{2,1,0:T(8,128)(2,1)S(1)} %collective-permute-done.11.refs_3_), channel_id=1, source_target_pairs={{0,32},{1,225},{2,34},{3,227},{4,36},{5,229},{6,38},{7,231},{8,40}... | collective-permute-start | bytes 786440 | tf_op jit(solution)/shard_map/ppermute | solution.py:54
  48.8 7.6 %copy-start.23 = (bf16[80,512]{1,0:T(8,128)(2,1)}, bf16[80,512]{1,0:T(8,128)(2,1)S(1)}, u32[]{:S(2)}) copy-start(bf16[80,512]{1,0:T(8,128)(2,1)S(1)} %collective-permute-done.7.refs_1_) | copy-start | bytes 245764
  48.8 13.8 %collective-permute-start.15 = (bf16[2,512,128]{2,1,0:T(8,128)(2,1)S(1)}, bf16[2,512,128]{2,1,0:T(8,128)(2,1)}, u32[]{:S(2)}, u32[]{:S(2)}) collective-permute-start(bf16[2,512,128]{2,1,0:T(8,128)(2,1)S(1)} %collective-permute-done.12.refs_5_), channel_id=1, source_target_pairs={{0,224},{1,33},{2,226},{3,35},{4,228},{5,37},{6,230},{7,39},{8,232... | collective-permute-start | bytes 786440 | tf_op jit(solution)/shard_map/ppermute | solution.py:54
  50.9 12.8 %collective-permute-start.17 = (bf16[2,512,128]{2,1,0:T(8,128)(2,1)S(1)}, bf16[2,512,128]{2,1,0:T(8,128)(2,1)S(1)}, u32[]{:S(2)}, u32[]{:S(2)}) collective-permute-start(bf16[2,512,128]{2,1,0:T(8,128)(2,1)S(1)} %collective-permute-done.11.refs_3_), channel_id=1, source_target_pairs={{0,1},{1,0},{2,3},{3,2},{4,5},{5,4},{6,7},{7,6},{8,9},{9,8},{10,11... | collective-permute-start | bytes 786440 | tf_op jit(solution)/shard_map/ppermute | solution.py:54
  50.9 12.8 %collective-permute-start.16 = (bf16[2,512,128]{2,1,0:T(8,128)(2,1)S(1)}, bf16[2,512,128]{2,1,0:T(8,128)(2,1)S(1)}, u32[]{:S(2)}, u32[]{:S(2)}) collective-permute-start(bf16[2,512,128]{2,1,0:T(8,128)(2,1)S(1)} %collective-permute-done.12.refs_5_), channel_id=1, source_target_pairs={{0,1},{1,0},{2,3},{3,2},{4,5},{5,4},{6,7},{7,6},{8,9},{9,8},{10,11... | collective-permute-start | bytes 786440 | tf_op jit(solution)/shard_map/ppermute | solution.py:54
  51.6 29.1 %copy-start.1 = (bf16[128,2048]{1,0:T(8,128)(2,1)}, bf16[128,2048]{1,0:T(8,128)(2,1)S(1)}, u32[]{:S(2)}) copy-start(bf16[128,2048]{1,0:T(8,128)(2,1)S(1)} %collective-permute-done.25.refs_1_) | copy-start | bytes 1572868
  51.6 27.9 %collective-permute-start.26 = (bf16[128,2048]{1,0:T(8,128)(2,1)S(1)}, bf16[128,2048]{1,0:T(8,128)(2,1)S(1)}, u32[]{:S(2)}, u32[]{:S(2)}) collective-permute-start(bf16[128,2048]{1,0:T(8,128)(2,1)S(1)} %copy-done), channel_id=1, source_target_pairs={{0,6},{1,3},{2,0},{3,5},{4,2},{5,7},{6,4},{7,1},{8,14},{9,11},{10,... | collective-permute-start | bytes 1572872 | tf_op jit(solution)/shard_map/ppermute | solution.py:54
  62.5 16.3 %copy-start.14 = (bf16[2,512,128]{2,1,0:T(8,128)(2,1)}, bf16[2,512,128]{2,1,0:T(8,128)(2,1)S(1)}, u32[]{:S(2)}) copy-start(bf16[2,512,128]{2,1,0:T(8,128)(2,1)S(1)} %collective-permute-done.14.refs_3_) | copy-start | bytes 786436
  62.5 17.0 %collective-permute-start.27 = (bf16[128,2048]{1,0:T(8,128)(2,1)S(1)}, bf16[128,2048]{1,0:T(8,128)(2,1)S(1)}, u32[]{:S(2)}, u32[]{:S(2)}) collective-permute-start(bf16[128,2048]{1,0:T(8,128)(2,1)S(1)} %collective-permute-done.25.refs_1_), channel_id=1, source_target_pairs={{0,2},{1,7},{2,4},{3,1},{4,6},{5,3},{6,0},{7,5},{8,10},{9,15},{10,... | collective-permute-start | bytes 1572872 | tf_op jit(solution)/shard_map/ppermute | solution.py:54
  62.6 17.4 %collective-permute-start.21 = (bf16[2,512,128]{2,1,0:T(8,128)(2,1)S(1)}, bf16[2,512,128]{2,1,0:T(8,128)(2,1)}, u32[]{:S(2)}, u32[]{:S(2)}) collective-permute-start(bf16[2,512,128]{2,1,0:T(8,128)(2,1)S(1)} %collective-permute-done.14.refs_3_), channel_id=1, source_target_pairs={{0,1},{1,0},{2,3},{3,2},{4,5},{5,4},{6,7},{7,6},{8,9},{9,8},{10,11... | collective-permute-start | bytes 786440 | tf_op jit(solution)/shard_map/ppermute | solution.py:54
  63.7 15.1 %collective-permute-start.18 = (bf16[2,512,128]{2,1,0:T(8,128)(2,1)S(1)}, bf16[2,512,128]{2,1,0:T(8,128)(2,1)}, u32[]{:S(2)}, u32[]{:S(2)}) collective-permute-start(bf16[2,512,128]{2,1,0:T(8,128)(2,1)S(1)} %collective-permute-done.14.refs_3_), channel_id=1, source_target_pairs={{0,32},{1,225},{2,34},{3,227},{4,36},{5,229},{6,38},{7,231},{8,40}... | collective-permute-start | bytes 786440 | tf_op jit(solution)/shard_map/ppermute | solution.py:54
  63.7 15.6 %collective-permute-start.19 = (bf16[2,512,128]{2,1,0:T(8,128)(2,1)}, bf16[2,512,128]{2,1,0:T(8,128)(2,1)}, u32[]{:S(2)}, u32[]{:S(2)}) collective-permute-start(bf16[2,512,128]{2,1,0:T(8,128)(2,1)} %collective-permute-done.15.refs_5_), channel_id=1, source_target_pairs={{0,224},{1,33},{2,226},{3,35},{4,228},{5,37},{6,230},{7,39},{8,232... | collective-permute-start | bytes 786440 | tf_op jit(solution)/shard_map/ppermute | solution.py:54
  78.8 1.9 %collective-permute-start.20 = (bf16[2,512,128]{2,1,0:T(8,128)(2,1)}, bf16[2,512,128]{2,1,0:T(8,128)(2,1)S(1)}, u32[]{:S(2)}, u32[]{:S(2)}) collective-permute-start(bf16[2,512,128]{2,1,0:T(8,128)(2,1)} %collective-permute-done.15.refs_5_), channel_id=1, source_target_pairs={{0,1},{1,0},{2,3},{3,2},{4,5},{5,4},{6,7},{7,6},{8,9},{9,8},{10,11... | collective-permute-start | bytes 786440 | tf_op jit(solution)/shard_map/ppermute | solution.py:54
  79.3 1.8 %collective-permute-start.23 = (bf16[2,512,128]{2,1,0:T(8,128)(2,1)}, bf16[2,512,128]{2,1,0:T(8,128)(2,1)S(1)}, u32[]{:S(2)}, u32[]{:S(2)}) collective-permute-start(bf16[2,512,128]{2,1,0:T(8,128)(2,1)} %collective-permute-done.19.refs_5_), channel_id=1, source_target_pairs={{0,1},{1,0},{2,3},{3,2},{4,5},{5,4},{6,7},{7,6},{8,9},{9,8},{10,11... | collective-permute-start | bytes 786440 | tf_op jit(solution)/shard_map/ppermute | solution.py:54
  79.4 12.3 %copy-start.2 = (bf16[128,2048]{1,0:T(8,128)(2,1)}, bf16[128,2048]{1,0:T(8,128)(2,1)S(1)}, u32[]{:S(2)}) copy-start(bf16[128,2048]{1,0:T(8,128)(2,1)S(1)} %collective-permute-done.26.refs_2_) | copy-start | bytes 1572868
  79.4 6.7 %collective-permute-start.22 = (bf16[2,512,128]{2,1,0:T(8,128)(2,1)}, bf16[2,512,128]{2,1,0:T(8,128)(2,1)}, u32[]{:S(2)}, u32[]{:S(2)}) collective-permute-start(bf16[2,512,128]{2,1,0:T(8,128)(2,1)} %collective-permute-done.18.refs_3_), channel_id=1, source_target_pairs={{0,32},{1,225},{2,34},{3,227},{4,36},{5,229},{6,38},{7,231},{8,40}... | collective-permute-start | bytes 786440 | tf_op jit(solution)/shard_map/ppermute | solution.py:54
  79.4 12.3 %copy-start.3 = (bf16[128,2048]{1,0:T(8,128)(2,1)}, bf16[128,2048]{1,0:T(8,128)(2,1)S(1)}, u32[]{:S(2)}) copy-start(bf16[128,2048]{1,0:T(8,128)(2,1)S(1)} %collective-permute-done.27.refs_3_) | copy-start | bytes 1572868
  79.5 22.0 %collective-permute-start.28 = (bf16[128,2048]{1,0:T(8,128)(2,1)S(1)}, bf16[128,2048]{1,0:T(8,128)(2,1)S(1)}, u32[]{:S(2)}, u32[]{:S(2)}) collective-permute-start(bf16[128,2048]{1,0:T(8,128)(2,1)S(1)} %copy-done), channel_id=1, source_target_pairs={{0,1},{1,0},{2,3},{3,2},{4,5},{5,4},{6,7},{7,6},{8,9},{9,8},{10,11... | collective-permute-start | bytes 1572872 | tf_op jit(solution)/shard_map/ppermute | solution.py:54
  80.0 21.5 %collective-permute-start.30 = (bf16[128,2048]{1,0:T(8,128)(2,1)S(1)}, bf16[128,2048]{1,0:T(8,128)(2,1)S(1)}, u32[]{:S(2)}, u32[]{:S(2)}) collective-permute-start(bf16[128,2048]{1,0:T(8,128)(2,1)S(1)} %collective-permute-done.26.refs_2_), channel_id=1, source_target_pairs={{0,1},{1,0},{2,3},{3,2},{4,5},{5,4},{6,7},{7,6},{8,9},{9,8},{10,11... | collective-permute-start | bytes 1572872 | tf_op jit(solution)/shard_map/ppermute | solution.py:54
  80.7 20.8 %collective-permute-start.29 = (bf16[128,2048]{1,0:T(8,128)(2,1)S(1)}, bf16[128,2048]{1,0:T(8,128)(2,1)}, u32[]{:S(2)}, u32[]{:S(2)}) collective-permute-start(bf16[128,2048]{1,0:T(8,128)(2,1)S(1)} %collective-permute-done.25.refs_1_), channel_id=1, source_target_pairs={{0,1},{1,0},{2,3},{3,2},{4,5},{5,4},{6,7},{7,6},{8,9},{9,8},{10,11... | collective-permute-start | bytes 1572872 | tf_op jit(solution)/shard_map/ppermute | solution.py:54
  81.1 10.7 %collective-permute-start.24 = (bf16[2,512,128]{2,1,0:T(8,128)(2,1)}, bf16[2,512,128]{2,1,0:T(8,128)(2,1)S(1)}, u32[]{:S(2)}, u32[]{:S(2)}) collective-permute-start(bf16[2,512,128]{2,1,0:T(8,128)(2,1)} %collective-permute-done.18.refs_3_), channel_id=1, source_target_pairs={{0,1},{1,0},{2,3},{3,2},{4,5},{5,4},{6,7},{7,6},{8,9},{9,8},{10,11... | collective-permute-start | bytes 786440 | tf_op jit(solution)/shard_map/ppermute | solution.py:54
  86.1 15.4 %collective-permute-start.31 = (bf16[128,2048]{1,0:T(8,128)(2,1)S(1)}, bf16[128,2048]{1,0:T(8,128)(2,1)}, u32[]{:S(2)}, u32[]{:S(2)}) collective-permute-start(bf16[128,2048]{1,0:T(8,128)(2,1)S(1)} %collective-permute-done.27.refs_3_), channel_id=1, source_target_pairs={{0,1},{1,0},{2,3},{3,2},{4,5},{5,4},{6,7},{7,6},{8,9},{9,8},{10,11... | collective-permute-start | bytes 1572872 | tf_op jit(solution)/shard_map/ppermute | solution.py:54
  91.7 9.7 %collective-permute-start.32 = (bf16[2,512,128]{2,1,0:T(8,128)(2,1)}, bf16[2,512,128]{2,1,0:T(8,128)(2,1)}, u32[]{:S(2)}, u32[]{:S(2)}) collective-permute-start(bf16[2,512,128]{2,1,0:T(8,128)(2,1)} %collective-permute-done.22.refs_3_), channel_id=1, source_target_pairs={{0,1},{1,0},{2,3},{3,2},{4,5},{5,4},{6,7},{7,6},{8,9},{9,8},{10,11... | collective-permute-start | bytes 786440 | tf_op jit(solution)/shard_map/ppermute | solution.py:54
  101.4 5.6 %copy-start.4 = (bf16[128,2048]{1,0:T(8,128)(2,1)}, bf16[128,2048]{1,0:T(8,128)(2,1)S(1)}, u32[]{:S(2)}) copy-start(bf16[128,2048]{1,0:T(8,128)(2,1)S(1)} %collective-permute-done.28.refs_4_) | copy-start | bytes 1572868
  101.5 5.6 %copy-start.5 = (bf16[128,2048]{1,0:T(8,128)(2,1)}, bf16[128,2048]{1,0:T(8,128)(2,1)S(1)}, u32[]{:S(2)}) copy-start(bf16[128,2048]{1,0:T(8,128)(2,1)S(1)} %collective-permute-done.30.refs_6_) | copy-start | bytes 1572868
  109.5 17.3 %collective-permute-start.33 = (bf16[64,512]{1,0:T(8,128)(2,1)}, bf16[64,512]{1,0:T(8,128)(2,1)S(1)}, u32[]{:S(2)}, u32[]{:S(2)}) collective-permute-start(bf16[64,512]{1,0:T(8,128)(2,1)} %get-tuple-element.87), channel_id=1, source_target_pairs={{0,0},{16,1},{2,2},{18,3},{4,4},{20,5},{6,6},{22,7},{1,8},{17,9},{... | collective-permute-start | bytes 196616 | tf_op jit(solution)/shard_map/ppermute | solution.py:54
  122.8 9.7 %collective-permute-start.34 = (bf16[64,512]{1,0:T(8,128)(2,1)}, bf16[64,512]{1,0:T(8,128)(2,1)S(1)}, u32[]{:S(2)}, u32[]{:S(2)}) collective-permute-start(bf16[64,512]{1,0:T(8,128)(2,1)} %get-tuple-element.88), channel_id=1, source_target_pairs={{8,0},{24,1},{10,2},{26,3},{12,4},{28,5},{14,6},{30,7},{9,8},{25,9... | collective-permute-start | bytes 196616 | tf_op jit(solution)/shard_map/ppermute | solution.py:54
  (12 other events, 24.0 us)

commit v2 on v1

--- a/solution.py
+++ b/solution.py
@@ -162,27 +162,37 @@
     lane = lax.broadcasted_iota(jnp.int32, (1, LANES), 1)
     ones = jnp.broadcast_to(jnp.where(lane < 3, 1.0, 0.0), (256, LANES)).astype(jnp.bfloat16)
     out = None
-    for i, place in enumerate(places):
-        keys = jnp.concatenate([m_ref[place, :256], ones], axis=1)
-        for half in (1, 0):
-            scores = jnp.dot(keys, q_ref[b, half], preferred_element_type=jnp.float32)
-            w = w_ref.at[2 * i + half]
-            for s in (CHUNK, 0):
-                for n in range(TOK // LANES):
-                    t = slice(n * LANES, (n + 1) * LANES)
-                    start = n * LANES - s - 256 * half
-                    w[s : s + CHUNK, t], carries[n] = chunk_weights(
-                        scores[s : s + CHUNK, t],
-                        None if ahead is None else start + TOK * ahead,
-                        carries[n],
-                    )
-            first = 256 + 2 * HEAD * half
-            values = jnp.concatenate(
-                [m_ref[place, first : first + HEAD], m_ref[place, first + HEAD : first + 2 * HEAD]],
-                axis=1,
-            )
-            part = jnp.dot(values, w[...], preferred_element_type=jnp.float32)
+    stages = [(i, half) for i in range(len(places)) for half in (1, 0)]
+
+    def scores_of(i, half):
+        keys = jnp.concatenate([m_ref[places[i], :256], ones], axis=1)
+        return jnp.dot(keys, q_ref[b, half], preferred_element_type=jnp.float32)
+
+    def product(i, half):
+        first = 256 + 2 * HEAD * half
+        values = [m_ref[places[i], first + n * HEAD : first + (n + 1) * HEAD] for n in range(2)]
+        return jnp.dot(
+            jnp.concatenate(values, axis=1), w_ref[2 * i + half], preferred_element_type=jnp.float32
+        )
+
+    following = scores_of(*stages[0])
+    for k, (i, half) in enumerate(stages):
+        scores = following
+        if k + 1 < len(stages):
+            following = scores_of(*stages[k + 1])
+        if k:
+            part = product(*stages[k - 1])
             out = part if out is None else out + part
+        for s in (CHUNK, 0):
+            for n in range(TOK // LANES):
+                t = slice(n * LANES, (n + 1) * LANES)
+                start = n * LANES - s - 256 * half
+                w_ref[2 * i + half, s : s + CHUNK, t], carries[n] = chunk_weights(
+                    scores[s : s + CHUNK, t],
+                    None if ahead is None else start + TOK * ahead,
+                    carries[n],
+                )
+    out = out + product(*stages[-1])
     kept = kept_ref[g, b]
     acc_ref[g, b] = acc_ref[g, b] + kept[0:1] * out
     kept_ref[g, b] = kept * jnp.concatenate(carries, axis=1)
@@ -317,9 +327,9 @@
     return lax.optimization_barrier((a, *others))[0]
 
 
-def across_x(a):
+def across_x(a, *before):
     first, second = send(a, X_FIRST), send(a, X_SECOND)
-    return [a, first, second, send(first, X_FIRST)]
+    return [a, first, second, send(after(first, *before), X_FIRST)]
 
 
 def from_all_tp(mine):
@@ -330,7 +340,7 @@
     sp, tp = lax.axis_index("sp"), lax.axis_index("tp")
     pos = jnp.stack([sp, tp]).astype(jnp.int32)
     y = sp % Y
-    mine = across_x(tokens)
+    mine = across_x(tokens, pos)
     pieces = from_all_tp(mine)
     q0, q1, kv0, kv1 = project(pos, head_bias, pieces, (w_query, w_key, w_value))
     q0, q1 = send(q0, Q_MOVE[0]), send(q1, Q_MOVE[1])

time: 146 us -> 141 us (0.966)
  Pallas kernels: 49.2 us -> 45.4 us
    pallas_call x5, Pallas kernels: 38.2 us -> 34.4 us  [attend(): pl.pallas_call(body, out_shape=(jax.ShapeDtypeStruct((count, 2, HEAD, TOK...]
  transfers between devices with their start and end apart: 35 -> 35, of which waited for: 10 -> 10; matrix products, arithmetic and copies ran while one was open for 0% -> 0% of each run, Pallas kernels for 22% -> 21%
where the time goes in v2:
time: 141 us; the launch traced here: 140 us
  starting transfers between devices  51.7 us (37%)
  Pallas kernels  45.4 us (32%)
  waiting for transfers between devices  31 us (22%)
  blocking collectives  9.48 us (7%)
  local copies, waits for them, and re-layouts  1.68 us (1%)
    ppermute x35, starting transfers between devices, send(): return lax.ppermute(a, AXES, move)  51.7 us
    pallas_call x5, Pallas kernels, attend(): pl.pallas_call(body, out_shape=(jax.ShapeDtypeStruct((count, 2, HEAD, TOK...  34.4 us
    ppermute x35, waiting for transfers between devices, send(): return lax.ppermute(a, AXES, move)  31 us
    all_to_all x1, blocking collectives, shards(): lax.all_to_all(att.reshape(X * C, ROWS, 2 * HEAD), 'tp', 0, 0, tiled=True)  9.48 us
    pallas_call x1, Pallas kernels, project(): pl.pallas_call(project_body, out_shape=(jax.ShapeDtypeStruct((QROWS, TOK)...  4.88 us
    pallas_call x1, Pallas kernels, output(): pl.pallas_call(output_body, out_shape=jax.ShapeDtypeStruct((ROWS, 2048),...  3.6 us
  transfers between devices with their start and end apart: 35, of which 10 were waited for; matrix products, arithmetic and copies ran while one was open for 0% of the time, Pallas kernels for 21%

profile of v2, /device:TPU:56, one launch (start us, length us, event | category | flops | bytes accessed | tf_op | source)
XLA Modules:
  0.0 140.3 jit_solution(6676263616254828110)
XLA Ops:
  0.0 1.5 %collective-permute-start = (bf16[64,2048]{1,0:T(8,128)(2,1)}, bf16[64,2048]{1,0:T(8,128)(2,1)S(1)}, u32[]{:S(2)}, u32[]{:S(2)}) collective-permute-start(bf16[64,2048]{1,0:T(8,128)(2,1)} %refs_0_.1), channel_id=1, source_target_pairs={{0,2},{1,7},{2,4},{3,1},{4,6},{5,3},{6,0},{7,5},{8,10},{9,15},{10,... | collective-permute-start | bytes 786440 | tf_op jit(solution)/shard_map/ppermute | solution.py:54
  1.5 1.7 %collective-permute-start.1 = (bf16[64,2048]{1,0:T(8,128)(2,1)}, bf16[64,2048]{1,0:T(8,128)(2,1)S(1)}, u32[]{:S(2)}, u32[]{:S(2)}) collective-permute-start(bf16[64,2048]{1,0:T(8,128)(2,1)} %refs_0_.1), channel_id=1, source_target_pairs={{0,6},{1,3},{2,0},{3,5},{4,2},{5,7},{6,4},{7,1},{8,14},{9,11},{10,... | collective-permute-start | bytes 786440 | tf_op jit(solution)/shard_map/ppermute | solution.py:54
  3.2 0.6 pad_add_fusion.pos.refs_0_
  3.9 5.4 %collective-permute-done.refs_1_ = bf16[64,2048]{1,0:T(8,128)(2,1)S(1)} collective-permute-done((bf16[64,2048]{1,0:T(8,128)(2,1)}, bf16[64,2048]{1,0:T(8,128)(2,1)S(1)}, u32[]{:S(2)}, u32[]{:S(2)}) %collective-permute-start) | collective-permute-done | bytes 262176 | tf_op jit(solution)/shard_map/ppermute | solution.py:54
  9.3 1.5 %collective-permute-start.2 = (bf16[64,2048]{1,0:T(8,128)(2,1)S(1)}, bf16[64,2048]{1,0:T(8,128)(2,1)S(1)}, u32[]{:S(2)}, u32[]{:S(2)}) collective-permute-start(bf16[64,2048]{1,0:T(8,128)(2,1)S(1)} %collective-permute-done.refs_1_), channel_id=1, source_target_pairs={{0,2},{1,7},{2,4},{3,1},{4,6},{5,3},{6,0},{7,5},{8,10},{9,15},{10,... | collective-permute-start | bytes 786440 | tf_op jit(solution)/shard_map/ppermute | solution.py:54
  10.7 0.5 collective-permute-start.4
  11.3 5.5 %collective-permute-done.2.refs_3_ = bf16[64,2048]{1,0:T(8,128)(2,1)S(1)} collective-permute-done((bf16[64,2048]{1,0:T(8,128)(2,1)S(1)}, bf16[64,2048]{1,0:T(8,128)(2,1)S(1)}, u32[]{:S(2)}, u32[]{:S(2)}) %collective-permute-start.2) | collective-permute-done | bytes 262176 | tf_op jit(solution)/shard_map/ppermute | solution.py:54
  16.9 1.5 %collective-permute-done.6.refs_7_ = bf16[64,2048]{1,0:T(8,128)(2,1)S(1)} collective-permute-done((bf16[64,2048]{1,0:T(8,128)(2,1)S(1)}, bf16[64,2048]{1,0:T(8,128)(2,1)S(1)}, u32[]{:S(2)}, u32[]{:S(2)}) %collective-permute-start.6) | collective-permute-done | bytes 262176 | tf_op jit(solution)/shard_map/ppermute | solution.py:54
  18.4 0.7 copy-done.13
  19.1 4.9 %project.1 = (bf16[80,512]{1,0:T(8,128)(2,1)}, bf16[80,512]{1,0:T(8,128)(2,1)}, bf16[512,128]{1,0:T(8,128)(2,1)}, bf16[512,128]{1,0:T(8,128)(2,1)}) custom-call(s32[2]{0:T(128)} %pad_add_fusion.pos.refs_0_, f32[2]{0:T(128)} %bias.1, bf16[64,2048]{1,0:T(8,128)(2,1)} %refs_0_.1, bf16[64,2048]{1,0:T(8,128)(2,1)} %copy-done.7, bf16[64,2048]{1,0:T(8,128)(2,1)} %copy-done.8, ...), custom_call_target="tpu_custom_call" | custom-call | flops 67108864 | bytes 4194304 | tf_op jit(solution)/shard_map/project/pallas_call | solution.py:119
  24.0 3.0 %collective-permute-start.9 = (bf16[512,128]{1,0:T(8,128)(2,1)}, bf16[512,128]{1,0:T(8,128)(2,1)S(1)}, u32[]{:S(2)}, u32[]{:S(2)}) collective-permute-start(bf16[512,128]{1,0:T(8,128)(2,1)} %get-tuple-element.55), channel_id=1, source_target_pairs={{0,0},{1,16},{2,2},{3,18},{4,4},{5,20},{6,6},{7,22},{8,1},{9,17},{... | collective-permute-start | bytes 393224 | tf_op jit(solution)/shard_map/ppermute | solution.py:54
  27.0 2.2 %collective-permute-start.10 = (bf16[512,128]{1,0:T(8,128)(2,1)}, bf16[512,128]{1,0:T(8,128)(2,1)S(1)}, u32[]{:S(2)}, u32[]{:S(2)}) collective-permute-start(bf16[512,128]{1,0:T(8,128)(2,1)} %get-tuple-element.56), channel_id=1, source_target_pairs={{0,8},{1,24},{2,10},{3,26},{4,12},{5,28},{6,14},{7,30},{8,9},{9,25... | collective-permute-start | bytes 393224 | tf_op jit(solution)/shard_map/ppermute | solution.py:54
  29.3 2.6 %collective-permute-done.9 = bf16[512,128]{1,0:T(8,128)(2,1)S(1)} collective-permute-done((bf16[512,128]{1,0:T(8,128)(2,1)}, bf16[512,128]{1,0:T(8,128)(2,1)S(1)}, u32[]{:S(2)}, u32[]{:S(2)}) %collective-permute-start.9) | collective-permute-done | bytes 131104 | tf_op jit(solution)/shard_map/ppermute | solution.py:54
  31.9 1.5 %collective-permute-done.10 = bf16[512,128]{1,0:T(8,128)(2,1)S(1)} collective-permute-done((bf16[512,128]{1,0:T(8,128)(2,1)}, bf16[512,128]{1,0:T(8,128)(2,1)S(1)}, u32[]{:S(2)}, u32[]{:S(2)}) %collective-permute-start.10) | collective-permute-done | bytes 131104 | tf_op jit(solution)/shard_map/ppermute | solution.py:54
  33.5 0.3 collective-permute-start.25
  33.8 0.2 collective-permute-start.12
  34.0 1.8 %collective-permute-start.11 = (bf16[2,512,128]{2,1,0:T(8,128)(2,1)S(1)}, bf16[2,512,128]{2,1,0:T(8,128)(2,1)S(1)}, u32[]{:S(2)}, u32[]{:S(2)}) collective-permute-start(bf16[2,512,128]{2,1,0:T(8,128)(2,1)S(1)} %pad_maximum_fusion.refs_3_), channel_id=1, source_target_pairs={{0,32},{1,225},{2,34},{3,227},{4,36},{5,229},{6,38},{7,231},{8,40}... | collective-permute-start | bytes 786440 | tf_op jit(solution)/shard_map/ppermute | solution.py:54
  35.8 8.4 %collective-permute-start.7 = (bf16[80,512]{1,0:T(8,128)(2,1)}, bf16[80,512]{1,0:T(8,128)(2,1)S(1)}, u32[]{:S(2)}, u32[]{:S(2)}) collective-permute-start(bf16[80,512]{1,0:T(8,128)(2,1)} %get-tuple-element.53), channel_id=1, source_target_pairs={{0,0},{1,16},{2,2},{3,18},{4,4},{5,20},{6,6},{7,22},{8,1},{9,17},{... | collective-permute-start | bytes 245768 | tf_op jit(solution)/shard_map/ppermute | solution.py:54
  44.2 3.5 %collective-permute-start.8 = (bf16[80,512]{1,0:T(8,128)(2,1)}, bf16[80,512]{1,0:T(8,128)(2,1)S(1)}, u32[]{:S(2)}, u32[]{:S(2)}) collective-permute-start(bf16[80,512]{1,0:T(8,128)(2,1)} %get-tuple-element.54), channel_id=1, source_target_pairs={{0,8},{1,24},{2,10},{3,26},{4,12},{5,28},{6,14},{7,30},{8,9},{9,25... | collective-permute-start | bytes 245768 | tf_op jit(solution)/shard_map/ppermute | solution.py:54
  47.8 1.0 collective-permute-start.14
  48.8 1.5 %collective-permute-start.15 = (bf16[2,512,128]{2,1,0:T(8,128)(2,1)S(1)}, bf16[2,512,128]{2,1,0:T(8,128)(2,1)}, u32[]{:S(2)}, u32[]{:S(2)}) collective-permute-start(bf16[2,512,128]{2,1,0:T(8,128)(2,1)S(1)} %collective-permute-done.12.refs_5_), channel_id=1, source_target_pairs={{0,224},{1,33},{2,226},{3,35},{4,228},{5,37},{6,230},{7,39},{8,232... | collective-permute-start | bytes 786440 | tf_op jit(solution)/shard_map/ppermute | solution.py:54
  50.3 0.7 collective-permute-done.8.refs_2_
  50.9 0.5 collective-permute-start.16
  51.4 0.1 copy-done.24
  51.6 4.5 %collective-permute-start.26 = (bf16[128,2048]{1,0:T(8,128)(2,1)S(1)}, bf16[128,2048]{1,0:T(8,128)(2,1)S(1)}, u32[]{:S(2)}, u32[]{:S(2)}) collective-permute-start(bf16[128,2048]{1,0:T(8,128)(2,1)S(1)} %copy-done), channel_id=1, source_target_pairs={{0,6},{1,3},{2,0},{3,5},{4,2},{5,7},{6,4},{7,1},{8,14},{9,11},{10,... | collective-permute-start | bytes 1572872 | tf_op jit(solution)/shard_map/ppermute | solution.py:54
  56.0 5.5 %shard_map.64 = (f32[1,2,64,512]{3,2,1,0:T(8,128)}, f32[1,2,8,512]{3,2,1,0:T(8,128)}) custom-call(s32[2]{0:T(128)} %pad_add_fusion.pos.refs_0_, bf16[80,512]{1,0:T(8,128)(2,1)} %copy-done.23, bf16[80,512]{1,0:T(8,128)(2,1)} %copy-done.24, bf16[2,512,128]{2,1,0:T(8,128)(2,1)} %copy-done.6, bf16[2,512,128]{2,1,0:T(8,128)(2,1)} %copy-done.19), custom_call_target="tpu_custom_call" | custom-call | flops 2147483648 | bytes 1048576 | tf_op jit(solution)/shard_map/pallas_call | solution.py:260
  61.7 1.1 collective-permute-start.21
  62.8 3.0 %collective-permute-start.19 = (bf16[2,512,128]{2,1,0:T(8,128)(2,1)}, bf16[2,512,128]{2,1,0:T(8,128)(2,1)}, u32[]{:S(2)}, u32[]{:S(2)}) collective-permute-start(bf16[2,512,128]{2,1,0:T(8,128)(2,1)} %collective-permute-done.15.refs_5_), channel_id=1, source_target_pairs={{0,224},{1,33},{2,226},{3,35},{4,228},{5,37},{6,230},{7,39},{8,232... | collective-permute-start | bytes 786440 | tf_op jit(solution)/shard_map/ppermute | solution.py:54
  65.9 10.4 %shard_map.65 = (f32[2,2,64,512]{3,2,1,0:T(8,128)}, f32[2,2,8,512]{3,2,1,0:T(8,128)}) custom-call(s32[2]{0:T(128)} %pad_add_fusion.pos.refs_0_, bf16[80,512]{1,0:T(8,128)(2,1)} %copy-done.23, bf16[80,512]{1,0:T(8,128)(2,1)} %copy-done.24, bf16[2,512,128]{2,1,0:T(8,128)(2,1)} %copy-done.16, bf16[2,512,128]{2,1,0:T(8,128)(2,1)} %copy-done.21, ...), custom_call_target="tpu_custom_call" | custom-call | flops 4294967296 | bytes 1048576 | tf_op jit(solution)/shard_map/pallas_call | solution.py:260
  76.3 0.5 collective-permute-start.20
  76.8 0.1 collective-permute-start.23
  76.9 1.0 collective-permute-start.28
  78.0 0.1 collective-permute-done.20.refs_4_
  78.1 0.6 collective-permute-start.29
  78.7 0.1 collective-permute-start.24
  78.9 0.6 copy-done.17
  79.4 4.1 %collective-permute-done.22.refs_3_ = bf16[2,512,128]{2,1,0:T(8,128)(2,1)} collective-permute-done((bf16[2,512,128]{2,1,0:T(8,128)(2,1)}, bf16[2,512,128]{2,1,0:T(8,128)(2,1)}, u32[]{:S(2)}, u32[]{:S(2)}) %collective-permute-start.22) | collective-permute-done | bytes 262176 | tf_op jit(solution)/shard_map/ppermute | solution.py:54
  83.6 5.0 %shard_map.66 = (f32[2,2,64,512]{3,2,1,0:T(8,128)}, f32[2,2,8,512]{3,2,1,0:T(8,128)}) custom-call(s32[2]{0:T(128)} %pad_add_fusion.pos.refs_0_, bf16[80,512]{1,0:T(8,128)(2,1)} %copy-done.23, bf16[80,512]{1,0:T(8,128)(2,1)} %copy-done.24, bf16[2,512,128]{2,1,0:T(8,128)(2,1)} %copy-done.14, bf16[2,512,128]{2,1,0:T(8,128)(2,1)} %copy-done.18, ...), custom_call_target="tpu_custom_call" | custom-call | flops 4294967296 | bytes 1048576 | tf_op jit(solution)/shard_map/pallas_call | solution.py:260
  88.6 0.6 collective-permute-start.32
  89.3 8.4 %shard_map.67 = (f32[2,2,64,512]{3,2,1,0:T(8,128)}, f32[2,2,8,512]{3,2,1,0:T(8,128)}) custom-call(s32[2]{0:T(128)} %pad_add_fusion.pos.refs_0_, bf16[80,512]{1,0:T(8,128)(2,1)} %copy-done.23, bf16[80,512]{1,0:T(8,128)(2,1)} %copy-done.24, bf16[2,512,128]{2,1,0:T(8,128)(2,1)} %collective-permute-done.18.refs_3_, bf16[2,512,128]{2,1,0:T(8,128)(2,1)} %copy-done.17, ...), custom_call_target="tpu_custom_call" | custom-call | flops 4294967296 | bytes 1048576 | tf_op jit(solution)/shard_map/pallas_call | solution.py:260
  97.8 5.0 %shard_map.68 = (f32[1,2,64,512]{3,2,1,0:T(8,128)}, f32[1,2,8,512]{3,2,1,0:T(8,128)}) custom-call(s32[2]{0:T(128)} %pad_add_fusion.pos.refs_0_, bf16[80,512]{1,0:T(8,128)(2,1)} %copy-done.23, bf16[80,512]{1,0:T(8,128)(2,1)} %copy-done.24, bf16[2,512,128]{2,1,0:T(8,128)(2,1)} %collective-permute-done.22.refs_3_, ...), custom_call_target="tpu_custom_call" | custom-call | flops 2147483648 | bytes 1048576 | tf_op jit(solution)/shard_map/pallas_call | solution.py:260
  102.8 2.5 %merge.1 = (bf16[64,512]{1,0:T(8,128)(2,1)}, bf16[64,512]{1,0:T(8,128)(2,1)}) custom-call(s32[2]{0:T(128)} %pad_add_fusion.pos.refs_0_, f32[1,2,64,512]{3,2,1,0:T(8,128)} %get-tuple-element.61.refs_1_, f32[2,2,64,512]{3,2,1,0:T(8,128)} %get-tuple-element.67.refs_2_, f32[2,2,64,512]{3,2,1,0:T(8,128)} %get-tuple-element.73.refs_3_, ...), custom_call_target="tpu_custom_call" | custom-call | tf_op jit(solution)/shard_map/merge/pallas_call | solution.py:298
  105.3 12.1 %collective-permute-start.33 = (bf16[64,512]{1,0:T(8,128)(2,1)}, bf16[64,512]{1,0:T(8,128)(2,1)S(1)}, u32[]{:S(2)}, u32[]{:S(2)}) collective-permute-start(bf16[64,512]{1,0:T(8,128)(2,1)} %get-tuple-element.89), channel_id=1, source_target_pairs={{0,0},{16,1},{2,2},{18,3},{4,4},{20,5},{6,6},{22,7},{1,8},{17,9},{... | collective-permute-start | bytes 196616 | tf_op jit(solution)/shard_map/ppermute | solution.py:54
  117.5 3.7 %collective-permute-done.33 = bf16[64,512]{1,0:T(8,128)(2,1)S(1)} collective-permute-done((bf16[64,512]{1,0:T(8,128)(2,1)}, bf16[64,512]{1,0:T(8,128)(2,1)S(1)}, u32[]{:S(2)}, u32[]{:S(2)}) %collective-permute-start.33) | collective-permute-done | bytes 65568 | tf_op jit(solution)/shard_map/ppermute | solution.py:54
  121.3 5.8 %collective-permute-done.34 = bf16[64,512]{1,0:T(8,128)(2,1)S(1)} collective-permute-done((bf16[64,512]{1,0:T(8,128)(2,1)}, bf16[64,512]{1,0:T(8,128)(2,1)S(1)}, u32[]{:S(2)}, u32[]{:S(2)}) %collective-permute-start.34) | collective-permute-done | bytes 65568 | tf_op jit(solution)/shard_map/ppermute | solution.py:54
  127.1 0.1 copy.7
  127.3 9.5 %all_to_all.5.att = bf16[8,64,128]{2,1,0:T(8,128)(2,1)} all-to-all(bf16[8,64,128]{2,1,0:T(8,128)(2,1)S(1)} %bitcast.7), channel_id=1, replica_groups=mesh['sp'=32,'tp'=8] {'tp'}, dimensions={0} | all-to-all | bytes 262144 | tf_op jit(solution)/shard_map/all_to_all | solution.py:372
  136.7 3.6 %output.1 = bf16[64,2048]{1,0:T(8,128)(2,1)} custom-call(s32[2]{0:T(128)} %pad_add_fusion.pos.refs_0_, bf16[8,64,128]{2,1,0:T(8,128)(2,1)} %all_to_all.5.att, bf16[128,2048]{1,0:T(8,128)(2,1)} %refs_0_.2, bf16[128,2048]{1,0:T(8,128)(2,1)} %copy-done.1, bf16[128,2048]{1,0:T(8,128)(2,1)} %copy-done.2, bf16[128,2048]{1,0:T(8,128)(2,1)} %copy-done.3, ...), custom_call_target="tpu_custom_call" | custom-call | tf_op jit(solution)/shard_map/output/pallas_call | solution.py:317
  (85 shorter events, 0.7 us)
Async XLA Ops:
  0.0 9.3 %collective-permute-start = (bf16[64,2048]{1,0:T(8,128)(2,1)}, bf16[64,2048]{1,0:T(8,128)(2,1)S(1)}, u32[]{:S(2)}, u32[]{:S(2)}) collective-permute-start(bf16[64,2048]{1,0:T(8,128)(2,1)} %refs_0_.1), channel_id=1, source_target_pairs={{0,2},{1,7},{2,4},{3,1},{4,6},{5,3},{6,0},{7,5},{8,10},{9,15},{10,... | collective-permute-start | bytes 786440 | tf_op jit(solution)/shard_map/ppermute | solution.py:54
  1.5 9.7 %collective-permute-start.1 = (bf16[64,2048]{1,0:T(8,128)(2,1)}, bf16[64,2048]{1,0:T(8,128)(2,1)S(1)}, u32[]{:S(2)}, u32[]{:S(2)}) collective-permute-start(bf16[64,2048]{1,0:T(8,128)(2,1)} %refs_0_.1), channel_id=1, source_target_pairs={{0,6},{1,3},{2,0},{3,5},{4,2},{5,7},{6,4},{7,1},{8,14},{9,11},{10,... | collective-permute-start | bytes 786440 | tf_op jit(solution)/shard_map/ppermute | solution.py:54
  9.3 9.1 %copy-start.7 = (bf16[64,2048]{1,0:T(8,128)(2,1)}, bf16[64,2048]{1,0:T(8,128)(2,1)S(1)}, u32[]{:S(2)}) copy-start(bf16[64,2048]{1,0:T(8,128)(2,1)S(1)} %collective-permute-done.refs_1_) | copy-start | bytes 786436
  9.3 7.6 %collective-permute-start.2 = (bf16[64,2048]{1,0:T(8,128)(2,1)S(1)}, bf16[64,2048]{1,0:T(8,128)(2,1)S(1)}, u32[]{:S(2)}, u32[]{:S(2)}) collective-permute-start(bf16[64,2048]{1,0:T(8,128)(2,1)S(1)} %collective-permute-done.refs_1_), channel_id=1, source_target_pairs={{0,2},{1,7},{2,4},{3,1},{4,6},{5,3},{6,0},{7,5},{8,10},{9,15},{10,... | collective-permute-start | bytes 786440 | tf_op jit(solution)/shard_map/ppermute | solution.py:54
  10.7 6.1 %collective-permute-start.3 = (bf16[64,2048]{1,0:T(8,128)(2,1)}, bf16[64,2048]{1,0:T(8,128)(2,1)S(1)}, u32[]{:S(2)}, u32[]{:S(2)}) collective-permute-start(bf16[64,2048]{1,0:T(8,128)(2,1)} %refs_0_.1), channel_id=1, source_target_pairs={{0,1},{1,0},{2,3},{3,2},{4,5},{5,4},{6,7},{7,6},{8,9},{9,8},{10,11... | collective-permute-start | bytes 786440 | tf_op jit(solution)/shard_map/ppermute | solution.py:54
  10.7 6.2 %collective-permute-start.4 = (bf16[64,2048]{1,0:T(8,128)(2,1)S(1)}, bf16[64,2048]{1,0:T(8,128)(2,1)S(1)}, u32[]{:S(2)}, u32[]{:S(2)}) collective-permute-start(bf16[64,2048]{1,0:T(8,128)(2,1)S(1)} %collective-permute-done.refs_1_), channel_id=1, source_target_pairs={{0,1},{1,0},{2,3},{3,2},{4,5},{5,4},{6,7},{7,6},{8,9},{9,8},{10,11... | collective-permute-start | bytes 786440 | tf_op jit(solution)/shard_map/ppermute | solution.py:54
  11.2 7.2 %copy-start.8 = (bf16[64,2048]{1,0:T(8,128)(2,1)}, bf16[64,2048]{1,0:T(8,128)(2,1)S(1)}, u32[]{:S(2)}) copy-start(bf16[64,2048]{1,0:T(8,128)(2,1)S(1)} %collective-permute-done.1.refs_2_) | copy-start | bytes 786436
  11.2 5.6 %collective-permute-start.5 = (bf16[64,2048]{1,0:T(8,128)(2,1)S(1)}, bf16[64,2048]{1,0:T(8,128)(2,1)S(1)}, u32[]{:S(2)}, u32[]{:S(2)}) collective-permute-start(bf16[64,2048]{1,0:T(8,128)(2,1)S(1)} %collective-permute-done.1.refs_2_), channel_id=1, source_target_pairs={{0,1},{1,0},{2,3},{3,2},{4,5},{5,4},{6,7},{7,6},{8,9},{9,8},{10,11... | collective-permute-start | bytes 786440 | tf_op jit(solution)/shard_map/ppermute | solution.py:54
  16.8 1.5 %collective-permute-start.6 = (bf16[64,2048]{1,0:T(8,128)(2,1)S(1)}, bf16[64,2048]{1,0:T(8,128)(2,1)S(1)}, u32[]{:S(2)}, u32[]{:S(2)}) collective-permute-start(bf16[64,2048]{1,0:T(8,128)(2,1)S(1)} %collective-permute-done.2.refs_3_), channel_id=1, source_target_pairs={{0,1},{1,0},{2,3},{3,2},{4,5},{5,4},{6,7},{7,6},{8,9},{9,8},{10,11... | collective-permute-start | bytes 786440 | tf_op jit(solution)/shard_map/ppermute | solution.py:54
  24.0 9.4 %copy-start = (bf16[128,2048]{1,0:T(8,128)(2,1)S(1)}, bf16[128,2048]{1,0:T(8,128)(2,1)}, u32[]{:S(2)}) copy-start(bf16[128,2048]{1,0:T(8,128)(2,1)} %refs_0_.2) | copy-start | bytes 1572868
  24.0 7.9 %collective-permute-start.9 = (bf16[512,128]{1,0:T(8,128)(2,1)}, bf16[512,128]{1,0:T(8,128)(2,1)S(1)}, u32[]{:S(2)}, u32[]{:S(2)}) collective-permute-start(bf16[512,128]{1,0:T(8,128)(2,1)} %get-tuple-element.55), channel_id=1, source_target_pairs={{0,0},{1,16},{2,2},{3,18},{4,4},{5,20},{6,6},{7,22},{8,1},{9,17},{... | collective-permute-start | bytes 393224 | tf_op jit(solution)/shard_map/ppermute | solution.py:54
  27.0 6.4 %collective-permute-start.10 = (bf16[512,128]{1,0:T(8,128)(2,1)}, bf16[512,128]{1,0:T(8,128)(2,1)S(1)}, u32[]{:S(2)}, u32[]{:S(2)}) collective-permute-start(bf16[512,128]{1,0:T(8,128)(2,1)} %get-tuple-element.56), channel_id=1, source_target_pairs={{0,8},{1,24},{2,10},{3,26},{4,12},{5,28},{6,14},{7,30},{8,9},{9,25... | collective-permute-start | bytes 393224 | tf_op jit(solution)/shard_map/ppermute | solution.py:54
  33.4 22.6 %copy-start.6 = (bf16[2,512,128]{2,1,0:T(8,128)(2,1)}, bf16[2,512,128]{2,1,0:T(8,128)(2,1)S(1)}, u32[]{:S(2)}) copy-start(bf16[2,512,128]{2,1,0:T(8,128)(2,1)S(1)} %pad_maximum_fusion.refs_3_) | copy-start | bytes 786436
  33.5 18.1 %collective-permute-start.25 = (bf16[128,2048]{1,0:T(8,128)(2,1)S(1)}, bf16[128,2048]{1,0:T(8,128)(2,1)S(1)}, u32[]{:S(2)}, u32[]{:S(2)}) collective-permute-start(bf16[128,2048]{1,0:T(8,128)(2,1)S(1)} %copy-done), channel_id=1, source_target_pairs={{0,2},{1,7},{2,4},{3,1},{4,6},{5,3},{6,0},{7,5},{8,10},{9,15},{10,... | collective-permute-start | bytes 1572872 | tf_op jit(solution)/shard_map/ppermute | solution.py:54
  33.8 10.4 %collective-permute-start.12 = (bf16[2,512,128]{2,1,0:T(8,128)(2,1)S(1)}, bf16[2,512,128]{2,1,0:T(8,128)(2,1)S(1)}, u32[]{:S(2)}, u32[]{:S(2)}) collective-permute-start(bf16[2,512,128]{2,1,0:T(8,128)(2,1)S(1)} %pad_maximum_fusion.refs_3_), channel_id=1, source_target_pairs={{0,224},{1,33},{2,226},{3,35},{4,228},{5,37},{6,230},{7,39},{8,232... | collective-permute-start | bytes 786440 | tf_op jit(solution)/shard_map/ppermute | solution.py:54
  34.0 13.8 %collective-permute-start.11 = (bf16[2,512,128]{2,1,0:T(8,128)(2,1)S(1)}, bf16[2,512,128]{2,1,0:T(8,128)(2,1)S(1)}, u32[]{:S(2)}, u32[]{:S(2)}) collective-permute-start(bf16[2,512,128]{2,1,0:T(8,128)(2,1)S(1)} %pad_maximum_fusion.refs_3_), channel_id=1, source_target_pairs={{0,32},{1,225},{2,34},{3,227},{4,36},{5,229},{6,38},{7,231},{8,40}... | collective-permute-start | bytes 786440 | tf_op jit(solution)/shard_map/ppermute | solution.py:54
  35.8 15.1 %collective-permute-start.13 = (bf16[2,512,128]{2,1,0:T(8,128)(2,1)S(1)}, bf16[2,512,128]{2,1,0:T(8,128)(2,1)S(1)}, u32[]{:S(2)}, u32[]{:S(2)}) collective-permute-start(bf16[2,512,128]{2,1,0:T(8,128)(2,1)S(1)} %pad_maximum_fusion.refs_3_), channel_id=1, source_target_pairs={{0,1},{1,0},{2,3},{3,2},{4,5},{5,4},{6,7},{7,6},{8,9},{9,8},{10,11... | collective-permute-start | bytes 786440 | tf_op jit(solution)/shard_map/ppermute | solution.py:54
  35.8 13.0 %collective-permute-start.7 = (bf16[80,512]{1,0:T(8,128)(2,1)}, bf16[80,512]{1,0:T(8,128)(2,1)S(1)}, u32[]{:S(2)}, u32[]{:S(2)}) collective-permute-start(bf16[80,512]{1,0:T(8,128)(2,1)} %get-tuple-element.53), channel_id=1, source_target_pairs={{0,0},{1,16},{2,2},{3,18},{4,4},{5,20},{6,6},{7,22},{8,1},{9,17},{... | collective-permute-start | bytes 245768 | tf_op jit(solution)/shard_map/ppermute | solution.py:54
  44.2 17.4 %copy-start.15 = (bf16[2,512,128]{2,1,0:T(8,128)(2,1)}, bf16[2,512,128]{2,1,0:T(8,128)(2,1)S(1)}, u32[]{:S(2)}) copy-start(bf16[2,512,128]{2,1,0:T(8,128)(2,1)S(1)} %collective-permute-done.12.refs_5_) | copy-start | bytes 786436
  44.2 6.7 %collective-permute-start.8 = (bf16[80,512]{1,0:T(8,128)(2,1)}, bf16[80,512]{1,0:T(8,128)(2,1)S(1)}, u32[]{:S(2)}, u32[]{:S(2)}) collective-permute-start(bf16[80,512]{1,0:T(8,128)(2,1)} %get-tuple-element.54), channel_id=1, source_target_pairs={{0,8},{1,24},{2,10},{3,26},{4,12},{5,28},{6,14},{7,30},{8,9},{9,25... | collective-permute-start | bytes 245768 | tf_op jit(solution)/shard_map/ppermute | solution.py:54
  47.8 13.8 %copy-start.16 = (bf16[2,512,128]{2,1,0:T(8,128)(2,1)}, bf16[2,512,128]{2,1,0:T(8,128)(2,1)S(1)}, u32[]{:S(2)}) copy-start(bf16[2,512,128]{2,1,0:T(8,128)(2,1)S(1)} %collective-permute-done.11.refs_3_) | copy-start | bytes 786436
  47.8 13.8 %collective-permute-start.14 = (bf16[2,512,128]{2,1,0:T(8,128)(2,1)S(1)}, bf16[2,512,128]{2,1,0:T(8,128)(2,1)S(1)}, u32[]{:S(2)}, u32[]{:S(2)}) collective-permute-start(bf16[2,512,128]{2,1,0:T(8,128)(2,1)S(1)} %collective-permute-done.11.refs_3_), channel_id=1, source_target_pairs={{0,32},{1,225},{2,34},{3,227},{4,36},{5,229},{6,38},{7,231},{8,40}... | collective-permute-start | bytes 786440 | tf_op jit(solution)/shard_map/ppermute | solution.py:54
  48.8 7.3 %copy-start.23 = (bf16[80,512]{1,0:T(8,128)(2,1)}, bf16[80,512]{1,0:T(8,128)(2,1)S(1)}, u32[]{:S(2)}) copy-start(bf16[80,512]{1,0:T(8,128)(2,1)S(1)} %collective-permute-done.7.refs_1_) | copy-start | bytes 245764
  48.8 12.9 %collective-permute-start.15 = (bf16[2,512,128]{2,1,0:T(8,128)(2,1)S(1)}, bf16[2,512,128]{2,1,0:T(8,128)(2,1)}, u32[]{:S(2)}, u32[]{:S(2)}) collective-permute-start(bf16[2,512,128]{2,1,0:T(8,128)(2,1)S(1)} %collective-permute-done.12.refs_5_), channel_id=1, source_target_pairs={{0,224},{1,33},{2,226},{3,35},{4,228},{5,37},{6,230},{7,39},{8,232... | collective-permute-start | bytes 786440 | tf_op jit(solution)/shard_map/ppermute | solution.py:54
  50.9 11.9 %collective-permute-start.17 = (bf16[2,512,128]{2,1,0:T(8,128)(2,1)S(1)}, bf16[2,512,128]{2,1,0:T(8,128)(2,1)S(1)}, u32[]{:S(2)}, u32[]{:S(2)}) collective-permute-start(bf16[2,512,128]{2,1,0:T(8,128)(2,1)S(1)} %collective-permute-done.11.refs_3_), channel_id=1, source_target_pairs={{0,1},{1,0},{2,3},{3,2},{4,5},{5,4},{6,7},{7,6},{8,9},{9,8},{10,11... | collective-permute-start | bytes 786440 | tf_op jit(solution)/shard_map/ppermute | solution.py:54
  50.9 5.1 %copy-start.19 = (bf16[2,512,128]{2,1,0:T(8,128)(2,1)}, bf16[2,512,128]{2,1,0:T(8,128)(2,1)S(1)}, u32[]{:S(2)}) copy-start(bf16[2,512,128]{2,1,0:T(8,128)(2,1)S(1)} %collective-permute-done.13.refs_4_) | copy-start | bytes 786436
  50.9 11.9 %collective-permute-start.16 = (bf16[2,512,128]{2,1,0:T(8,128)(2,1)S(1)}, bf16[2,512,128]{2,1,0:T(8,128)(2,1)S(1)}, u32[]{:S(2)}, u32[]{:S(2)}) collective-permute-start(bf16[2,512,128]{2,1,0:T(8,128)(2,1)S(1)} %collective-permute-done.12.refs_5_), channel_id=1, source_target_pairs={{0,1},{1,0},{2,3},{3,2},{4,5},{5,4},{6,7},{7,6},{8,9},{9,8},{10,11... | collective-permute-start | bytes 786440 | tf_op jit(solution)/shard_map/ppermute | solution.py:54
  51.5 26.6 %copy-start.1 = (bf16[128,2048]{1,0:T(8,128)(2,1)}, bf16[128,2048]{1,0:T(8,128)(2,1)S(1)}, u32[]{:S(2)}) copy-start(bf16[128,2048]{1,0:T(8,128)(2,1)S(1)} %collective-permute-done.25.refs_1_) | copy-start | bytes 1572868
  51.6 25.3 %collective-permute-start.26 = (bf16[128,2048]{1,0:T(8,128)(2,1)S(1)}, bf16[128,2048]{1,0:T(8,128)(2,1)S(1)}, u32[]{:S(2)}, u32[]{:S(2)}) collective-permute-start(bf16[128,2048]{1,0:T(8,128)(2,1)S(1)} %copy-done), channel_id=1, source_target_pairs={{0,6},{1,3},{2,0},{3,5},{4,2},{5,7},{6,4},{7,1},{8,14},{9,11},{10,... | collective-permute-start | bytes 1572872 | tf_op jit(solution)/shard_map/ppermute | solution.py:54
  61.6 14.7 %copy-start.14 = (bf16[2,512,128]{2,1,0:T(8,128)(2,1)}, bf16[2,512,128]{2,1,0:T(8,128)(2,1)S(1)}, u32[]{:S(2)}) copy-start(bf16[2,512,128]{2,1,0:T(8,128)(2,1)S(1)} %collective-permute-done.14.refs_3_) | copy-start | bytes 786436
  61.6 15.3 %collective-permute-start.27 = (bf16[128,2048]{1,0:T(8,128)(2,1)S(1)}, bf16[128,2048]{1,0:T(8,128)(2,1)S(1)}, u32[]{:S(2)}, u32[]{:S(2)}) collective-permute-start(bf16[128,2048]{1,0:T(8,128)(2,1)S(1)} %collective-permute-done.25.refs_1_), channel_id=1, source_target_pairs={{0,2},{1,7},{2,4},{3,1},{4,6},{5,3},{6,0},{7,5},{8,10},{9,15},{10,... | collective-permute-start | bytes 1572872 | tf_op jit(solution)/shard_map/ppermute | solution.py:54
  61.7 16.2 %collective-permute-start.21 = (bf16[2,512,128]{2,1,0:T(8,128)(2,1)S(1)}, bf16[2,512,128]{2,1,0:T(8,128)(2,1)}, u32[]{:S(2)}, u32[]{:S(2)}) collective-permute-start(bf16[2,512,128]{2,1,0:T(8,128)(2,1)S(1)} %collective-permute-done.14.refs_3_), channel_id=1, source_target_pairs={{0,1},{1,0},{2,3},{3,2},{4,5},{5,4},{6,7},{7,6},{8,9},{9,8},{10,11... | collective-permute-start | bytes 786440 | tf_op jit(solution)/shard_map/ppermute | solution.py:54
  62.8 13.4 %collective-permute-start.18 = (bf16[2,512,128]{2,1,0:T(8,128)(2,1)S(1)}, bf16[2,512,128]{2,1,0:T(8,128)(2,1)}, u32[]{:S(2)}, u32[]{:S(2)}) collective-permute-start(bf16[2,512,128]{2,1,0:T(8,128)(2,1)S(1)} %collective-permute-done.14.refs_3_), channel_id=1, source_target_pairs={{0,32},{1,225},{2,34},{3,227},{4,36},{5,229},{6,38},{7,231},{8,40}... | collective-permute-start | bytes 786440 | tf_op jit(solution)/shard_map/ppermute | solution.py:54
  62.8 13.9 %collective-permute-start.19 = (bf16[2,512,128]{2,1,0:T(8,128)(2,1)}, bf16[2,512,128]{2,1,0:T(8,128)(2,1)}, u32[]{:S(2)}, u32[]{:S(2)}) collective-permute-start(bf16[2,512,128]{2,1,0:T(8,128)(2,1)} %collective-permute-done.15.refs_5_), channel_id=1, source_target_pairs={{0,224},{1,33},{2,226},{3,35},{4,228},{5,37},{6,230},{7,39},{8,232... | collective-permute-start | bytes 786440 | tf_op jit(solution)/shard_map/ppermute | solution.py:54
  76.3 1.9 %collective-permute-start.20 = (bf16[2,512,128]{2,1,0:T(8,128)(2,1)}, bf16[2,512,128]{2,1,0:T(8,128)(2,1)S(1)}, u32[]{:S(2)}, u32[]{:S(2)}) collective-permute-start(bf16[2,512,128]{2,1,0:T(8,128)(2,1)} %collective-permute-done.15.refs_5_), channel_id=1, source_target_pairs={{0,1},{1,0},{2,3},{3,2},{4,5},{5,4},{6,7},{7,6},{8,9},{9,8},{10,11... | collective-permute-start | bytes 786440 | tf_op jit(solution)/shard_map/ppermute | solution.py:54
  76.8 2.0 %collective-permute-start.23 = (bf16[2,512,128]{2,1,0:T(8,128)(2,1)}, bf16[2,512,128]{2,1,0:T(8,128)(2,1)S(1)}, u32[]{:S(2)}, u32[]{:S(2)}) collective-permute-start(bf16[2,512,128]{2,1,0:T(8,128)(2,1)} %collective-permute-done.19.refs_5_), channel_id=1, source_target_pairs={{0,1},{1,0},{2,3},{3,2},{4,5},{5,4},{6,7},{7,6},{8,9},{9,8},{10,11... | collective-permute-start | bytes 786440 | tf_op jit(solution)/shard_map/ppermute | solution.py:54
  76.9 11.7 %copy-start.2 = (bf16[128,2048]{1,0:T(8,128)(2,1)}, bf16[128,2048]{1,0:T(8,128)(2,1)S(1)}, u32[]{:S(2)}) copy-start(bf16[128,2048]{1,0:T(8,128)(2,1)S(1)} %collective-permute-done.26.refs_2_) | copy-start | bytes 1572868
  76.9 6.7 %collective-permute-start.22 = (bf16[2,512,128]{2,1,0:T(8,128)(2,1)}, bf16[2,512,128]{2,1,0:T(8,128)(2,1)}, u32[]{:S(2)}, u32[]{:S(2)}) collective-permute-start(bf16[2,512,128]{2,1,0:T(8,128)(2,1)} %collective-permute-done.18.refs_3_), channel_id=1, source_target_pairs={{0,32},{1,225},{2,34},{3,227},{4,36},{5,229},{6,38},{7,231},{8,40}... | collective-permute-start | bytes 786440 | tf_op jit(solution)/shard_map/ppermute | solution.py:54
  76.9 11.7 %copy-start.3 = (bf16[128,2048]{1,0:T(8,128)(2,1)}, bf16[128,2048]{1,0:T(8,128)(2,1)S(1)}, u32[]{:S(2)}) copy-start(bf16[128,2048]{1,0:T(8,128)(2,1)S(1)} %collective-permute-done.27.refs_3_) | copy-start | bytes 1572868
  76.9 20.9 %collective-permute-start.28 = (bf16[128,2048]{1,0:T(8,128)(2,1)S(1)}, bf16[128,2048]{1,0:T(8,128)(2,1)S(1)}, u32[]{:S(2)}, u32[]{:S(2)}) collective-permute-start(bf16[128,2048]{1,0:T(8,128)(2,1)S(1)} %copy-done), channel_id=1, source_target_pairs={{0,1},{1,0},{2,3},{3,2},{4,5},{5,4},{6,7},{7,6},{8,9},{9,8},{10,11... | collective-permute-start | bytes 1572872 | tf_op jit(solution)/shard_map/ppermute | solution.py:54
  77.9 19.9 %collective-permute-start.30 = (bf16[128,2048]{1,0:T(8,128)(2,1)S(1)}, bf16[128,2048]{1,0:T(8,128)(2,1)S(1)}, u32[]{:S(2)}, u32[]{:S(2)}) collective-permute-start(bf16[128,2048]{1,0:T(8,128)(2,1)S(1)} %collective-permute-done.26.refs_2_), channel_id=1, source_target_pairs={{0,1},{1,0},{2,3},{3,2},{4,5},{5,4},{6,7},{7,6},{8,9},{9,8},{10,11... | collective-permute-start | bytes 1572872 | tf_op jit(solution)/shard_map/ppermute | solution.py:54
  78.1 5.4 %copy-start.18 = (bf16[2,512,128]{2,1,0:T(8,128)(2,1)}, bf16[2,512,128]{2,1,0:T(8,128)(2,1)S(1)}, u32[]{:S(2)}) copy-start(bf16[2,512,128]{2,1,0:T(8,128)(2,1)S(1)} %collective-permute-done.20.refs_4_) | copy-start | bytes 786436
  78.1 19.7 %collective-permute-start.29 = (bf16[128,2048]{1,0:T(8,128)(2,1)S(1)}, bf16[128,2048]{1,0:T(8,128)(2,1)}, u32[]{:S(2)}, u32[]{:S(2)}) collective-permute-start(bf16[128,2048]{1,0:T(8,128)(2,1)S(1)} %collective-permute-done.25.refs_1_), channel_id=1, source_target_pairs={{0,1},{1,0},{2,3},{3,2},{4,5},{5,4},{6,7},{7,6},{8,9},{9,8},{10,11... | collective-permute-start | bytes 1572872 | tf_op jit(solution)/shard_map/ppermute | solution.py:54
  78.7 9.9 %collective-permute-start.24 = (bf16[2,512,128]{2,1,0:T(8,128)(2,1)}, bf16[2,512,128]{2,1,0:T(8,128)(2,1)S(1)}, u32[]{:S(2)}, u32[]{:S(2)}) collective-permute-start(bf16[2,512,128]{2,1,0:T(8,128)(2,1)} %collective-permute-done.18.refs_3_), channel_id=1, source_target_pairs={{0,1},{1,0},{2,3},{3,2},{4,5},{5,4},{6,7},{7,6},{8,9},{9,8},{10,11... | collective-permute-start | bytes 786440 | tf_op jit(solution)/shard_map/ppermute | solution.py:54
  83.6 14.2 %collective-permute-start.31 = (bf16[128,2048]{1,0:T(8,128)(2,1)S(1)}, bf16[128,2048]{1,0:T(8,128)(2,1)}, u32[]{:S(2)}, u32[]{:S(2)}) collective-permute-start(bf16[128,2048]{1,0:T(8,128)(2,1)S(1)} %collective-permute-done.27.refs_3_), channel_id=1, source_target_pairs={{0,1},{1,0},{2,3},{3,2},{4,5},{5,4},{6,7},{7,6},{8,9},{9,8},{10,11... | collective-permute-start | bytes 1572872 | tf_op jit(solution)/shard_map/ppermute | solution.py:54
  88.6 9.2 %collective-permute-start.32 = (bf16[2,512,128]{2,1,0:T(8,128)(2,1)}, bf16[2,512,128]{2,1,0:T(8,128)(2,1)}, u32[]{:S(2)}, u32[]{:S(2)}) collective-permute-start(bf16[2,512,128]{2,1,0:T(8,128)(2,1)} %collective-permute-done.22.refs_3_), channel_id=1, source_target_pairs={{0,1},{1,0},{2,3},{3,2},{4,5},{5,4},{6,7},{7,6},{8,9},{9,8},{10,11... | collective-permute-start | bytes 786440 | tf_op jit(solution)/shard_map/ppermute | solution.py:54
  105.3 15.9 %collective-permute-start.33 = (bf16[64,512]{1,0:T(8,128)(2,1)}, bf16[64,512]{1,0:T(8,128)(2,1)S(1)}, u32[]{:S(2)}, u32[]{:S(2)}) collective-permute-start(bf16[64,512]{1,0:T(8,128)(2,1)} %get-tuple-element.89), channel_id=1, source_target_pairs={{0,0},{16,1},{2,2},{18,3},{4,4},{20,5},{6,6},{22,7},{1,8},{17,9},{... | collective-permute-start | bytes 196616 | tf_op jit(solution)/shard_map/ppermute | solution.py:54
  117.4 9.7 %collective-permute-start.34 = (bf16[64,512]{1,0:T(8,128)(2,1)}, bf16[64,512]{1,0:T(8,128)(2,1)S(1)}, u32[]{:S(2)}, u32[]{:S(2)}) collective-permute-start(bf16[64,512]{1,0:T(8,128)(2,1)} %get-tuple-element.90), channel_id=1, source_target_pairs={{8,0},{24,1},{10,2},{26,3},{12,4},{28,5},{14,6},{30,7},{9,8},{25,9... | collective-permute-start | bytes 196616 | tf_op jit(solution)/shard_map/ppermute | solution.py:54
  (12 other events, 25.1 us)

commit v3 on v2

--- a/solution.py
+++ b/solution.py
@@ -349,7 +349,6 @@
     steps = [(own,), (send(own, Z_FIRST), send(own, Z_SECOND))]
     theirs = [(send(own, OTHER_CORE),)]
     parts = []
-    w_mine = across_x(after(w_out, own))
     w_pieces = []
     for n in range(len(fars)):
         if n + 1 < len(fars):
@@ -364,7 +363,9 @@
             q0, q1, *w_pieces = lax.optimization_barrier((q0, q1, *w_pieces))
         kvs = [a for pair in zip(steps[n], theirs[n]) for a in pair]
         parts.append(attend(fars[n], pos, q0, q1, kvs))
-        if n == 1:
+        if n == 0:
+            w_mine = across_x(after(w_out, parts[0]))
+        if n == 2:
             w_pieces = from_all_tp([after(w, parts[n]) for w in w_mine])
     att0, att1 = merge(fars, pos, parts)
     att0, att1 = send(att0, Q_BACK[0]), send(att1, Q_BACK[1])

time: 141 us -> 150 us (1.064)
  the two profiles are of different devices: /device:TPU:56 before, /device:TPU:32 now
where the time goes in v3:
time: 150 us
  Pallas kernels  45 us (30%)
  waiting for transfers between devices  42.3 us (28%)
  starting transfers between devices  42 us (28%)
  blocking collectives  15.8 us (11%)
  local copies, waits for them, and re-layouts  3.62 us (2%)
    ppermute x35, waiting for transfers between devices, send(): return lax.ppermute(a, AXES, move)  42.3 us
    ppermute x35, starting transfers between devices, send(): return lax.ppermute(a, AXES, move)  42 us
    pallas_call x5, Pallas kernels, attend(): pl.pallas_call(body, out_shape=(jax.ShapeDtypeStruct((count, 2, HEAD, TOK...  34 us
    all_to_all x1, blocking collectives, shards(): lax.all_to_all(att.reshape(X * C, ROWS, 2 * HEAD), 'tp', 0, 0, tiled=True)  15.8 us
    pallas_call x1, Pallas kernels, project(): pl.pallas_call(project_body, out_shape=(jax.ShapeDtypeStruct((QROWS, TOK)...  4.88 us
    pallas_call x1, Pallas kernels, output(): pl.pallas_call(output_body, out_shape=jax.ShapeDtypeStruct((ROWS, 2048),...  3.6 us
    unnamed x56, local copies, waits for them, and re-layouts  3.5 us
  transfers between devices with their start and end apart: 35, of which 11 were waited for; matrix products, arithmetic and copies ran while one was open for 0% of the time, Pallas kernels for 16%

profile of v3, /device:TPU:32, one launch (start us, length us, event | category | flops | bytes accessed | tf_op | source)
XLA Modules:
  0.0 149.7 jit_solution(4301620175159026125)
XLA Ops:
  0.0 1.5 collective-permute-start
  1.5 1.7 %collective-permute-start.1 = (bf16[64,2048]{1,0:T(8,128)(2,1)}, bf16[64,2048]{1,0:T(8,128)(2,1)S(1)}, u32[]{:S(2)}, u32[]{:S(2)}) collective-permute-start(bf16[64,2048]{1,0:T(8,128)(2,1)} %refs_0_.1), channel_id=1, source_target_pairs={{0,6},{1,3},{2,0},{3,5},{4,2},{5,7},{6,4},{7,1},{8,14},{9,11},{10,... | collective-permute-start | bytes 786440 | tf_op jit(solution)/shard_map/ppermute | solution.py:54
  3.2 0.7 pad_add_fusion.pos.refs_0_
  3.9 5.4 %collective-permute-done.refs_1_ = bf16[64,2048]{1,0:T(8,128)(2,1)S(1)} collective-permute-done((bf16[64,2048]{1,0:T(8,128)(2,1)}, bf16[64,2048]{1,0:T(8,128)(2,1)S(1)}, u32[]{:S(2)}, u32[]{:S(2)}) %collective-permute-start) | collective-permute-done | bytes 262176 | tf_op jit(solution)/shard_map/ppermute | solution.py:54
  9.3 1.5 collective-permute-start.2
  10.7 0.5 collective-permute-start.4
  11.3 5.5 %collective-permute-done.2.refs_3_ = bf16[64,2048]{1,0:T(8,128)(2,1)S(1)} collective-permute-done((bf16[64,2048]{1,0:T(8,128)(2,1)S(1)}, bf16[64,2048]{1,0:T(8,128)(2,1)S(1)}, u32[]{:S(2)}, u32[]{:S(2)}) %collective-permute-start.2) | collective-permute-done | bytes 262176 | tf_op jit(solution)/shard_map/ppermute | solution.py:54
  16.9 1.5 collective-permute-done.6.refs_7_
  18.4 0.7 copy-done.13
  19.1 4.9 %project.1 = (bf16[80,512]{1,0:T(8,128)(2,1)}, bf16[80,512]{1,0:T(8,128)(2,1)}, bf16[512,128]{1,0:T(8,128)(2,1)}, bf16[512,128]{1,0:T(8,128)(2,1)}) custom-call(s32[2]{0:T(128)} %pad_add_fusion.pos.refs_0_, f32[2]{0:T(128)} %bias.1, bf16[64,2048]{1,0:T(8,128)(2,1)} %refs_0_.1, bf16[64,2048]{1,0:T(8,128)(2,1)} %copy-done.7, bf16[64,2048]{1,0:T(8,128)(2,1)} %copy-done.8, ...), custom_call_target="tpu_custom_call" | custom-call | flops 67108864 | bytes 4194304 | tf_op jit(solution)/shard_map/project/pallas_call | solution.py:119
  24.0 1.6 %collective-permute-start.9 = (bf16[512,128]{1,0:T(8,128)(2,1)}, bf16[512,128]{1,0:T(8,128)(2,1)S(1)}, u32[]{:S(2)}, u32[]{:S(2)}) collective-permute-start(bf16[512,128]{1,0:T(8,128)(2,1)} %get-tuple-element.55), channel_id=1, source_target_pairs={{0,0},{1,16},{2,2},{3,18},{4,4},{5,20},{6,6},{7,22},{8,1},{9,17},{... | collective-permute-start | bytes 393224 | tf_op jit(solution)/shard_map/ppermute | solution.py:54
  25.6 2.2 %collective-permute-start.10 = (bf16[512,128]{1,0:T(8,128)(2,1)}, bf16[512,128]{1,0:T(8,128)(2,1)S(1)}, u32[]{:S(2)}, u32[]{:S(2)}) collective-permute-start(bf16[512,128]{1,0:T(8,128)(2,1)} %get-tuple-element.56), channel_id=1, source_target_pairs={{0,8},{1,24},{2,10},{3,26},{4,12},{5,28},{6,14},{7,30},{8,9},{9,25... | collective-permute-start | bytes 393224 | tf_op jit(solution)/shard_map/ppermute | solution.py:54
  27.8 6.3 %collective-permute-done.10 = bf16[512,128]{1,0:T(8,128)(2,1)S(1)} collective-permute-done((bf16[512,128]{1,0:T(8,128)(2,1)}, bf16[512,128]{1,0:T(8,128)(2,1)S(1)}, u32[]{:S(2)}, u32[]{:S(2)}) %collective-permute-start.10) | collective-permute-done | bytes 131104 | tf_op jit(solution)/shard_map/ppermute | solution.py:54
  34.1 1.2 collective-permute-start.12
  35.3 0.9 collective-permute-start.11
  36.2 0.8 collective-permute-start.13
  37.0 0.7 collective-permute-start.7
  37.6 3.2 %collective-permute-start.8 = (bf16[80,512]{1,0:T(8,128)(2,1)S(1)}, bf16[80,512]{1,0:T(8,128)(2,1)S(1)}, u32[]{:S(2)}, u32[]{:S(2)}) collective-permute-start(bf16[80,512]{1,0:T(8,128)(2,1)S(1)} %copy-done.26), channel_id=1, source_target_pairs={{0,8},{1,24},{2,10},{3,26},{4,12},{5,28},{6,14},{7,30},{8,9},{9,25... | collective-permute-start | bytes 245768 | tf_op jit(solution)/shard_map/ppermute | solution.py:54
  40.8 0.6 collective-permute-done.12.refs_5_
  41.4 3.1 %collective-permute-done.11.refs_3_ = bf16[2,512,128]{2,1,0:T(8,128)(2,1)S(1)} collective-permute-done((bf16[2,512,128]{2,1,0:T(8,128)(2,1)S(1)}, bf16[2,512,128]{2,1,0:T(8,128)(2,1)S(1)}, u32[]{:S(2)}, u32[]{:S(2)}) %collective-permute-start.11) | collective-permute-done | bytes 262176 | tf_op jit(solution)/shard_map/ppermute | solution.py:54
  44.5 6.7 %collective-permute-done.8.refs_2_ = bf16[80,512]{1,0:T(8,128)(2,1)S(1)} collective-permute-done((bf16[80,512]{1,0:T(8,128)(2,1)S(1)}, bf16[80,512]{1,0:T(8,128)(2,1)S(1)}, u32[]{:S(2)}, u32[]{:S(2)}) %collective-permute-start.8) | collective-permute-done | bytes 81952 | tf_op jit(solution)/shard_map/ppermute | solution.py:54
  51.2 0.6 copy-done.25
  51.8 0.7 copy-done.22
  52.5 5.5 %shard_map.64 = (f32[1,2,64,512]{3,2,1,0:T(8,128)}, f32[1,2,8,512]{3,2,1,0:T(8,128)}) custom-call(s32[2]{0:T(128)} %pad_add_fusion.pos.refs_0_, bf16[80,512]{1,0:T(8,128)(2,1)} %copy-done.24, bf16[80,512]{1,0:T(8,128)(2,1)} %copy-done.25, bf16[2,512,128]{2,1,0:T(8,128)(2,1)} %copy-done.6, bf16[2,512,128]{2,1,0:T(8,128)(2,1)} %copy-done.22), custom_call_target="tpu_custom_call" | custom-call | flops 2147483648 | bytes 1048576 | tf_op jit(solution)/shard_map/pallas_call | solution.py:260
  58.2 0.7 collective-permute-start.14
  58.9 5.0 %collective-permute-start.15 = (bf16[2,512,128]{2,1,0:T(8,128)(2,1)S(1)}, bf16[2,512,128]{2,1,0:T(8,128)(2,1)S(1)}, u32[]{:S(2)}, u32[]{:S(2)}) collective-permute-start(bf16[2,512,128]{2,1,0:T(8,128)(2,1)S(1)} %collective-permute-done.12.refs_5_), channel_id=1, source_target_pairs={{0,224},{1,33},{2,226},{3,35},{4,228},{5,37},{6,230},{7,39},{8,232... | collective-permute-start | bytes 786440 | tf_op jit(solution)/shard_map/ppermute | solution.py:54
  63.9 0.5 collective-permute-start.17
  64.5 5.0 %collective-permute-done.14.refs_3_ = bf16[2,512,128]{2,1,0:T(8,128)(2,1)S(1)} collective-permute-done((bf16[2,512,128]{2,1,0:T(8,128)(2,1)S(1)}, bf16[2,512,128]{2,1,0:T(8,128)(2,1)S(1)}, u32[]{:S(2)}, u32[]{:S(2)}) %collective-permute-start.14) | collective-permute-done | bytes 262176 | tf_op jit(solution)/shard_map/ppermute | solution.py:54
  69.5 0.9 collective-permute-done.15.refs_5_
  70.5 0.6 collective-permute-start.18
  71.0 2.4 %collective-permute-start.26 = (bf16[128,2048]{1,0:T(8,128)(2,1)S(1)}, bf16[128,2048]{1,0:T(8,128)(2,1)S(1)}, u32[]{:S(2)}, u32[]{:S(2)}) collective-permute-start(bf16[128,2048]{1,0:T(8,128)(2,1)S(1)} %copy-done), channel_id=1, source_target_pairs={{0,6},{1,3},{2,0},{3,5},{4,2},{5,7},{6,4},{7,1},{8,14},{9,11},{10,... | collective-permute-start | bytes 1572872 | tf_op jit(solution)/shard_map/ppermute | solution.py:54
  73.4 1.3 collective-permute-start.21
  74.7 1.3 collective-permute-start.19
  76.1 3.3 %collective-permute-done.18.refs_3_ = bf16[2,512,128]{2,1,0:T(8,128)(2,1)S(1)} collective-permute-done((bf16[2,512,128]{2,1,0:T(8,128)(2,1)S(1)}, bf16[2,512,128]{2,1,0:T(8,128)(2,1)S(1)}, u32[]{:S(2)}, u32[]{:S(2)}) %collective-permute-start.18) | collective-permute-done | bytes 262176 | tf_op jit(solution)/shard_map/ppermute | solution.py:54
  79.4 1.5 collective-permute-start.27
  80.9 10.4 %shard_map.65 = (f32[2,2,64,512]{3,2,1,0:T(8,128)}, f32[2,2,8,512]{3,2,1,0:T(8,128)}) custom-call(s32[2]{0:T(128)} %pad_add_fusion.pos.refs_0_, bf16[80,512]{1,0:T(8,128)(2,1)} %copy-done.24, bf16[80,512]{1,0:T(8,128)(2,1)} %copy-done.25, bf16[2,512,128]{2,1,0:T(8,128)(2,1)} %copy-done.16, bf16[2,512,128]{2,1,0:T(8,128)(2,1)} %copy-done.21, ...), custom_call_target="tpu_custom_call" | custom-call | flops 4294967296 | bytes 1048576 | tf_op jit(solution)/shard_map/pallas_call | solution.py:260
  92.0 0.6 copy-done.20
  92.6 5.0 %shard_map.66 = (f32[2,2,64,512]{3,2,1,0:T(8,128)}, f32[2,2,8,512]{3,2,1,0:T(8,128)}) custom-call(s32[2]{0:T(128)} %pad_add_fusion.pos.refs_0_, bf16[80,512]{1,0:T(8,128)(2,1)} %copy-done.24, bf16[80,512]{1,0:T(8,128)(2,1)} %copy-done.25, bf16[2,512,128]{2,1,0:T(8,128)(2,1)} %copy-done.17, bf16[2,512,128]{2,1,0:T(8,128)(2,1)} %copy-done.20, ...), custom_call_target="tpu_custom_call" | custom-call | flops 4294967296 | bytes 1048576 | tf_op jit(solution)/shard_map/pallas_call | solution.py:260
  97.6 1.2 collective-permute-start.28
  99.8 8.4 %shard_map.67 = (f32[2,2,64,512]{3,2,1,0:T(8,128)}, f32[2,2,8,512]{3,2,1,0:T(8,128)}) custom-call(s32[2]{0:T(128)} %pad_add_fusion.pos.refs_0_, bf16[80,512]{1,0:T(8,128)(2,1)} %copy-done.24, bf16[80,512]{1,0:T(8,128)(2,1)} %copy-done.25, bf16[2,512,128]{2,1,0:T(8,128)(2,1)} %copy-done.14, bf16[2,512,128]{2,1,0:T(8,128)(2,1)} %collective-permute-done.23.refs_4_, ...), custom_call_target="tpu_custom_call" | custom-call | flops 4294967296 | bytes 1048576 | tf_op jit(solution)/shard_map/pallas_call | solution.py:260
  108.4 0.8 copy-done.23
  109.1 4.7 %shard_map.68 = (f32[1,2,64,512]{3,2,1,0:T(8,128)}, f32[1,2,8,512]{3,2,1,0:T(8,128)}) custom-call(s32[2]{0:T(128)} %pad_add_fusion.pos.refs_0_, bf16[80,512]{1,0:T(8,128)(2,1)} %copy-done.24, bf16[80,512]{1,0:T(8,128)(2,1)} %copy-done.25, bf16[2,512,128]{2,1,0:T(8,128)(2,1)} %collective-permute-done.22.refs_3_, bf16[2,512,128]{2,1,0:T(8,128)(2,1)} %copy-done.23), custom_call_target="tpu_custom_call" | custom-call | flops 2147483648 | bytes 1048576 | tf_op jit(solution)/shard_map/pallas_call | solution.py:260
  113.8 2.5 %merge.1 = (bf16[64,512]{1,0:T(8,128)(2,1)}, bf16[64,512]{1,0:T(8,128)(2,1)}) custom-call(s32[2]{0:T(128)} %pad_add_fusion.pos.refs_0_, f32[1,2,64,512]{3,2,1,0:T(8,128)} %get-tuple-element.61.refs_1_, f32[2,2,64,512]{3,2,1,0:T(8,128)} %get-tuple-element.67.refs_2_, f32[2,2,64,512]{3,2,1,0:T(8,128)} %get-tuple-element.73.refs_3_, ...), custom_call_target="tpu_custom_call" | custom-call | tf_op jit(solution)/shard_map/merge/pallas_call | solution.py:298
  116.3 1.5 collective-permute-start.33
  117.8 8.3 %collective-permute-start.34 = (bf16[64,512]{1,0:T(8,128)(2,1)}, bf16[64,512]{1,0:T(8,128)(2,1)S(1)}, u32[]{:S(2)}, u32[]{:S(2)}) collective-permute-start(bf16[64,512]{1,0:T(8,128)(2,1)} %get-tuple-element.90), channel_id=1, source_target_pairs={{8,0},{24,1},{10,2},{26,3},{12,4},{28,5},{14,6},{30,7},{9,8},{25,9... | collective-permute-start | bytes 196616 | tf_op jit(solution)/shard_map/ppermute | solution.py:54
  126.1 4.0 %collective-permute-done.34 = bf16[64,512]{1,0:T(8,128)(2,1)S(1)} collective-permute-done((bf16[64,512]{1,0:T(8,128)(2,1)}, bf16[64,512]{1,0:T(8,128)(2,1)S(1)}, u32[]{:S(2)}, u32[]{:S(2)}) %collective-permute-start.34) | collective-permute-done | bytes 65568 | tf_op jit(solution)/shard_map/ppermute | solution.py:54
  130.3 15.8 %all_to_all.5.att = bf16[8,64,128]{2,1,0:T(8,128)(2,1)} all-to-all(bf16[8,64,128]{2,1,0:T(8,128)(2,1)S(1)} %bitcast.7), channel_id=1, replica_groups=mesh['sp'=32,'tp'=8] {'tp'}, dimensions={0} | all-to-all | bytes 262144 | tf_op jit(solution)/shard_map/all_to_all | solution.py:373
  146.1 3.6 %output.1 = bf16[64,2048]{1,0:T(8,128)(2,1)} custom-call(s32[2]{0:T(128)} %pad_add_fusion.pos.refs_0_, bf16[8,64,128]{2,1,0:T(8,128)(2,1)} %all_to_all.5.att, bf16[128,2048]{1,0:T(8,128)(2,1)} %refs_0_.2, bf16[128,2048]{1,0:T(8,128)(2,1)} %copy-done.1, bf16[128,2048]{1,0:T(8,128)(2,1)} %copy-done.2, bf16[128,2048]{1,0:T(8,128)(2,1)} %copy-done.3, ...), custom_call_target="tpu_custom_call" | custom-call | tf_op jit(solution)/shard_map/output/pallas_call | solution.py:317
  (91 shorter events, 2.6 us)
Async XLA Ops:
  0.0 9.3 %collective-permute-start = (bf16[64,2048]{1,0:T(8,128)(2,1)}, bf16[64,2048]{1,0:T(8,128)(2,1)S(1)}, u32[]{:S(2)}, u32[]{:S(2)}) collective-permute-start(bf16[64,2048]{1,0:T(8,128)(2,1)} %refs_0_.1), channel_id=1, source_target_pairs={{0,2},{1,7},{2,4},{3,1},{4,6},{5,3},{6,0},{7,5},{8,10},{9,15},{10,... | collective-permute-start | bytes 786440 | tf_op jit(solution)/shard_map/ppermute | solution.py:54
  1.5 9.7 %collective-permute-start.1 = (bf16[64,2048]{1,0:T(8,128)(2,1)}, bf16[64,2048]{1,0:T(8,128)(2,1)S(1)}, u32[]{:S(2)}, u32[]{:S(2)}) collective-permute-start(bf16[64,2048]{1,0:T(8,128)(2,1)} %refs_0_.1), channel_id=1, source_target_pairs={{0,6},{1,3},{2,0},{3,5},{4,2},{5,7},{6,4},{7,1},{8,14},{9,11},{10,... | collective-permute-start | bytes 786440 | tf_op jit(solution)/shard_map/ppermute | solution.py:54
  9.3 9.1 %copy-start.7 = (bf16[64,2048]{1,0:T(8,128)(2,1)}, bf16[64,2048]{1,0:T(8,128)(2,1)S(1)}, u32[]{:S(2)}) copy-start(bf16[64,2048]{1,0:T(8,128)(2,1)S(1)} %collective-permute-done.refs_1_) | copy-start | bytes 786436
  9.3 7.6 %collective-permute-start.2 = (bf16[64,2048]{1,0:T(8,128)(2,1)S(1)}, bf16[64,2048]{1,0:T(8,128)(2,1)S(1)}, u32[]{:S(2)}, u32[]{:S(2)}) collective-permute-start(bf16[64,2048]{1,0:T(8,128)(2,1)S(1)} %collective-permute-done.refs_1_), channel_id=1, source_target_pairs={{0,2},{1,7},{2,4},{3,1},{4,6},{5,3},{6,0},{7,5},{8,10},{9,15},{10,... | collective-permute-start | bytes 786440 | tf_op jit(solution)/shard_map/ppermute | solution.py:54
  10.7 6.1 %collective-permute-start.3 = (bf16[64,2048]{1,0:T(8,128)(2,1)}, bf16[64,2048]{1,0:T(8,128)(2,1)S(1)}, u32[]{:S(2)}, u32[]{:S(2)}) collective-permute-start(bf16[64,2048]{1,0:T(8,128)(2,1)} %refs_0_.1), channel_id=1, source_target_pairs={{0,1},{1,0},{2,3},{3,2},{4,5},{5,4},{6,7},{7,6},{8,9},{9,8},{10,11... | collective-permute-start | bytes 786440 | tf_op jit(solution)/shard_map/ppermute | solution.py:54
  10.7 6.2 %collective-permute-start.4 = (bf16[64,2048]{1,0:T(8,128)(2,1)S(1)}, bf16[64,2048]{1,0:T(8,128)(2,1)S(1)}, u32[]{:S(2)}, u32[]{:S(2)}) collective-permute-start(bf16[64,2048]{1,0:T(8,128)(2,1)S(1)} %collective-permute-done.refs_1_), channel_id=1, source_target_pairs={{0,1},{1,0},{2,3},{3,2},{4,5},{5,4},{6,7},{7,6},{8,9},{9,8},{10,11... | collective-permute-start | bytes 786440 | tf_op jit(solution)/shard_map/ppermute | solution.py:54
  11.2 7.2 %copy-start.8 = (bf16[64,2048]{1,0:T(8,128)(2,1)}, bf16[64,2048]{1,0:T(8,128)(2,1)S(1)}, u32[]{:S(2)}) copy-start(bf16[64,2048]{1,0:T(8,128)(2,1)S(1)} %collective-permute-done.1.refs_2_) | copy-start | bytes 786436
  11.2 5.6 %collective-permute-start.5 = (bf16[64,2048]{1,0:T(8,128)(2,1)S(1)}, bf16[64,2048]{1,0:T(8,128)(2,1)S(1)}, u32[]{:S(2)}, u32[]{:S(2)}) collective-permute-start(bf16[64,2048]{1,0:T(8,128)(2,1)S(1)} %collective-permute-done.1.refs_2_), channel_id=1, source_target_pairs={{0,1},{1,0},{2,3},{3,2},{4,5},{5,4},{6,7},{7,6},{8,9},{9,8},{10,11... | collective-permute-start | bytes 786440 | tf_op jit(solution)/shard_map/ppermute | solution.py:54
  16.8 1.5 %collective-permute-start.6 = (bf16[64,2048]{1,0:T(8,128)(2,1)S(1)}, bf16[64,2048]{1,0:T(8,128)(2,1)S(1)}, u32[]{:S(2)}, u32[]{:S(2)}) collective-permute-start(bf16[64,2048]{1,0:T(8,128)(2,1)S(1)} %collective-permute-done.2.refs_3_), channel_id=1, source_target_pairs={{0,1},{1,0},{2,3},{3,2},{4,5},{5,4},{6,7},{7,6},{8,9},{9,8},{10,11... | collective-permute-start | bytes 786440 | tf_op jit(solution)/shard_map/ppermute | solution.py:54
  24.0 3.7 %collective-permute-start.9 = (bf16[512,128]{1,0:T(8,128)(2,1)}, bf16[512,128]{1,0:T(8,128)(2,1)S(1)}, u32[]{:S(2)}, u32[]{:S(2)}) collective-permute-start(bf16[512,128]{1,0:T(8,128)(2,1)} %get-tuple-element.55), channel_id=1, source_target_pairs={{0,0},{1,16},{2,2},{3,18},{4,4},{5,20},{6,6},{7,22},{8,1},{9,17},{... | collective-permute-start | bytes 393224 | tf_op jit(solution)/shard_map/ppermute | solution.py:54
  25.6 8.5 %collective-permute-start.10 = (bf16[512,128]{1,0:T(8,128)(2,1)}, bf16[512,128]{1,0:T(8,128)(2,1)S(1)}, u32[]{:S(2)}, u32[]{:S(2)}) collective-permute-start(bf16[512,128]{1,0:T(8,128)(2,1)} %get-tuple-element.56), channel_id=1, source_target_pairs={{0,8},{1,24},{2,10},{3,26},{4,12},{5,28},{6,14},{7,30},{8,9},{9,25... | collective-permute-start | bytes 393224 | tf_op jit(solution)/shard_map/ppermute | solution.py:54
  34.1 17.1 %copy-start.6 = (bf16[2,512,128]{2,1,0:T(8,128)(2,1)}, bf16[2,512,128]{2,1,0:T(8,128)(2,1)S(1)}, u32[]{:S(2)}) copy-start(bf16[2,512,128]{2,1,0:T(8,128)(2,1)S(1)} %pad_maximum_fusion.refs_3_) | copy-start | bytes 786436
  34.1 7.3 %collective-permute-start.12 = (bf16[2,512,128]{2,1,0:T(8,128)(2,1)S(1)}, bf16[2,512,128]{2,1,0:T(8,128)(2,1)S(1)}, u32[]{:S(2)}, u32[]{:S(2)}) collective-permute-start(bf16[2,512,128]{2,1,0:T(8,128)(2,1)S(1)} %pad_maximum_fusion.refs_3_), channel_id=1, source_target_pairs={{0,224},{1,33},{2,226},{3,35},{4,228},{5,37},{6,230},{7,39},{8,232... | collective-permute-start | bytes 786440 | tf_op jit(solution)/shard_map/ppermute | solution.py:54
  35.3 9.2 %collective-permute-start.11 = (bf16[2,512,128]{2,1,0:T(8,128)(2,1)S(1)}, bf16[2,512,128]{2,1,0:T(8,128)(2,1)S(1)}, u32[]{:S(2)}, u32[]{:S(2)}) collective-permute-start(bf16[2,512,128]{2,1,0:T(8,128)(2,1)S(1)} %pad_maximum_fusion.refs_3_), channel_id=1, source_target_pairs={{0,32},{1,225},{2,34},{3,227},{4,36},{5,229},{6,38},{7,231},{8,40}... | collective-permute-start | bytes 786440 | tf_op jit(solution)/shard_map/ppermute | solution.py:54
  36.2 15.0 %collective-permute-start.13 = (bf16[2,512,128]{2,1,0:T(8,128)(2,1)S(1)}, bf16[2,512,128]{2,1,0:T(8,128)(2,1)S(1)}, u32[]{:S(2)}, u32[]{:S(2)}) collective-permute-start(bf16[2,512,128]{2,1,0:T(8,128)(2,1)S(1)} %pad_maximum_fusion.refs_3_), channel_id=1, source_target_pairs={{0,1},{1,0},{2,3},{3,2},{4,5},{5,4},{6,7},{7,6},{8,9},{9,8},{10,11... | collective-permute-start | bytes 786440 | tf_op jit(solution)/shard_map/ppermute | solution.py:54
  37.0 7.5 %collective-permute-start.7 = (bf16[80,512]{1,0:T(8,128)(2,1)S(1)}, bf16[80,512]{1,0:T(8,128)(2,1)S(1)}, u32[]{:S(2)}, u32[]{:S(2)}) collective-permute-start(bf16[80,512]{1,0:T(8,128)(2,1)S(1)} %copy-done.27), channel_id=1, source_target_pairs={{0,0},{1,16},{2,2},{3,18},{4,4},{5,20},{6,6},{7,22},{8,1},{9,17},{... | collective-permute-start | bytes 245768 | tf_op jit(solution)/shard_map/ppermute | solution.py:54
  37.6 20.4 %copy-start = (bf16[128,2048]{1,0:T(8,128)(2,1)S(1)}, bf16[128,2048]{1,0:T(8,128)(2,1)}, u32[]{:S(2)}) copy-start(bf16[128,2048]{1,0:T(8,128)(2,1)} %refs_0_.2) | copy-start | bytes 1572868
  37.6 13.5 %collective-permute-start.8 = (bf16[80,512]{1,0:T(8,128)(2,1)S(1)}, bf16[80,512]{1,0:T(8,128)(2,1)S(1)}, u32[]{:S(2)}, u32[]{:S(2)}) collective-permute-start(bf16[80,512]{1,0:T(8,128)(2,1)S(1)} %copy-done.26), channel_id=1, source_target_pairs={{0,8},{1,24},{2,10},{3,26},{4,12},{5,28},{6,14},{7,30},{8,9},{9,25... | collective-permute-start | bytes 245768 | tf_op jit(solution)/shard_map/ppermute | solution.py:54
  41.4 23.1 %copy-start.15 = (bf16[2,512,128]{2,1,0:T(8,128)(2,1)}, bf16[2,512,128]{2,1,0:T(8,128)(2,1)S(1)}, u32[]{:S(2)}) copy-start(bf16[2,512,128]{2,1,0:T(8,128)(2,1)S(1)} %collective-permute-done.12.refs_5_) | copy-start | bytes 786436
  44.5 19.5 %copy-start.16 = (bf16[2,512,128]{2,1,0:T(8,128)(2,1)}, bf16[2,512,128]{2,1,0:T(8,128)(2,1)S(1)}, u32[]{:S(2)}) copy-start(bf16[2,512,128]{2,1,0:T(8,128)(2,1)S(1)} %collective-permute-done.11.refs_3_) | copy-start | bytes 786436
  44.5 6.7 %copy-start.24 = (bf16[80,512]{1,0:T(8,128)(2,1)}, bf16[80,512]{1,0:T(8,128)(2,1)S(1)}, u32[]{:S(2)}) copy-start(bf16[80,512]{1,0:T(8,128)(2,1)S(1)} %collective-permute-done.7.refs_1_) | copy-start | bytes 245764
  58.0 15.4 %collective-permute-start.25 = (bf16[128,2048]{1,0:T(8,128)(2,1)S(1)}, bf16[128,2048]{1,0:T(8,128)(2,1)S(1)}, u32[]{:S(2)}, u32[]{:S(2)}) collective-permute-start(bf16[128,2048]{1,0:T(8,128)(2,1)S(1)} %copy-done), channel_id=1, source_target_pairs={{0,2},{1,7},{2,4},{3,1},{4,6},{5,3},{6,0},{7,5},{8,10},{9,15},{10,... | collective-permute-start | bytes 1572872 | tf_op jit(solution)/shard_map/ppermute | solution.py:54
  58.2 11.3 %collective-permute-start.14 = (bf16[2,512,128]{2,1,0:T(8,128)(2,1)S(1)}, bf16[2,512,128]{2,1,0:T(8,128)(2,1)S(1)}, u32[]{:S(2)}, u32[]{:S(2)}) collective-permute-start(bf16[2,512,128]{2,1,0:T(8,128)(2,1)S(1)} %collective-permute-done.11.refs_3_), channel_id=1, source_target_pairs={{0,32},{1,225},{2,34},{3,227},{4,36},{5,229},{6,38},{7,231},{8,40}... | collective-permute-start | bytes 786440 | tf_op jit(solution)/shard_map/ppermute | solution.py:54
  58.9 11.5 %collective-permute-start.15 = (bf16[2,512,128]{2,1,0:T(8,128)(2,1)S(1)}, bf16[2,512,128]{2,1,0:T(8,128)(2,1)S(1)}, u32[]{:S(2)}, u32[]{:S(2)}) collective-permute-start(bf16[2,512,128]{2,1,0:T(8,128)(2,1)S(1)} %collective-permute-done.12.refs_5_), channel_id=1, source_target_pairs={{0,224},{1,33},{2,226},{3,35},{4,228},{5,37},{6,230},{7,39},{8,232... | collective-permute-start | bytes 786440 | tf_op jit(solution)/shard_map/ppermute | solution.py:54
  63.9 10.7 %collective-permute-start.17 = (bf16[2,512,128]{2,1,0:T(8,128)(2,1)S(1)}, bf16[2,512,128]{2,1,0:T(8,128)(2,1)S(1)}, u32[]{:S(2)}, u32[]{:S(2)}) collective-permute-start(bf16[2,512,128]{2,1,0:T(8,128)(2,1)S(1)} %collective-permute-done.11.refs_3_), channel_id=1, source_target_pairs={{0,1},{1,0},{2,3},{3,2},{4,5},{5,4},{6,7},{7,6},{8,9},{9,8},{10,11... | collective-permute-start | bytes 786440 | tf_op jit(solution)/shard_map/ppermute | solution.py:54
  64.5 10.3 %collective-permute-start.16 = (bf16[2,512,128]{2,1,0:T(8,128)(2,1)S(1)}, bf16[2,512,128]{2,1,0:T(8,128)(2,1)S(1)}, u32[]{:S(2)}, u32[]{:S(2)}) collective-permute-start(bf16[2,512,128]{2,1,0:T(8,128)(2,1)S(1)} %collective-permute-done.12.refs_5_), channel_id=1, source_target_pairs={{0,1},{1,0},{2,3},{3,2},{4,5},{5,4},{6,7},{7,6},{8,9},{9,8},{10,11... | collective-permute-start | bytes 786440 | tf_op jit(solution)/shard_map/ppermute | solution.py:54
  69.5 21.8 %copy-start.17 = (bf16[2,512,128]{2,1,0:T(8,128)(2,1)}, bf16[2,512,128]{2,1,0:T(8,128)(2,1)S(1)}, u32[]{:S(2)}) copy-start(bf16[2,512,128]{2,1,0:T(8,128)(2,1)S(1)} %collective-permute-done.14.refs_3_) | copy-start | bytes 786436
  70.5 20.8 %copy-start.18 = (bf16[2,512,128]{2,1,0:T(8,128)(2,1)}, bf16[2,512,128]{2,1,0:T(8,128)(2,1)S(1)}, u32[]{:S(2)}) copy-start(bf16[2,512,128]{2,1,0:T(8,128)(2,1)S(1)} %collective-permute-done.15.refs_5_) | copy-start | bytes 786436
  70.5 9.0 %collective-permute-start.18 = (bf16[2,512,128]{2,1,0:T(8,128)(2,1)S(1)}, bf16[2,512,128]{2,1,0:T(8,128)(2,1)S(1)}, u32[]{:S(2)}, u32[]{:S(2)}) collective-permute-start(bf16[2,512,128]{2,1,0:T(8,128)(2,1)S(1)} %collective-permute-done.14.refs_3_), channel_id=1, source_target_pairs={{0,32},{1,225},{2,34},{3,227},{4,36},{5,229},{6,38},{7,231},{8,40}... | collective-permute-start | bytes 786440 | tf_op jit(solution)/shard_map/ppermute | solution.py:54
  71.0 26.6 %collective-permute-start.26 = (bf16[128,2048]{1,0:T(8,128)(2,1)S(1)}, bf16[128,2048]{1,0:T(8,128)(2,1)S(1)}, u32[]{:S(2)}, u32[]{:S(2)}) collective-permute-start(bf16[128,2048]{1,0:T(8,128)(2,1)S(1)} %copy-done), channel_id=1, source_target_pairs={{0,6},{1,3},{2,0},{3,5},{4,2},{5,7},{6,4},{7,1},{8,14},{9,11},{10,... | collective-permute-start | bytes 1572872 | tf_op jit(solution)/shard_map/ppermute | solution.py:54
  73.4 25.6 %copy-start.1 = (bf16[128,2048]{1,0:T(8,128)(2,1)}, bf16[128,2048]{1,0:T(8,128)(2,1)S(1)}, u32[]{:S(2)}) copy-start(bf16[128,2048]{1,0:T(8,128)(2,1)S(1)} %collective-permute-done.25.refs_1_) | copy-start | bytes 1572868
  73.4 18.0 %collective-permute-start.21 = (bf16[2,512,128]{2,1,0:T(8,128)(2,1)S(1)}, bf16[2,512,128]{2,1,0:T(8,128)(2,1)}, u32[]{:S(2)}, u32[]{:S(2)}) collective-permute-start(bf16[2,512,128]{2,1,0:T(8,128)(2,1)S(1)} %collective-permute-done.14.refs_3_), channel_id=1, source_target_pairs={{0,1},{1,0},{2,3},{3,2},{4,5},{5,4},{6,7},{7,6},{8,9},{9,8},{10,11... | collective-permute-start | bytes 786440 | tf_op jit(solution)/shard_map/ppermute | solution.py:54
  74.6 17.3 %collective-permute-start.20 = (bf16[2,512,128]{2,1,0:T(8,128)(2,1)S(1)}, bf16[2,512,128]{2,1,0:T(8,128)(2,1)S(1)}, u32[]{:S(2)}, u32[]{:S(2)}) collective-permute-start(bf16[2,512,128]{2,1,0:T(8,128)(2,1)S(1)} %collective-permute-done.15.refs_5_), channel_id=1, source_target_pairs={{0,1},{1,0},{2,3},{3,2},{4,5},{5,4},{6,7},{7,6},{8,9},{9,8},{10,11... | collective-permute-start | bytes 786440 | tf_op jit(solution)/shard_map/ppermute | solution.py:54
  74.7 16.5 %collective-permute-start.19 = (bf16[2,512,128]{2,1,0:T(8,128)(2,1)S(1)}, bf16[2,512,128]{2,1,0:T(8,128)(2,1)}, u32[]{:S(2)}, u32[]{:S(2)}) collective-permute-start(bf16[2,512,128]{2,1,0:T(8,128)(2,1)S(1)} %collective-permute-done.15.refs_5_), channel_id=1, source_target_pairs={{0,224},{1,33},{2,226},{3,35},{4,228},{5,37},{6,230},{7,39},{8,232... | collective-permute-start | bytes 786440 | tf_op jit(solution)/shard_map/ppermute | solution.py:54
  79.4 12.5 %copy-start.14 = (bf16[2,512,128]{2,1,0:T(8,128)(2,1)}, bf16[2,512,128]{2,1,0:T(8,128)(2,1)S(1)}, u32[]{:S(2)}) copy-start(bf16[2,512,128]{2,1,0:T(8,128)(2,1)S(1)} %collective-permute-done.18.refs_3_) | copy-start | bytes 786436
  79.4 19.4 %collective-permute-start.27 = (bf16[128,2048]{1,0:T(8,128)(2,1)S(1)}, bf16[128,2048]{1,0:T(8,128)(2,1)S(1)}, u32[]{:S(2)}, u32[]{:S(2)}) collective-permute-start(bf16[128,2048]{1,0:T(8,128)(2,1)S(1)} %collective-permute-done.25.refs_1_), channel_id=1, source_target_pairs={{0,2},{1,7},{2,4},{3,1},{4,6},{5,3},{6,0},{7,5},{8,10},{9,15},{10,... | collective-permute-start | bytes 1572872 | tf_op jit(solution)/shard_map/ppermute | solution.py:54
  91.3 7.6 %collective-permute-start.23 = (bf16[2,512,128]{2,1,0:T(8,128)(2,1)}, bf16[2,512,128]{2,1,0:T(8,128)(2,1)}, u32[]{:S(2)}, u32[]{:S(2)}) collective-permute-start(bf16[2,512,128]{2,1,0:T(8,128)(2,1)} %collective-permute-done.19.refs_5_), channel_id=1, source_target_pairs={{0,1},{1,0},{2,3},{3,2},{4,5},{5,4},{6,7},{7,6},{8,9},{9,8},{10,11... | collective-permute-start | bytes 786440 | tf_op jit(solution)/shard_map/ppermute | solution.py:54
  91.4 8.1 %collective-permute-start.24 = (bf16[2,512,128]{2,1,0:T(8,128)(2,1)S(1)}, bf16[2,512,128]{2,1,0:T(8,128)(2,1)}, u32[]{:S(2)}, u32[]{:S(2)}) collective-permute-start(bf16[2,512,128]{2,1,0:T(8,128)(2,1)S(1)} %collective-permute-done.18.refs_3_), channel_id=1, source_target_pairs={{0,1},{1,0},{2,3},{3,2},{4,5},{5,4},{6,7},{7,6},{8,9},{9,8},{10,11... | collective-permute-start | bytes 786440 | tf_op jit(solution)/shard_map/ppermute | solution.py:54
  91.9 7.4 %collective-permute-start.22 = (bf16[2,512,128]{2,1,0:T(8,128)(2,1)S(1)}, bf16[2,512,128]{2,1,0:T(8,128)(2,1)}, u32[]{:S(2)}, u32[]{:S(2)}) collective-permute-start(bf16[2,512,128]{2,1,0:T(8,128)(2,1)S(1)} %collective-permute-done.18.refs_3_), channel_id=1, source_target_pairs={{0,32},{1,225},{2,34},{3,227},{4,36},{5,229},{6,38},{7,231},{8,40}... | collective-permute-start | bytes 786440 | tf_op jit(solution)/shard_map/ppermute | solution.py:54
  97.6 10.6 %copy-start.2 = (bf16[128,2048]{1,0:T(8,128)(2,1)}, bf16[128,2048]{1,0:T(8,128)(2,1)S(1)}, u32[]{:S(2)}) copy-start(bf16[128,2048]{1,0:T(8,128)(2,1)S(1)} %collective-permute-done.26.refs_2_) | copy-start | bytes 1572868
  97.6 10.6 %collective-permute-start.28 = (bf16[128,2048]{1,0:T(8,128)(2,1)S(1)}, bf16[128,2048]{1,0:T(8,128)(2,1)S(1)}, u32[]{:S(2)}, u32[]{:S(2)}) collective-permute-start(bf16[128,2048]{1,0:T(8,128)(2,1)S(1)} %copy-done), channel_id=1, source_target_pairs={{0,1},{1,0},{2,3},{3,2},{4,5},{5,4},{6,7},{7,6},{8,9},{9,8},{10,11... | collective-permute-start | bytes 1572872 | tf_op jit(solution)/shard_map/ppermute | solution.py:54
  98.8 9.5 %copy-start.3 = (bf16[128,2048]{1,0:T(8,128)(2,1)}, bf16[128,2048]{1,0:T(8,128)(2,1)S(1)}, u32[]{:S(2)}) copy-start(bf16[128,2048]{1,0:T(8,128)(2,1)S(1)} %collective-permute-done.27.refs_3_) | copy-start | bytes 1572868
  98.8 9.5 %collective-permute-start.30 = (bf16[128,2048]{1,0:T(8,128)(2,1)S(1)}, bf16[128,2048]{1,0:T(8,128)(2,1)S(1)}, u32[]{:S(2)}, u32[]{:S(2)}) collective-permute-start(bf16[128,2048]{1,0:T(8,128)(2,1)S(1)} %collective-permute-done.26.refs_2_), channel_id=1, source_target_pairs={{0,1},{1,0},{2,3},{3,2},{4,5},{5,4},{6,7},{7,6},{8,9},{9,8},{10,11... | collective-permute-start | bytes 1572872 | tf_op jit(solution)/shard_map/ppermute | solution.py:54
  98.9 9.4 %collective-permute-start.29 = (bf16[128,2048]{1,0:T(8,128)(2,1)S(1)}, bf16[128,2048]{1,0:T(8,128)(2,1)}, u32[]{:S(2)}, u32[]{:S(2)}) collective-permute-start(bf16[128,2048]{1,0:T(8,128)(2,1)S(1)} %collective-permute-done.25.refs_1_), channel_id=1, source_target_pairs={{0,1},{1,0},{2,3},{3,2},{4,5},{5,4},{6,7},{7,6},{8,9},{9,8},{10,11... | collective-permute-start | bytes 1572872 | tf_op jit(solution)/shard_map/ppermute | solution.py:54
  99.3 9.0 %collective-permute-start.31 = (bf16[128,2048]{1,0:T(8,128)(2,1)S(1)}, bf16[128,2048]{1,0:T(8,128)(2,1)}, u32[]{:S(2)}, u32[]{:S(2)}) collective-permute-start(bf16[128,2048]{1,0:T(8,128)(2,1)S(1)} %collective-permute-done.27.refs_3_), channel_id=1, source_target_pairs={{0,1},{1,0},{2,3},{3,2},{4,5},{5,4},{6,7},{7,6},{8,9},{9,8},{10,11... | collective-permute-start | bytes 1572872 | tf_op jit(solution)/shard_map/ppermute | solution.py:54
  99.5 8.9 %collective-permute-start.32 = (bf16[2,512,128]{2,1,0:T(8,128)(2,1)}, bf16[2,512,128]{2,1,0:T(8,128)(2,1)S(1)}, u32[]{:S(2)}, u32[]{:S(2)}) collective-permute-start(bf16[2,512,128]{2,1,0:T(8,128)(2,1)} %collective-permute-done.22.refs_3_), channel_id=1, source_target_pairs={{0,1},{1,0},{2,3},{3,2},{4,5},{5,4},{6,7},{7,6},{8,9},{9,8},{10,11... | collective-permute-start | bytes 786440 | tf_op jit(solution)/shard_map/ppermute | solution.py:54
  116.3 9.8 %collective-permute-start.33 = (bf16[64,512]{1,0:T(8,128)(2,1)}, bf16[64,512]{1,0:T(8,128)(2,1)S(1)}, u32[]{:S(2)}, u32[]{:S(2)}) collective-permute-start(bf16[64,512]{1,0:T(8,128)(2,1)} %get-tuple-element.89), channel_id=1, source_target_pairs={{0,0},{16,1},{2,2},{18,3},{4,4},{20,5},{6,6},{22,7},{1,8},{17,9},{... | collective-permute-start | bytes 196616 | tf_op jit(solution)/shard_map/ppermute | solution.py:54
  117.8 12.3 %collective-permute-start.34 = (bf16[64,512]{1,0:T(8,128)(2,1)}, bf16[64,512]{1,0:T(8,128)(2,1)S(1)}, u32[]{:S(2)}, u32[]{:S(2)}) collective-permute-start(bf16[64,512]{1,0:T(8,128)(2,1)} %get-tuple-element.90), channel_id=1, source_target_pairs={{8,0},{24,1},{10,2},{26,3},{12,4},{28,5},{14,6},{30,7},{9,8},{25,9... | collective-permute-start | bytes 196616 | tf_op jit(solution)/shard_map/ppermute | solution.py:54
  (15 other events, 30.0 us)
